TPU v7x, 32 devices: a whole 2x2x4 slice. The times are simulated.
32 devices in a mesh: grp: 2 (over y), sp: 4 (over z), tp: 4 (over x, core).
Axes of the slice: x: 2, y: 2, z: 4, core: 2. Of those that a mesh axis runs over, the one named last changes fastest.
Arguments:
- queries: bfloat16 [1024, 2048], P(('grp', 'sp'), 'tp'), parts along dimension 0, may hold values from -8 to 8
- keys: bfloat16 [1024, 1024], P(('grp', 'sp'), 'tp'), parts along dimension 0, may hold values from -6 to 6
- values: bfloat16 [1024, 1024], P(('grp', 'sp'), 'tp'), parts along dimension 0, may hold values from -6 to 6
- head_bias: float32 [16], P('tp'), may hold values from -15 to -5
- documents: int32 [1024], P(('grp', 'sp')), parts along dimension 0, may hold values from 0 to 2, never falling along the last dimension, each value on 1 to 384 neighbouring positions
- w_out: bfloat16 [2048, 2048], P('tp'), may hold values from -0.125 to 0.125
- resid: bfloat16 [1024, 2048], P(('grp', 'sp', 'tp')), parts along dimension 0, may hold values from -6 to 6
- norm_gain: float32 [2048], replicated, may hold values from 0.1 to 1.9
- expert_ids: int32 [1024, 2], P(('grp', 'sp', 'tp')), parts along dimension 0, may hold values from 0 to 3, all different within a row; in each aligned block of 32 rows (0 to 31, 32 to 63, ...) at most 32 rows name the same one
- expert_gates: float32 [1024, 2], P(('grp', 'sp', 'tp')), parts along dimension 0, may hold values from 0.1 to 0.9
- w_gate: bfloat16 [4, 2048, 3072], P('sp', None, 'tp'), may hold values from -0.125 to 0.125
- w_up: bfloat16 [4, 2048, 3072], P('sp', None, 'tp'), may hold values from -0.125 to 0.125
- w_down: bfloat16 [4, 3072, 2048], P('sp', 'tp'), may hold values from -0.109375 to 0.109375
Outputs:
- layer_out: bfloat16 [1024, 2048], P(('grp', 'sp', 'tp')), parts along dimension 0
There are 2 independent parts, one for each index of `grp`. A program takes and returns all parts, laid end to end along the dimension named above; an argument that names none is the same for every part. Nothing has to cross between parts.
Inputs may be any that keep to these rules, and one draw needn't show every extreme that they name: Document numbers never fall along the sequence; each of the 3 documents holds at least one position and the longest exactly 384 positions. `expert_ids`: each position names 2 different experts. Among the 32 positions of one device (aligned blocks of 32 rows) no expert is named more than 32 times, and in some block some expert exactly 32 times.
All inputs are finite; a program needn't handle non-finite values.
Results may differ from a plain program's by a relative error of at most 0.012.
Values may be sent and summed in bfloat16 or wider, within the bound.
No kernel may reach another device: no remote copies, remote signals or barrier semaphores. Data moves between devices by JAX's collectives and lax.ppermute only.
A program may use at most 64 MiB of HBM per device.

v0:
```python
import jax
import jax.numpy as jnp
from jax import lax
from jax.sharding import PartitionSpec as P

D = 2048
HEADS = 16
KV_HEADS = 8
DH = 128
TOPK = 2


def passed_along(value, axis, steps):
    count = lax.axis_size(axis)
    initial, last = (max(0, -steps), min(count, count - steps))
    return lax.ppermute(value, axis, [(source, source + steps) for source in range(initial, last)])


def attend_terms(query_grid, bias_grid, key_block, value_block, live, carried):
    kv_local = bias_grid.shape[0]
    key_count = key_block.shape[0]
    logits = (
        jnp.einsum(
            "qgrd,sgd->grqs",
            query_grid,
            key_block.reshape(key_count, kv_local, DH),
            preferred_element_type=jnp.float32,
        )
        * DH ** (-0.5)
        + bias_grid[:, :, None, None]
    )
    keep = jnp.where(live, jax.nn.log_sigmoid(-logits), 0.0)
    after = lax.cumsum(keep, axis=3, reverse=True) - keep + carried[:, :, :, None]
    weight = jnp.where(live, jnp.exp(jax.nn.log_sigmoid(logits) + after), 0.0).astype(jnp.bfloat16)
    partial_mix = jnp.einsum(
        "grqs,sgd->qgrd",
        weight,
        value_block.reshape(key_count, kv_local, DH),
        preferred_element_type=jnp.float32,
    )
    return (partial_mix, jnp.sum(keep, axis=3))


def local(
    queries,
    keys,
    values,
    head_bias,
    documents,
    w_out,
    resid,
    norm_gain,
    expert_ids,
    expert_gates,
    w_gate,
    w_up,
    w_down,
):
    tok_count = queries.shape[0]
    kv_local = keys.shape[1] // DH
    group_size = HEADS // KV_HEADS
    sp_count = lax.axis_size("sp")
    tp_count = lax.axis_size("tp")
    sp_index = lax.axis_index("sp")
    query_grid = queries.reshape(tok_count, kv_local, group_size, DH)
    bias_grid = head_bias.reshape(kv_local, group_size)
    doc_here = documents.astype(jnp.bfloat16)
    doc_column = doc_here.reshape(tok_count, 1)
    local_pos = jnp.arange(tok_count, dtype=jnp.int32)
    live_local = (local_pos[None, :] < local_pos[:, None]) & (
        documents[None, :] == documents[:, None]
    )
    zero_carry = jnp.zeros((kv_local, group_size, tok_count), jnp.float32)
    mix_total, carried = attend_terms(query_grid, bias_grid, keys, values, live_local, zero_carry)

    def visit(turn_index, state):
        mix_sum, carry_sum, key_block, value_block, doc_block = state
        key_block, value_block, doc_block = passed_along(
            (key_block, value_block, doc_block), "sp", 1
        )
        live = (doc_block[:, 0][None, :] == doc_here[:, None]) & (sp_index - turn_index >= 0)
        partial_mix, block_keep = attend_terms(
            query_grid, bias_grid, key_block, value_block, live, carry_sum
        )
        return (mix_sum + partial_mix, carry_sum + block_keep, key_block, value_block, doc_block)

    mix_total, carried, key_last, value_last, doc_last = lax.fori_loop(
        1, sp_count, visit, (mix_total, carried, keys, values, doc_column)
    )
    mixed = mix_total.reshape(tok_count, kv_local * group_size * DH).astype(jnp.bfloat16)
    projected = lax.psum_scatter(
        jnp.dot(mixed, w_out, preferred_element_type=jnp.float32).astype(jnp.bfloat16),
        "tp",
        scatter_dimension=0,
        tiled=True,
    ).astype(jnp.float32)
    middle = (resid.astype(jnp.float32) + projected).astype(jnp.bfloat16)
    middle_value = middle.astype(jnp.float32)
    normed = (
        middle_value
        * lax.rsqrt(jnp.mean(middle_value * middle_value, axis=1, keepdims=True) + 1e-06)
        * norm_gain
    ).astype(jnp.bfloat16)
    row_count = normed.shape[0]
    expert_count = w_gate.shape[0] * sp_count
    slot_limit = min(row_count, max(2, 2 * TOPK * row_count // expert_count))
    flat_ids = expert_ids.reshape(-1)
    onehot_ids = (flat_ids[:, None] == jnp.arange(expert_count, dtype=jnp.int32)[None, :]).astype(
        jnp.int32
    )
    earlier = jnp.cumsum(onehot_ids, axis=0) - onehot_ids
    slot_ids = jnp.sum(earlier * onehot_ids, axis=1)
    target = flat_ids * slot_limit + slot_ids
    placing = (
        jnp.arange(expert_count * slot_limit, dtype=jnp.int32)[:, None] == target[None, :]
    ).astype(jnp.bfloat16)
    by_token = jnp.sum(placing.reshape(expert_count * slot_limit, row_count, TOPK), axis=2)
    outgoing = jnp.dot(by_token, normed, preferred_element_type=jnp.float32).astype(jnp.bfloat16)
    outgoing = outgoing.reshape(expert_count, slot_limit, D)
    arrived = lax.all_to_all(outgoing, "sp", split_axis=0, concat_axis=0, tiled=True)
    gathered = lax.all_gather(arrived, "tp", axis=0, tiled=True)
    expert_rows = gathered.reshape(-1, D)
    gate_value = jnp.dot(expert_rows, w_gate[0], preferred_element_type=jnp.float32)
    up_value = jnp.dot(expert_rows, w_up[0], preferred_element_type=jnp.float32)
    hidden = (jax.nn.silu(gate_value) * up_value).astype(jnp.bfloat16)
    partial_out = jnp.dot(hidden, w_down[0], preferred_element_type=jnp.float32)
    summed = lax.psum_scatter(
        partial_out.reshape(tp_count, sp_count * slot_limit, D).astype(jnp.bfloat16),
        "tp",
        scatter_dimension=0,
        tiled=True,
    ).astype(jnp.float32)
    expert_result = summed.reshape(sp_count, slot_limit, D).astype(jnp.bfloat16)
    returned = lax.all_to_all(expert_result, "sp", split_axis=0, concat_axis=0, tiled=True)
    routed = jnp.dot(placing.T, returned.reshape(-1, D), preferred_element_type=jnp.float32)
    combined = jnp.sum(expert_gates[:, :, None] * routed.reshape(row_count, TOPK, D), axis=1)
    return (middle_value + combined).astype(jnp.bfloat16)


def solution(mesh):
    return jax.shard_map(
        local,
        mesh=mesh,
        in_specs=(
            P(("grp", "sp"), "tp"),
            P(("grp", "sp"), "tp"),
            P(("grp", "sp"), "tp"),
            P("tp"),
            P(("grp", "sp")),
            P("tp", None),
            P(("grp", "sp", "tp"), None),
            P(),
            P(("grp", "sp", "tp"), None),
            P(("grp", "sp", "tp"), None),
            P("sp", None, "tp"),
            P("sp", None, "tp"),
            P("sp", "tp", None),
        ),
        out_specs=P(("grp", "sp", "tp"), None),
        check_vma=False,
    )
```

profile of v0, /device:TPU:0, one launch (start us, length us, event | category | flops | bytes accessed | tf_op | source)
XLA Modules:
  0.0 232.2 jit_solution(13194715823110891600)
XLA Ops:
  6.5 0.9 fusion.50
  7.5 1.3 fusion.58
  8.8 1.5 reshape.106
  10.2 1.6 copy.78
  11.8 1.5 reshape.108
  13.3 1.6 copy.79
  14.8 1.0 copy.73
  15.9 1.3 add.157
  17.1 0.8 copy.80
  17.9 2.4 %fusion.56 = (f32[2,2,128]{2,1,0:T(2,128)}, f32[2,2,128,128]{2,3,1,0:T(8,128)S(1)}, f32[2,2,128,128]{2,3,1,0:T(8,128)}) fusion(pred[128,128]{0,1:T(8,128)(4,1)S(1)} %fusion.50, f32[2,2]{1,0:T(2,128)} %add.157, bf16[128,2,2,128]{0,3,2,1:T(8,128)(2,1)S(1)} %bitcast.78, bf16[128,2,128,1]{2,1,0,3:T(2,128)(2,1)} %bitcast.81), kind=kOutput, calls=%fused_computation.74 | convolution fusion | flops 17497600 | bytes 739344 | tf_op jit(solution)/shard_map/qgrd,sgd->grqs/dot_general | solution.py:23
  20.3 5.1 %reduce_window_sum.31 = f32[2,2,128,128]{2,3,1,0:T(8,128)} reduce-window(f32[2,2,128,128]{2,3,1,0:T(8,128)S(1)} %get-tuple-element.239, f32[]{:T(128)} %constant.57.clone.1), window={size=1x1x1x128 pad=0_0x0_0x0_0x0_127}, to_apply=%region_0.1 | reduce-window | flops 8323072 | bytes 524292 | tf_op jit(solution)/shard_map/attend_terms/reduce_window_sum | solution.py:33
  25.5 2.3 convolution_bitcast_fusion.1
  27.7 69.8 %while.21 = (s32[]{:T(128)}, f32[128,2,2,128]{3,0,2,1:T(8,128)}, f32[2,2,128]{2,1,0:T(2,128)}, bf16[128,256]{0,1:T(8,128)(2,1)}, bf16[128,256]{0,1:T(8,128)(2,1)...) while((s32[]{:T(128)}, f32[128,2,2,128]{3,0,2,1:T(8,128)}, ...), condition=%wide.region_5.6_spmd, body=%wide.region_2.5_spmd.sunk | while | flops 44105732 | bytes 3207487 | solution.py:87
  27.7 4.9 %collective-permute-start.1 = (bf16[128,1]{0,1:T(2,128)(2,1)}, bf16[128,1]{0,1:T(2,128)(2,1)S(1)}, u32[]{:S(2)}, u32[]{:S(2)}) collective-permute-start(bf16[128,1]{0,1:T(2,128)(2,1)} %get-tuple-element.328), channel_id=1, source_target_pairs={{0,4},{4,8},{8,12},{1,5},{5,9},{9,13},{2,6},{6,10},{10,14},{3,7},{... | collective-permute-start | bytes 776 | tf_op jit(solution)/shard_map/while/body/eval_jaxpr/ppermute | solution.py:16
  32.7 3.5 %collective-permute-start.2 = (bf16[128,256]{0,1:T(8,128)(2,1)}, bf16[128,256]{0,1:T(8,128)(2,1)S(1)}, u32[]{:S(2)}, u32[]{:S(2)}) collective-permute-start(bf16[128,256]{0,1:T(8,128)(2,1)} %get-tuple-element.326), channel_id=1, source_target_pairs={{0,4},{4,8},{8,12},{1,5},{5,9},{9,13},{2,6},{6,10},{10,14},{3,7},{... | collective-permute-start | bytes 196616 | tf_op jit(solution)/shard_map/while/body/eval_jaxpr/ppermute | solution.py:16
  36.2 3.5 %collective-permute-start = (bf16[128,256]{0,1:T(8,128)(2,1)}, bf16[128,256]{0,1:T(8,128)(2,1)S(1)}, u32[]{:S(2)}, u32[]{:S(2)}) collective-permute-start(bf16[128,256]{0,1:T(8,128)(2,1)} %get-tuple-element.327), channel_id=1, source_target_pairs={{0,4},{4,8},{8,12},{1,5},{5,9},{9,13},{2,6},{6,10},{10,14},{3,7},{... | collective-permute-start | bytes 196616 | tf_op jit(solution)/shard_map/while/body/eval_jaxpr/ppermute | solution.py:16
  41.7 2.6 %fusion.80 = (f32[2,2,128]{2,1,0:T(2,128)}, f32[2,2,128,128]{2,3,1,0:T(8,128)}, f32[2,2,128,128]{2,3,1,0:T(8,128)}) fusion(pred[128,128]{0,1:T(8,128)(4,1)S(1)} %compare_and_fusion.2, f32[2,2]{1,0:T(2,128)S(1)} %add.252, bf16[128,2,128,1]{0,2,3,1:T(8,128)(2,1)S(1)} %bitcast.74, bf16[128,2,2,128]{3,0,2,1:T(8,128)(2,1)} %get-tuple-element.344), kind=kOutput, calls=%fused_computation.19.clone.1 | convolution fusion | flops 17497600 | bytes 739344 | tf_op jit(solution)/shard_map/while/body/eval_jaxpr/qgrd,sgd->grqs/dot_general | solution.py:23
  44.3 5.4 %reduce_window_sum.34 = f32[2,2,128,128]{2,3,1,0:T(8,128)S(1)} reduce-window(f32[2,2,128,128]{2,3,1,0:T(8,128)} %get-tuple-element.307, f32[]{:T(128)} %constant.57.clone.1..sunk), window={size=1x1x1x128 pad=0_0x0_0x0_0x0_127}, to_apply=%region_3.3 | reduce-window | flops 8323072 | bytes 524292 | tf_op jit(solution)/shard_map/while/body/eval_jaxpr/reduce_window_sum | solution.py:33
  49.7 2.3 fusion.81
  52.0 1.3 add.253
  54.5 1.9 collective-permute-start.1
  56.4 2.6 %collective-permute-start.2 = (bf16[128,256]{0,1:T(8,128)(2,1)}, bf16[128,256]{0,1:T(8,128)(2,1)S(1)}, u32[]{:S(2)}, u32[]{:S(2)}) collective-permute-start(bf16[128,256]{0,1:T(8,128)(2,1)} %get-tuple-element.326), channel_id=1, source_target_pairs={{0,4},{4,8},{8,12},{1,5},{5,9},{9,13},{2,6},{6,10},{10,14},{3,7},{... | collective-permute-start | bytes 196616 | tf_op jit(solution)/shard_map/while/body/eval_jaxpr/ppermute | solution.py:16
  59.0 1.9 collective-permute-start
  63.0 2.6 %fusion.80 = (f32[2,2,128]{2,1,0:T(2,128)}, f32[2,2,128,128]{2,3,1,0:T(8,128)}, f32[2,2,128,128]{2,3,1,0:T(8,128)}) fusion(pred[128,128]{0,1:T(8,128)(4,1)S(1)} %compare_and_fusion.2, f32[2,2]{1,0:T(2,128)S(1)} %add.252, bf16[128,2,128,1]{0,2,3,1:T(8,128)(2,1)S(1)} %bitcast.74, bf16[128,2,2,128]{3,0,2,1:T(8,128)(2,1)} %get-tuple-element.344), kind=kOutput, calls=%fused_computation.19.clone.1 | convolution fusion | flops 17497600 | bytes 739344 | tf_op jit(solution)/shard_map/while/body/eval_jaxpr/qgrd,sgd->grqs/dot_general | solution.py:23
  65.6 5.4 %reduce_window_sum.34 = f32[2,2,128,128]{2,3,1,0:T(8,128)S(1)} reduce-window(f32[2,2,128,128]{2,3,1,0:T(8,128)} %get-tuple-element.307, f32[]{:T(128)} %constant.57.clone.1..sunk), window={size=1x1x1x128 pad=0_0x0_0x0_0x0_127}, to_apply=%region_3.3 | reduce-window | flops 8323072 | bytes 524292 | tf_op jit(solution)/shard_map/while/body/eval_jaxpr/reduce_window_sum | solution.py:33
  71.0 2.3 fusion.81
  73.3 1.3 add.253
  75.8 2.7 %collective-permute-start.1 = (bf16[128,1]{0,1:T(2,128)(2,1)}, bf16[128,1]{0,1:T(2,128)(2,1)S(1)}, u32[]{:S(2)}, u32[]{:S(2)}) collective-permute-start(bf16[128,1]{0,1:T(2,128)(2,1)} %get-tuple-element.328), channel_id=1, source_target_pairs={{0,4},{4,8},{8,12},{1,5},{5,9},{9,13},{2,6},{6,10},{10,14},{3,7},{... | collective-permute-start | bytes 776 | tf_op jit(solution)/shard_map/while/body/eval_jaxpr/ppermute | solution.py:16
  78.5 2.2 collective-permute-start.2
  80.7 2.0 collective-permute-start
  84.7 2.6 %fusion.80 = (f32[2,2,128]{2,1,0:T(2,128)}, f32[2,2,128,128]{2,3,1,0:T(8,128)}, f32[2,2,128,128]{2,3,1,0:T(8,128)}) fusion(pred[128,128]{0,1:T(8,128)(4,1)S(1)} %compare_and_fusion.2, f32[2,2]{1,0:T(2,128)S(1)} %add.252, bf16[128,2,128,1]{0,2,3,1:T(8,128)(2,1)S(1)} %bitcast.74, bf16[128,2,2,128]{3,0,2,1:T(8,128)(2,1)} %get-tuple-element.344), kind=kOutput, calls=%fused_computation.19.clone.1 | convolution fusion | flops 17497600 | bytes 739344 | tf_op jit(solution)/shard_map/while/body/eval_jaxpr/qgrd,sgd->grqs/dot_general | solution.py:23
  87.3 5.4 %reduce_window_sum.34 = f32[2,2,128,128]{2,3,1,0:T(8,128)S(1)} reduce-window(f32[2,2,128,128]{2,3,1,0:T(8,128)} %get-tuple-element.307, f32[]{:T(128)} %constant.57.clone.1..sunk), window={size=1x1x1x128 pad=0_0x0_0x0_0x0_127}, to_apply=%region_3.3 | reduce-window | flops 8323072 | bytes 524292 | tf_op jit(solution)/shard_map/while/body/eval_jaxpr/reduce_window_sum | solution.py:33
  92.7 2.3 fusion.81
  95.0 1.3 add.253
  97.5 1.1 copy.81
  98.6 2.9 %convolution_convert_fusion.1 = bf16[128,2048]{1,0:T(8,128)(2,1)} fusion(bf16[128,512]{0,1:T(8,128)(2,1)S(1)} %bitcast.79, bf16[512,2048]{1,0:T(8,128)(2,1)} %param.20), kind=kOutput, calls=%fused_computation.28 | convolution fusion | flops 268697600 | bytes 2752512 | tf_op jit(solution)/shard_map/dot_general | solution.py:92
  102.6 19.0 %reduce-scatter.3.cloned.1.call-done = bf16[32,2048]{1,0:T(8,128)(2,1)} async-done(((bf16[128,2048]{1,0:T(8,128)(2,1)}), bf16[32,2048]{1,0:T(8,128)(2,1)}) %reduce-scatter.3.cloned.1.call-update) | async-done | bytes 131088 | tf_op jit(solution)/shard_map/reduce_scatter | solution.py:91
  121.6 1.1 fusion.31
  122.7 1.2 convolution_convert_fusion
  123.9 18.8 %all_to_all.10 = bf16[4,32,2048]{2,1,0:T(8,128)(2,1)} all-to-all(bf16[4,32,2048]{2,1,0:T(8,128)(2,1)S(1)} %bitcast.73), channel_id=1, replica_groups=mesh['grp'=2,'sp'=4,'tp'=4] {'sp'}, dimensions={0} | all-to-all | bytes 1048576 | tf_op jit(solution)/shard_map/all_to_all | solution.py:120
  142.8 20.8 %all-gather.2.cloned.1.call-done = bf16[16,32,2048]{2,1,0:T(8,128)(2,1)} async-done(((bf16[4,32,2048]{2,1,0:T(8,128)(2,1)}), bf16[16,32,2048]{2,1,0:T(8,128)(2,1)}) %all-gather.2.cloned.1.call-update) | async-done | bytes 2097168 | tf_op jit(solution)/shard_map/all_gather | solution.py:121
  163.6 4.5 %fusion.21 = f32[512,768]{1,0:T(8,128)S(1)} fusion(bf16[512,2048]{1,0:T(8,128)(2,1)} %bitcast.83, bf16[1,2048,768]{2,1,0:T(8,128)(2,1)} %param.25), kind=kOutput, calls=%fused_computation.24 | convolution fusion | flops 1610612736 | bytes 6815744 | tf_op jit(solution)/shard_map/dot_general | solution.py:123
  168.1 1.9 multiply_convert_fusion
  170.0 3.2 %fusion.23 = bf16[4,128,2048]{2,1,0:T(8,128)(2,1)} fusion(bf16[4,128,768]{2,1,0:T(8,128)(2,1)S(1)} %bitcast.85, bf16[1,768,2048]{2,1,0:T(8,128)(2,1)S(1)} %copy-done), kind=kOutput, calls=%fused_computation.26 | convolution fusion | flops 1611661312 | bytes 6029312 | tf_op jit(solution)/shard_map/dot_general | solution.py:126
  173.3 31.3 %reduce-scatter.5.cloned.1.call-done = bf16[1,128,2048]{2,1,0:T(8,128)(2,1)} async-done(((bf16[4,128,2048]{2,1,0:T(8,128)(2,1)}), bf16[1,128,2048]{2,1,0:T(8,128)(2,1)}) %reduce-scatter.5.cloned.1.call-update) | async-done | bytes 524304 | tf_op jit(solution)/shard_map/reduce_scatter | solution.py:127
  204.6 4.6 %all-to-all-start.1 = ((bf16[4,32,2048]{2,1,0:T(8,128)(2,1)}), bf16[4,32,2048]{2,1,0:T(8,128)(2,1)}, u32[]{:S(2)}, u32[]{:S(2)}) async-start(bf16[4,32,2048]{2,1,0:T(8,128)(2,1)} %bitcast.76), calls=%async_computation.3 | async-start | bytes 1048576 | tf_op jit(solution)/shard_map/all_to_all | solution.py:134
  209.3 14.3 %all-to-all-done.1 = bf16[4,32,2048]{2,1,0:T(8,128)(2,1)} async-done(((bf16[4,32,2048]{2,1,0:T(8,128)(2,1)}), bf16[4,32,2048]{2,1,0:T(8,128)(2,1)}, u32[]{:S(2)}, u32[]{:S(2)}) %all-to-all-start.1) | async-done | bytes 524320 | tf_op jit(solution)/shard_map/all_to_all | solution.py:134
  223.6 1.3 fusion.28
  (60 shorter events, 11.7 us)
Async XLA Ops:
  6.5 163.5 %copy-start = (bf16[1,768,2048]{2,1,0:T(8,128)(2,1)S(1)}, bf16[1,768,2048]{2,1,0:T(8,128)(2,1)}, u32[]{:S(2)}) copy-start(bf16[1,768,2048]{2,1,0:T(8,128)(2,1)} %param.27) | copy-start | bytes 9437188
  6.5 115.0 %reduce-scatter.3.cloned.1.call-start = ((), (), s32[]{:S(2)}) async-start(), calls=%async_computation.4 | async-start | bytes 655360 | tf_op jit(solution)/shard_map/reduce_scatter | solution.py:91
  27.7 12.7 %collective-permute-start.1 = (bf16[128,1]{0,1:T(2,128)(2,1)}, bf16[128,1]{0,1:T(2,128)(2,1)S(1)}, u32[]{:S(2)}, u32[]{:S(2)}) collective-permute-start(bf16[128,1]{0,1:T(2,128)(2,1)} %get-tuple-element.328), channel_id=1, source_target_pairs={{0,4},{4,8},{8,12},{1,5},{5,9},{9,13},{2,6},{6,10},{10,14},{3,7},{... | collective-permute-start | bytes 776 | tf_op jit(solution)/shard_map/while/body/eval_jaxpr/ppermute | solution.py:16
  32.7 9.0 %collective-permute-start.2 = (bf16[128,256]{0,1:T(8,128)(2,1)}, bf16[128,256]{0,1:T(8,128)(2,1)S(1)}, u32[]{:S(2)}, u32[]{:S(2)}) collective-permute-start(bf16[128,256]{0,1:T(8,128)(2,1)} %get-tuple-element.326), channel_id=1, source_target_pairs={{0,4},{4,8},{8,12},{1,5},{5,9},{9,13},{2,6},{6,10},{10,14},{3,7},{... | collective-permute-start | bytes 196616 | tf_op jit(solution)/shard_map/while/body/eval_jaxpr/ppermute | solution.py:16
  36.2 13.5 %collective-permute-start = (bf16[128,256]{0,1:T(8,128)(2,1)}, bf16[128,256]{0,1:T(8,128)(2,1)S(1)}, u32[]{:S(2)}, u32[]{:S(2)}) collective-permute-start(bf16[128,256]{0,1:T(8,128)(2,1)} %get-tuple-element.327), channel_id=1, source_target_pairs={{0,4},{4,8},{8,12},{1,5},{5,9},{9,13},{2,6},{6,10},{10,14},{3,7},{... | collective-permute-start | bytes 196616 | tf_op jit(solution)/shard_map/while/body/eval_jaxpr/ppermute | solution.py:16
  54.5 7.2 %collective-permute-start.1 = (bf16[128,1]{0,1:T(2,128)(2,1)}, bf16[128,1]{0,1:T(2,128)(2,1)S(1)}, u32[]{:S(2)}, u32[]{:S(2)}) collective-permute-start(bf16[128,1]{0,1:T(2,128)(2,1)} %get-tuple-element.328), channel_id=1, source_target_pairs={{0,4},{4,8},{8,12},{1,5},{5,9},{9,13},{2,6},{6,10},{10,14},{3,7},{... | collective-permute-start | bytes 776 | tf_op jit(solution)/shard_map/while/body/eval_jaxpr/ppermute | solution.py:16
  56.4 6.6 %collective-permute-start.2 = (bf16[128,256]{0,1:T(8,128)(2,1)}, bf16[128,256]{0,1:T(8,128)(2,1)S(1)}, u32[]{:S(2)}, u32[]{:S(2)}) collective-permute-start(bf16[128,256]{0,1:T(8,128)(2,1)} %get-tuple-element.326), channel_id=1, source_target_pairs={{0,4},{4,8},{8,12},{1,5},{5,9},{9,13},{2,6},{6,10},{10,14},{3,7},{... | collective-permute-start | bytes 196616 | tf_op jit(solution)/shard_map/while/body/eval_jaxpr/ppermute | solution.py:16
  59.0 12.0 %collective-permute-start = (bf16[128,256]{0,1:T(8,128)(2,1)}, bf16[128,256]{0,1:T(8,128)(2,1)S(1)}, u32[]{:S(2)}, u32[]{:S(2)}) collective-permute-start(bf16[128,256]{0,1:T(8,128)(2,1)} %get-tuple-element.327), channel_id=1, source_target_pairs={{0,4},{4,8},{8,12},{1,5},{5,9},{9,13},{2,6},{6,10},{10,14},{3,7},{... | collective-permute-start | bytes 196616 | tf_op jit(solution)/shard_map/while/body/eval_jaxpr/ppermute | solution.py:16
  75.8 7.6 %collective-permute-start.1 = (bf16[128,1]{0,1:T(2,128)(2,1)}, bf16[128,1]{0,1:T(2,128)(2,1)S(1)}, u32[]{:S(2)}, u32[]{:S(2)}) collective-permute-start(bf16[128,1]{0,1:T(2,128)(2,1)} %get-tuple-element.328), channel_id=1, source_target_pairs={{0,4},{4,8},{8,12},{1,5},{5,9},{9,13},{2,6},{6,10},{10,14},{3,7},{... | collective-permute-start | bytes 776 | tf_op jit(solution)/shard_map/while/body/eval_jaxpr/ppermute | solution.py:16
  78.5 6.2 %collective-permute-start.2 = (bf16[128,256]{0,1:T(8,128)(2,1)}, bf16[128,256]{0,1:T(8,128)(2,1)S(1)}, u32[]{:S(2)}, u32[]{:S(2)}) collective-permute-start(bf16[128,256]{0,1:T(8,128)(2,1)} %get-tuple-element.326), channel_id=1, source_target_pairs={{0,4},{4,8},{8,12},{1,5},{5,9},{9,13},{2,6},{6,10},{10,14},{3,7},{... | collective-permute-start | bytes 196616 | tf_op jit(solution)/shard_map/while/body/eval_jaxpr/ppermute | solution.py:16
  80.7 12.0 %collective-permute-start = (bf16[128,256]{0,1:T(8,128)(2,1)}, bf16[128,256]{0,1:T(8,128)(2,1)S(1)}, u32[]{:S(2)}, u32[]{:S(2)}) collective-permute-start(bf16[128,256]{0,1:T(8,128)(2,1)} %get-tuple-element.327), channel_id=1, source_target_pairs={{0,4},{4,8},{8,12},{1,5},{5,9},{9,13},{2,6},{6,10},{10,14},{3,7},{... | collective-permute-start | bytes 196616 | tf_op jit(solution)/shard_map/while/body/eval_jaxpr/ppermute | solution.py:16
  97.5 4.2 %copy-start.4 = (s32[32,2]{0,1:T(2,128)S(1)}, s32[32,2]{0,1:T(2,128)}, u32[]{:S(2)}) copy-start(s32[32,2]{0,1:T(2,128)} %param.23) | copy-start | bytes 772
  97.5 24.1 %copy-start.1 = (bf16[32,2048]{1,0:T(8,128)(2,1)S(1)}, bf16[32,2048]{1,0:T(8,128)(2,1)}, u32[]{:S(2)}) copy-start(bf16[32,2048]{1,0:T(8,128)(2,1)} %param.21) | copy-start | bytes 393220
  97.5 25.1 %copy-start.3 = (f32[2048]{0:T(1024)S(1)}, f32[2048]{0:T(1024)}, u32[]{:S(2)}) copy-start(f32[2048]{0:T(1024)} %param.22) | copy-start | bytes 24580
  101.5 62.1 %all-gather.2.cloned.1.call-start = ((), (), s32[]{:S(2)}) async-start(), calls=%async_computation.5 | async-start | bytes 2621440 | tf_op jit(solution)/shard_map/all_gather | solution.py:121
  142.8 61.8 %reduce-scatter.5.cloned.1.call-start = ((), (), s32[]{:S(2)}) async-start(), calls=%async_computation.6 | async-start | bytes 2621440 | tf_op jit(solution)/shard_map/reduce_scatter | solution.py:127
  163.6 4.5 %copy-start.6 = (bf16[1,2048,768]{2,1,0:T(8,128)(2,1)S(1)}, bf16[1,2048,768]{2,1,0:T(8,128)(2,1)}, u32[]{:S(2)}) copy-start(bf16[1,2048,768]{2,1,0:T(8,128)(2,1)} %param.26) | copy-start | bytes 9437188
  163.6 4.5 %copy-start.7 = (bf16[16,32,2048]{2,1,0:T(8,128)(2,1)S(1)}, bf16[16,32,2048]{2,1,0:T(8,128)(2,1)}, u32[]{:S(2)}) copy-start(bf16[16,32,2048]{2,1,0:T(8,128)(2,1)} %all-gather.2.cloned.1.call-done) | copy-start | bytes 6291460
  173.2 50.4 %copy-start.5 = (f32[32,2]{0,1:T(2,128)S(1)}, f32[32,2]{0,1:T(2,128)}, u32[]{:S(2)}) copy-start(f32[32,2]{0,1:T(2,128)} %param.24) | copy-start | bytes 772
  173.2 51.7 %copy-start.2 = (bf16[32,2048]{1,0:T(8,128)(2,1)S(1)}, bf16[32,2048]{1,0:T(8,128)(2,1)}, u32[]{:S(2)}) copy-start(bf16[32,2048]{1,0:T(8,128)(2,1)} %reduce-scatter.3.cloned.1.call-done) | copy-start | bytes 393220
  204.6 19.1 %all-to-all-start.1 = ((bf16[4,32,2048]{2,1,0:T(8,128)(2,1)}), bf16[4,32,2048]{2,1,0:T(8,128)(2,1)}, u32[]{:S(2)}, u32[]{:S(2)}) async-start(bf16[4,32,2048]{2,1,0:T(8,128)(2,1)} %bitcast.76), calls=%async_computation.3 | async-start | bytes 1048576 | tf_op jit(solution)/shard_map/all_to_all | solution.py:134
Sparse Core Ops, SparseCore 0:
  101.7 19.8 reduce-scatter.2
  142.9 20.6 all-gather.1
  173.4 31.1 reduce-scatter.4
where the time goes:
time: 233 us; the launch traced here: 232 us
  waiting for transfers between devices  85.5 us (37%)
  matrix products  34.5 us (15%)
  other arithmetic  31.5 us (14%)
  starting transfers between devices  30.1 us (13%)
  blocking collectives  18.8 us (8%)
  local copies, waits for them, and re-layouts  18.3 us (8%)
  between operations  13.2 us (6%)
    reduce_scatter x1, waiting for transfers between devices, local(): lax.psum_scatter(partial_out.reshape(tp_count, sp_count * slot_limit, D)....  31.3 us
    ppermute x9, starting transfers between devices, passed_along(): lax.ppermute(value, axis, [(source, source + steps) for source in range(i...  25.2 us
    another operation x4, other arithmetic, attend_terms(): lax.cumsum(keep, axis=3, reverse=True) - keep + carried[:, :, :, None]  21.2 us
    all_gather x1, waiting for transfers between devices, local(): gathered = lax.all_gather(arrived, 'tp', axis=0, tiled=True)  20.8 us
    reduce_scatter x1, waiting for transfers between devices, local(): lax.psum_scatter(jnp.dot(mixed, w_out, preferred_element_type=jnp.float32...  19 us
    all_to_all x1, blocking collectives, local(): lax.all_to_all(outgoing, 'sp', split_axis=0, concat_axis=0, tiled=True)  18.8 us
    all_to_all x1, waiting for transfers between devices, local(): lax.all_to_all(expert_result, 'sp', split_axis=0, concat_axis=0, tiled=True)  14.3 us
    dot_general x4, matrix products, attend_terms(): jnp.einsum('qgrd,sgd->grqs', query_grid, key_block.reshape(key_count, kv_...  10.4 us
  transfers between devices with their start and end apart: 13, of which 4 were waited for; matrix products, arithmetic and copies ran while one was open for 13% of the time, Pallas kernels for 0%

commit v1 on v0

--- a/solution.py
+++ b/solution.py
@@ -1,6 +1,10 @@
+import functools
+
 import jax
 import jax.numpy as jnp
 from jax import lax
+from jax.experimental import pallas as pl
+from jax.experimental.pallas import tpu as pltpu
 from jax.sharding import PartitionSpec as P
 
 D = 2048
@@ -8,6 +12,205 @@
 KV_HEADS = 8
 DH = 128
 TOPK = 2
+DOC_ROWS = 16
+DIRECT_KEYS = 1024
+VMEM = pl.BlockSpec(memory_space=pltpu.VMEM)
+SMEM = pl.BlockSpec(memory_space=pltpu.SMEM)
+
+
+def shifted(value, steps, wrap):
+    count = lax.axis_size("sp")
+    pairs = [(i, (i + steps) % count) for i in range(count) if wrap or 0 <= i + steps < count]
+    return lax.ppermute(value, "sp", pairs)
+
+
+def swapped(value, mask):
+    count = lax.axis_size("tp")
+    return lax.ppermute(value, "tp", [(i, i ^ mask) for i in range(count)])
+
+
+def block_terms(q_ref, bias_ref, key_of, value_of, live, carry):
+    heads = q_ref.shape[1] // DH
+    group = HEADS // KV_HEADS
+    rows = q_ref.shape[0]
+    parts = []
+    for h in range(heads):
+        part = lax.dot_general(
+            q_ref[:, h * DH : (h + 1) * DH],
+            key_of(h // group),
+            (((1,), (1,)), ((), ())),
+            preferred_element_type=jnp.float32,
+        )
+        parts.append(part * DH ** (-0.5) + bias_ref[h])
+    logits = jnp.concatenate(parts, axis=0)
+    live = jnp.concatenate([live] * heads, axis=0)
+    soft = jnp.log1p(jnp.exp(-jnp.abs(logits)))
+    keep = jnp.where(live, -jnp.maximum(logits, 0.0) - soft, 0.0)
+    keys = logits.shape[1]
+    later = lax.broadcasted_iota(jnp.int32, (keys, keys), 0) > lax.broadcasted_iota(
+        jnp.int32, (keys, keys), 1
+    )
+    later = later.astype(jnp.float32).astype(jnp.bfloat16)
+    high = keep.astype(jnp.bfloat16)
+    low = (keep - high.astype(jnp.float32)).astype(jnp.bfloat16)
+    after = jnp.dot(high, later, preferred_element_type=jnp.float32) + jnp.dot(
+        low, later, preferred_element_type=jnp.float32
+    )
+    weight = jnp.where(
+        live, jnp.exp(jnp.minimum(logits, 0.0) - soft + after + carry), 0.0
+    ).astype(jnp.bfloat16)
+    mixes = [
+        jnp.dot(
+            weight[h * rows : (h + 1) * rows], value_of(h // group), preferred_element_type=jnp.float32
+        )
+        for h in range(heads)
+    ]
+    return jnp.concatenate(mixes, axis=1), carry + jnp.sum(keep, axis=1, keepdims=True)
+
+
+def here_kernel(q_ref, k_ref, v_ref, bias_ref, col_ref, row_ref, mix_ref, carry_ref):
+    rows = q_ref.shape[0]
+    causal = lax.broadcasted_iota(jnp.int32, (rows, rows), 1) < lax.broadcasted_iota(
+        jnp.int32, (rows, rows), 0
+    )
+    live = causal & (col_ref[...] == row_ref[...])
+    carry = jnp.zeros((rows * (q_ref.shape[1] // DH), 1), jnp.float32)
+    mix, carry = block_terms(
+        q_ref,
+        bias_ref,
+        lambda g: k_ref[:, g * DH : (g + 1) * DH],
+        lambda g: v_ref[:, g * DH : (g + 1) * DH],
+        live,
+        carry,
+    )
+    mix_ref[...] = mix
+    carry_ref[...] = jnp.broadcast_to(carry, carry_ref.shape)
+
+
+def away_kernel(count, order, place_ref, q_ref, bias_ref, col_ref, mix_ref, carry_ref, w_ref, *refs):
+    sent, outs, mixed_ref = refs[:count], refs[count:-1], refs[-1]
+    rows = q_ref.shape[0]
+    width = q_ref.shape[1] // (HEADS // KV_HEADS)
+    mix = mix_ref[...]
+    carry = carry_ref[:, 0:1]
+    for step, block in enumerate(sent, 1):
+        doc_row = block[rows : rows + 1, 0:rows].astype(jnp.float32)
+        doc_row = jnp.where(place_ref[0] >= step, doc_row, -1.0)
+        live = col_ref[...] == doc_row
+        term, carry = block_terms(
+            q_ref,
+            bias_ref,
+            lambda g, block=block: block[0:rows, g * DH : (g + 1) * DH],
+            lambda g, block=block: block[0:rows, width + g * DH : width + (g + 1) * DH],
+            live,
+            carry,
+        )
+        mix = mix + term
+    mixed_ref[...] = mix
+    share = rows // len(order)
+    for mask, out in zip(order, outs):
+        first = pl.multiple_of((place_ref[1] ^ mask) * share, share)
+        piece = mixed_ref[pl.ds(first, share), :].astype(jnp.bfloat16)
+        out[...] = jnp.dot(piece, w_ref[...], preferred_element_type=jnp.float32).astype(jnp.bfloat16)
+
+
+def norm_kernel(resid_ref, gain_ref, *refs):
+    pieces, middle_ref, normed_ref = refs[:-2], refs[-2], refs[-1]
+    total = pieces[0][...].astype(jnp.float32)
+    for piece in pieces[1:]:
+        total = total + piece[...].astype(jnp.float32)
+    middle = (resid_ref[...].astype(jnp.float32) + total).astype(jnp.bfloat16)
+    middle_ref[...] = middle
+    value = middle.astype(jnp.float32)
+    scale = lax.rsqrt(jnp.mean(value * value, axis=1, keepdims=True) + 1e-06)
+    normed_ref[...] = (value * scale * gain_ref[...]).astype(jnp.bfloat16)
+
+
+def cost(flops, nbytes):
+    return pl.CostEstimate(flops=flops, bytes_accessed=nbytes, transcendentals=0)
+
+
+def middle_direct(queries, keys, values, head_bias, documents, w_out, resid, norm_gain):
+    rows, width = queries.shape
+    kv_width = keys.shape[1]
+    sp_count = lax.axis_size("sp")
+    tp_count = lax.axis_size("tp")
+    doc_real = documents.astype(jnp.bfloat16)
+    doc_rows = jnp.zeros((DOC_ROWS, 2 * kv_width), jnp.bfloat16)
+    doc_rows = doc_rows.at[0, :rows].set(doc_real)
+    packed = jnp.concatenate([jnp.concatenate([keys, values], axis=1), doc_rows], axis=0)
+    sent = [shifted(packed, steps, False) for steps in range(1, sp_count)]
+    col = documents.astype(jnp.float32).reshape(rows, 1)
+    row = documents.astype(jnp.float32).reshape(1, rows)
+    heads = width // DH
+    mix, carry = pl.pallas_call(
+        here_kernel,
+        out_shape=(
+            jax.ShapeDtypeStruct((rows, width), jnp.float32),
+            jax.ShapeDtypeStruct((rows * heads, DH), jnp.float32),
+        ),
+        in_specs=[VMEM, VMEM, VMEM, SMEM, VMEM, VMEM],
+        out_specs=(VMEM, VMEM),
+        cost_estimate=cost(6 * 10**9, 10**6),
+        name="attend_here",
+    )(queries, keys, values, head_bias, col, row)
+    place = jnp.stack([lax.axis_index("sp"), lax.axis_index("tp")]).astype(jnp.int32)
+    order = list(range(tp_count))
+    share = rows // tp_count
+    pieces = pl.pallas_call(
+        functools.partial(away_kernel, sp_count - 1, order),
+        out_shape=[jax.ShapeDtypeStruct((share, D), jnp.bfloat16)] * tp_count,
+        in_specs=[SMEM, VMEM, SMEM, VMEM, VMEM, VMEM, VMEM] + [VMEM] * (sp_count - 1),
+        out_specs=[VMEM] * tp_count,
+        scratch_shapes=[pltpu.VMEM((rows, width), jnp.float32)],
+        cost_estimate=cost(10 * 10**9, 4 * 10**6),
+        name="attend_away",
+    )(place, queries, head_bias, col, mix, carry, w_out, *sent)
+    arrived = [pieces[0]] + [swapped(pieces[mask], mask) for mask in order[:0:-1]]
+    return pl.pallas_call(
+        norm_kernel,
+        out_shape=[jax.ShapeDtypeStruct((share, D), jnp.bfloat16)] * 2,
+        in_specs=[VMEM] * (2 + tp_count),
+        out_specs=[VMEM] * 2,
+        cost_estimate=cost(10**8, 10**6),
+        name="middle_norm",
+    )(resid, norm_gain.reshape(1, D), *arrived)
+
+
+def experts_dense(middle, normed, expert_ids, expert_gates, w_gate, w_up, w_down):
+    rows = normed.shape[0]
+    sp_count = lax.axis_size("sp")
+    tp_count = lax.axis_size("tp")
+    masks = [1 << bit for bit in range(tp_count.bit_length() - 1)]
+    steps = [0] + [s for pair in zip(range(1, sp_count), range(sp_count - 1, 0, -1)) for s in pair]
+    steps = list(dict.fromkeys(steps))
+    half = (len(steps) + 1) // 2
+    moved = {s: normed if s == 0 else shifted(normed, s, True) for s in steps}
+    pieces = {}
+    for chunk in (steps[:half], steps[half:]):
+        held = jnp.concatenate([moved[s] for s in chunk], axis=0)
+        for mask in masks[::-1]:
+            held = jnp.concatenate([held, swapped(held, mask)], axis=0)
+        gate_value = jnp.dot(held, w_gate[0], preferred_element_type=jnp.float32)
+        up_value = jnp.dot(held, w_up[0], preferred_element_type=jnp.float32)
+        hidden = (jax.nn.silu(gate_value) * up_value).astype(jnp.bfloat16)
+        result = jnp.dot(hidden, w_down[0], preferred_element_type=jnp.float32).astype(jnp.bfloat16)
+        for mask in masks:
+            kept = result.shape[0] // 2
+            result = (
+                result[:kept].astype(jnp.float32) + swapped(result[kept:], mask).astype(jnp.float32)
+            ).astype(jnp.bfloat16)
+        for at, s in enumerate(chunk):
+            pieces[s] = result[at * rows : (at + 1) * rows]
+    own = lax.axis_index("sp")
+    total = middle.astype(jnp.float32)
+    combined = jnp.zeros_like(total)
+    for s in steps:
+        piece = pieces[s] if s == 0 else shifted(pieces[s], -s, True)
+        chosen = expert_ids == (own + s) % sp_count
+        scale = jnp.sum(jnp.where(chosen, expert_gates, 0.0), axis=1, keepdims=True)
+        combined = combined + scale * piece.astype(jnp.float32)
+    return (total + combined).astype(jnp.bfloat16)
 
 
 def passed_along(value, axis, steps):
@@ -41,26 +244,11 @@
     return (partial_mix, jnp.sum(keep, axis=3))
 
 
-def local(
-    queries,
-    keys,
-    values,
-    head_bias,
-    documents,
-    w_out,
-    resid,
-    norm_gain,
-    expert_ids,
-    expert_gates,
-    w_gate,
-    w_up,
-    w_down,
-):
+def middle_ring(queries, keys, values, head_bias, documents, w_out, resid, norm_gain):
     tok_count = queries.shape[0]
     kv_local = keys.shape[1] // DH
     group_size = HEADS // KV_HEADS
     sp_count = lax.axis_size("sp")
-    tp_count = lax.axis_size("tp")
     sp_index = lax.axis_index("sp")
     query_grid = queries.reshape(tok_count, kv_local, group_size, DH)
     bias_grid = head_bias.reshape(kv_local, group_size)
@@ -101,9 +289,15 @@
         * lax.rsqrt(jnp.mean(middle_value * middle_value, axis=1, keepdims=True) + 1e-06)
         * norm_gain
     ).astype(jnp.bfloat16)
+    return middle, normed
+
+
+def experts_routed(middle, normed, expert_ids, expert_gates, w_gate, w_up, w_down, slot_limit):
+    middle_value = middle.astype(jnp.float32)
+    sp_count = lax.axis_size("sp")
+    tp_count = lax.axis_size("tp")
     row_count = normed.shape[0]
     expert_count = w_gate.shape[0] * sp_count
-    slot_limit = min(row_count, max(2, 2 * TOPK * row_count // expert_count))
     flat_ids = expert_ids.reshape(-1)
     onehot_ids = (flat_ids[:, None] == jnp.arange(expert_count, dtype=jnp.int32)[None, :]).astype(
         jnp.int32
@@ -137,6 +331,38 @@
     return (middle_value + combined).astype(jnp.bfloat16)
 
 
+def local(
+    queries,
+    keys,
+    values,
+    head_bias,
+    documents,
+    w_out,
+    resid,
+    norm_gain,
+    expert_ids,
+    expert_gates,
+    w_gate,
+    w_up,
+    w_down,
+):
+    sp_count = lax.axis_size("sp")
+    tp_count = lax.axis_size("tp")
+    paired = tp_count & (tp_count - 1) == 0
+    direct = paired and sp_count * keys.shape[0] <= DIRECT_KEYS and sp_count > 1
+    middle_of = middle_direct if direct else middle_ring
+    middle, normed = middle_of(
+        queries, keys, values, head_bias, documents, w_out, resid, norm_gain
+    )
+    row_count = normed.shape[0]
+    expert_count = w_gate.shape[0] * sp_count
+    slot_limit = min(row_count, max(2, 2 * TOPK * row_count // expert_count))
+    routing = (middle, normed, expert_ids, expert_gates, w_gate, w_up, w_down)
+    if paired and slot_limit == row_count and w_gate.shape[0] == 1 and sp_count > 1:
+        return experts_dense(*routing)
+    return experts_routed(*routing, slot_limit)
+
+
 def solution(mesh):
     return jax.shard_map(
         local,

time: 233 us -> 118 us (0.51)
  waiting for transfers between devices: 85.5 us -> 45.1 us
  other arithmetic: 31.5 us -> 8.24 us
  blocking collectives: 18.8 us -> 0 us
  matrix products: 34.5 us -> 17 us
  between operations: 13.2 us -> 0.22 us
  Pallas kernels: 0 us -> 10.2 us
  local copies, waits for them, and re-layouts: 18.3 us -> 10.7 us
  starting transfers between devices: 30.1 us -> 26 us
    reduce_scatter x2 -> x0, waiting for transfers between devices: 50.3 us -> none  [the longest x1 31.3 us: local(): lax.psum_scatter(partial_out.reshape(tp_count, sp_count * slot_limit, D)....]
    ppermute x9 -> x20, waiting for transfers between devices: 0.02 us -> 45.1 us  [the longest x11 27.7 us: swapped(): return lax.ppermute(value, 'tp', [(i, i ^ mask) for i in range(count)])]
    all_gather x1 -> x0, waiting for transfers between devices: 20.8 us -> none  [local(): gathered = lax.all_gather(arrived, 'tp', axis=0, tiled=True)]
    another operation x5 -> x2, other arithmetic: 21.3 us -> 2 us  [the longest x4 21.2 us: attend_terms(): lax.cumsum(keep, axis=3, reverse=True) - keep + carried[:, :, :, None]]
    all_to_all x1 -> x0, blocking collectives: 18.8 us -> none  [local(): lax.all_to_all(outgoing, 'sp', split_axis=0, concat_axis=0, tiled=True)]
    dot_general x14 -> x4, matrix products: 34.5 us -> 17 us  [the longest x2 11.1 us: experts_dense(): jnp.dot(hidden, w_down[0], preferred_element_type=jnp.float32)]
    all_to_all x1 -> x0, waiting for transfers between devices: 14.3 us -> none  [local(): lax.all_to_all(expert_result, 'sp', split_axis=0, concat_axis=0, tiled=True)]
    while x13 -> x0, local copies, waits for them, and re-layouts: 10.5 us -> none
  transfers between devices with their start and end apart: 13 -> 20, of which waited for: 4 -> 10; matrix products, arithmetic and copies ran while one was open for 13% -> 24% of each run, Pallas kernels for 0% -> 2%
where the time goes in v1:
time: 118 us
  waiting for transfers between devices  45.1 us (38%)
  starting transfers between devices  26 us (22%)
  matrix products  17 us (14%)
  local copies, waits for them, and re-layouts  10.7 us (9%)
  Pallas kernels  10.2 us (9%)
  other arithmetic  8.24 us (7%)
    ppermute x11, waiting for transfers between devices, swapped(): return lax.ppermute(value, 'tp', [(i, i ^ mask) for i in range(count)])  27.7 us
    ppermute x9, starting transfers between devices, shifted(): return lax.ppermute(value, 'sp', pairs)  19.2 us
    ppermute x9, waiting for transfers between devices, shifted(): return lax.ppermute(value, 'sp', pairs)  17.4 us
    dot_general x2, matrix products, experts_dense(): jnp.dot(hidden, w_down[0], preferred_element_type=jnp.float32)  11.1 us
    ppermute x11, starting transfers between devices, swapped(): return lax.ppermute(value, 'tp', [(i, i ^ mask) for i in range(count)])  6.83 us
    dot_general x2, matrix products, experts_dense(): up_value = jnp.dot(held, w_up[0], preferred_element_type=jnp.float32)  5.94 us
    pallas_call x1, Pallas kernels, middle_direct(): pl.pallas_call(functools.partial(away_kernel, sp_count - 1, order), out_s...  5.83 us
    unnamed x30, local copies, waits for them, and re-layouts  4.24 us
  transfers between devices with their start and end apart: 20, of which 10 were waited for; matrix products, arithmetic and copies ran while one was open for 24% of the time, Pallas kernels for 2%

profile of v1, /device:TPU:0, one launch (start us, length us, event | category | flops | bytes accessed | tf_op | source)
XLA Modules:
  0.0 117.5 jit_solution(4766686987609247582)
XLA Ops:
  0.0 1.3 %convert_bitcast_fusion = (bf16[1,128]{1,0:T(2,128)(2,1)S(1)}, f32[1,128]{1,0:T(1,128)}, f32[128,1]{0,1:T(1,128)S(1)}) fusion(s32[128]{0:T(128)} %param.19), kind=kLoop, calls=%fused_computation.47 | loop fusion | flops 256 | bytes 1792 | tf_op jit(solution)/shard_map/reshape.30
  1.3 0.9 fusion.29
  2.2 5.0 %collective-permute-start = (bf16[144,512]{1,0:T(8,128)(2,1)S(1)}, bf16[144,512]{1,0:T(8,128)(2,1)S(1)}, u32[]{:S(2)}, u32[]{:S(2)}) collective-permute-start(bf16[144,512]{1,0:T(8,128)(2,1)S(1)} %fusion.29), channel_id=1, source_target_pairs={{0,4},{4,8},{8,12},{1,5},{5,9},{9,13},{2,6},{6,10},{10,14},{3,7},{... | collective-permute-start | bytes 442376 | tf_op jit(solution)/shard_map/ppermute | solution.py:24
  7.2 5.2 %collective-permute-start.1 = (bf16[144,512]{1,0:T(8,128)(2,1)S(1)}, bf16[144,512]{1,0:T(8,128)(2,1)}, u32[]{:S(2)}, u32[]{:S(2)}) collective-permute-start(bf16[144,512]{1,0:T(8,128)(2,1)S(1)} %fusion.29), channel_id=1, source_target_pairs={{0,8},{4,12},{1,9},{5,13},{2,10},{6,14},{3,11},{7,15},{16,24},{20,... | collective-permute-start | bytes 442376 | tf_op jit(solution)/shard_map/ppermute | solution.py:24
  12.4 1.9 %collective-permute-start.2 = (bf16[144,512]{1,0:T(8,128)(2,1)S(1)}, bf16[144,512]{1,0:T(8,128)(2,1)}, u32[]{:S(2)}, u32[]{:S(2)}) collective-permute-start(bf16[144,512]{1,0:T(8,128)(2,1)S(1)} %fusion.29), channel_id=1, source_target_pairs={{0,12},{1,13},{2,14},{3,15},{16,28},{17,29},{18,30},{19,31}} | collective-permute-start | bytes 442376 | tf_op jit(solution)/shard_map/ppermute | solution.py:24
  14.3 0.7 copy.15.col_ref
  15.0 2.4 %attend_here.1 = (f32[128,512]{1,0:T(8,128)}, f32[512,128]{1,0:T(8,128)}) custom-call(bf16[128,512]{1,0:T(8,128)(2,1)} %q_ref.3, bf16[128,256]{1,0:T(8,128)(2,1)} %k_ref.1, bf16[128,256]{1,0:T(8,128)(2,1)} %v_ref.1, f32[4]{0:T(128)} %bias_ref.3, f32[128,1]{1,0:T(8,128)} %copy.15.col_ref, f32[1,128]{1,0:T(1,128)} %get-tuple-element.40.row_ref), custom_call_target="tpu_custom_call" | custom-call | flops 6000000000 | bytes 1000000 | tf_op jit(solution)/shard_map/attend_here/pallas_call | solution.py:146
  17.4 0.7 pad_add_fusion.place_ref
  18.1 0.6 copy-done.11
  18.7 5.8 %attend_away.1 = (bf16[32,2048]{1,0:T(8,128)(2,1)}, bf16[32,2048]{1,0:T(8,128)(2,1)}, bf16[32,2048]{1,0:T(8,128)(2,1)}, bf16[32,2048]{1,0:T(8,128)(2,1)}) custom-call(s32[2]{0:T(128)} %pad_add_fusion.place_ref, bf16[128,512]{1,0:T(8,128)(2,1)} %q_ref.3, f32[4]{0:T(128)} %bias_ref.3, f32[128,1]{1,0:T(8,128)} %copy.15.col_ref, ...), custom_call_target="tpu_custom_call" | custom-call | flops 10000000000 | bytes 4000000 | tf_op jit(solution)/shard_map/attend_away/pallas_call | solution.py:160
  24.5 0.4 collective-permute-start.3
  24.9 1.2 %collective-permute-start.4 = (bf16[32,2048]{1,0:T(8,128)(2,1)}, bf16[32,2048]{1,0:T(8,128)(2,1)S(1)}, u32[]{:S(2)}, u32[]{:S(2)}) collective-permute-start(bf16[32,2048]{1,0:T(8,128)(2,1)} %get-tuple-element.29), channel_id=1, source_target_pairs={{0,2},{1,3},{2,0},{3,1},{4,6},{5,7},{6,4},{7,5},{8,10},{9,11},{10,... | collective-permute-start | bytes 393224 | tf_op jit(solution)/shard_map/ppermute | solution.py:29
  26.1 0.3 collective-permute-start.5
  26.4 4.1 %collective-permute-done.3.refs_1_ = bf16[32,2048]{1,0:T(8,128)(2,1)S(1)} collective-permute-done((bf16[32,2048]{1,0:T(8,128)(2,1)}, bf16[32,2048]{1,0:T(8,128)(2,1)S(1)}, u32[]{:S(2)}, u32[]{:S(2)}) %collective-permute-start.3) | collective-permute-done | bytes 131104 | tf_op jit(solution)/shard_map/ppermute | solution.py:29
  30.5 2.9 %collective-permute-done.4.refs_2_ = bf16[32,2048]{1,0:T(8,128)(2,1)S(1)} collective-permute-done((bf16[32,2048]{1,0:T(8,128)(2,1)}, bf16[32,2048]{1,0:T(8,128)(2,1)S(1)}, u32[]{:S(2)}, u32[]{:S(2)}) %collective-permute-start.4) | collective-permute-done | bytes 131104 | tf_op jit(solution)/shard_map/ppermute | solution.py:29
  33.4 0.6 copy-done.4
  34.1 2.0 %middle_norm.1 = (bf16[32,2048]{1,0:T(8,128)(2,1)}, bf16[32,2048]{1,0:T(8,128)(2,1)}) custom-call(bf16[32,2048]{1,0:T(8,128)(2,1)} %resid_ref.1, f32[1,2048]{1,0:T(1,128)} %bitcast.40, bf16[32,2048]{1,0:T(8,128)(2,1)} %get-tuple-element.27.refs_0_, bf16[32,2048]{1,0:T(8,128)(2,1)} %copy-done.3, bf16[32,2048]{1,0:T(8,128)(2,1)} %copy-done.4, ...), custom_call_target="tpu_custom_call" | custom-call | flops 100000000 | bytes 1000000 | tf_op jit(solution)/shard_map/middle_norm/pallas_call | solution.py:170
  36.1 5.5 %collective-permute-start.12 = (bf16[32,2048]{1,0:T(8,128)(2,1)}, bf16[32,2048]{1,0:T(8,128)(2,1)S(1)}, u32[]{:S(2)}, u32[]{:S(2)}) collective-permute-start(bf16[32,2048]{1,0:T(8,128)(2,1)} %get-tuple-element.32), channel_id=1, source_target_pairs={{0,12},{4,0},{8,4},{12,8},{1,13},{5,1},{9,5},{13,9},{2,14},{6,2},{... | collective-permute-start | bytes 393224 | tf_op jit(solution)/shard_map/ppermute | solution.py:24
  41.6 0.6 collective-permute-start.6
  42.3 0.9 constant_dynamic-update-slice_fusion.3
  43.2 2.7 %collective-permute-done.12 = bf16[32,2048]{1,0:T(8,128)(2,1)S(1)} collective-permute-done((bf16[32,2048]{1,0:T(8,128)(2,1)}, bf16[32,2048]{1,0:T(8,128)(2,1)S(1)}, u32[]{:S(2)}, u32[]{:S(2)}) %collective-permute-start.12) | collective-permute-done | bytes 131104 | tf_op jit(solution)/shard_map/ppermute | solution.py:24
  45.9 7.6 %collective-permute-done.13 = bf16[32,2048]{1,0:T(8,128)(2,1)S(1)} collective-permute-done((bf16[32,2048]{1,0:T(8,128)(2,1)}, bf16[32,2048]{1,0:T(8,128)(2,1)S(1)}, u32[]{:S(2)}, u32[]{:S(2)}) %collective-permute-start.13) | collective-permute-done | bytes 131104 | tf_op jit(solution)/shard_map/ppermute | solution.py:24
  53.5 0.8 collective-permute-start.14
  54.4 0.9 pad_maximum_fusion.2
  55.3 1.3 %collective-permute-start.7 = (bf16[64,2048]{1,0:T(8,128)(2,1)S(1)}, bf16[64,2048]{1,0:T(8,128)(2,1)S(1)}, u32[]{:S(2)}, u32[]{:S(2)}) collective-permute-start(bf16[64,2048]{1,0:T(8,128)(2,1)S(1)} %pad_maximum_fusion.2), channel_id=1, source_target_pairs={{0,2},{1,3},{2,0},{3,1},{4,6},{5,7},{6,4},{7,5},{8,10},{9,11},{10,... | collective-permute-start | bytes 786440 | tf_op jit(solution)/shard_map/ppermute | solution.py:29
  56.7 6.1 %collective-permute-done.14 = bf16[64,2048]{1,0:T(8,128)(2,1)S(1)} collective-permute-done((bf16[64,2048]{1,0:T(8,128)(2,1)S(1)}, bf16[64,2048]{1,0:T(8,128)(2,1)S(1)}, u32[]{:S(2)}, u32[]{:S(2)}) %collective-permute-start.14) | collective-permute-done | bytes 262176 | tf_op jit(solution)/shard_map/ppermute | solution.py:29
  62.9 4.0 %collective-permute-done.7 = bf16[64,2048]{1,0:T(8,128)(2,1)S(1)} collective-permute-done((bf16[64,2048]{1,0:T(8,128)(2,1)S(1)}, bf16[64,2048]{1,0:T(8,128)(2,1)S(1)}, u32[]{:S(2)}, u32[]{:S(2)}) %collective-permute-start.7) | collective-permute-done | bytes 262176 | tf_op jit(solution)/shard_map/ppermute | solution.py:29
  66.9 0.8 pad_maximum_fusion
  67.9 0.9 copy-done.6
  68.8 1.0 copy-done.7
  69.8 1.9 %fusion.4 = f32[256,768]{1,0:T(8,128)} fusion(bf16[256,2048]{1,0:T(8,128)(2,1)S(1)} %constant_dynamic-update-slice_fusion.4, bf16[1,2048,768]{2,1,0:T(8,128)(2,1)S(1)} %copy-done.10), kind=kOutput, calls=%fused_computation.4 | convolution fusion | flops 805306368 | bytes 4980736 | tf_op jit(solution)/shard_map/dot_general | solution.py:195
  71.6 5.6 %fusion.15 = bf16[256,2048]{1,0:T(8,128)(2,1)} fusion(bf16[1,768,2048]{2,1,0:T(8,128)(2,1)S(1)} %copy-done, f32[256,768]{1,0:T(8,128)} %fusion.4, bf16[256,2048]{1,0:T(8,128)(2,1)} %copy-done.7, bf16[1,2048,768]{2,1,0:T(8,128)(2,1)} %param.25), kind=kOutput, calls=%fused_computation.13 | convolution fusion | flops 1612316672 | bytes 9175040 | tf_op jit(solution)/shard_map/dot_general | solution.py:197
  77.2 1.9 %slice.71 = bf16[128,2048]{1,0:T(8,128)(2,1)} slice(bf16[256,2048]{1,0:T(8,128)(2,1)} %fusion.15), slice={[128:256], [0:2048]} | slice | bytes 1048576 | tf_op jit(solution)/shard_map/slice | solution.py:201
  79.1 0.5 collective-permute-start.16
  79.6 1.9 %constant_dynamic-update-slice_fusion = bf16[256,2048]{1,0:T(8,128)(2,1)} fusion(bf16[256,2048]{1,0:T(8,128)(2,1)} %copy-done.6, bf16[128,2048]{1,0:T(8,128)(2,1)} %collective-permute-done.8), kind=kLoop, calls=%fused_computation.30 | loop fusion | bytes 1048576 | tf_op jit(solution)/shard_map/concatenate | solution.py:193
  81.5 4.1 %fusion.6 = f32[256,768]{1,0:T(8,128)} fusion(bf16[256,2048]{1,0:T(8,128)(2,1)} %constant_dynamic-update-slice_fusion, bf16[1,2048,768]{2,1,0:T(8,128)(2,1)} %param.26), kind=kOutput, calls=%fused_computation.6 | convolution fusion | flops 805306368 | bytes 4980736 | tf_op jit(solution)/shard_map/dot_general | solution.py:195
  85.6 5.5 %fusion.12 = bf16[256,2048]{1,0:T(8,128)(2,1)} fusion(bf16[1,768,2048]{2,1,0:T(8,128)(2,1)S(1)} %copy-done, f32[256,768]{1,0:T(8,128)} %fusion.6, bf16[256,2048]{1,0:T(8,128)(2,1)} %constant_dynamic-update-slice_fusion, bf16[1,2048,768]{2,1,0:T(8,128)(2,1)} %param.25), kind=kOutput, calls=%fused_computation.12 | convolution fusion | flops 1612316672 | bytes 9175040 | tf_op jit(solution)/shard_map/dot_general | solution.py:197
  91.1 1.2 slice.65
  92.4 1.3 %add_convert_fusion = bf16[128,2048]{1,0:T(8,128)(2,1)S(1)} fusion(bf16[128,2048]{1,0:T(8,128)(2,1)} %collective-permute-done.16, bf16[256,2048]{1,0:T(8,128)(2,1)} %fusion.15), kind=kLoop, calls=%fused_computation.14 | loop fusion | flops 1048576 | bytes 1572864 | tf_op jit(solution)/shard_map/convert_element_type | solution.py:202
  93.8 0.9 collective-permute-start.17
  94.8 1.3 %collective-permute-start.10 = (bf16[64,2048]{1,0:T(8,128)(2,1)S(1)}, bf16[64,2048]{1,0:T(8,128)(2,1)S(1)}, u32[]{:S(2)}, u32[]{:S(2)}) collective-permute-start(bf16[64,2048]{1,0:T(8,128)(2,1)S(1)} %slice.67), channel_id=1, source_target_pairs={{0,2},{1,3},{2,0},{3,1},{4,6},{5,7},{6,4},{7,5},{8,10},{9,11},{10,... | collective-permute-start | bytes 786440 | tf_op jit(solution)/shard_map/ppermute | solution.py:29
  96.1 6.9 %collective-permute-done.17 = bf16[64,2048]{1,0:T(8,128)(2,1)S(1)} collective-permute-done((bf16[64,2048]{1,0:T(8,128)(2,1)S(1)}, bf16[64,2048]{1,0:T(8,128)(2,1)S(1)}, u32[]{:S(2)}, u32[]{:S(2)}) %collective-permute-start.17) | collective-permute-done | bytes 262176 | tf_op jit(solution)/shard_map/ppermute | solution.py:29
  103.1 0.7 fusion.36
  103.8 0.7 collective-permute-start.18
  104.5 3.7 %collective-permute-done.10 = bf16[64,2048]{1,0:T(8,128)(2,1)S(1)} collective-permute-done((bf16[64,2048]{1,0:T(8,128)(2,1)S(1)}, bf16[64,2048]{1,0:T(8,128)(2,1)S(1)}, u32[]{:S(2)}, u32[]{:S(2)}) %collective-permute-start.10) | collective-permute-done | bytes 262176 | tf_op jit(solution)/shard_map/ppermute | solution.py:29
  108.5 4.8 %collective-permute-done.19 = bf16[32,2048]{1,0:T(8,128)(2,1)} collective-permute-done((bf16[32,2048]{1,0:T(8,128)(2,1)}, bf16[32,2048]{1,0:T(8,128)(2,1)}, u32[]{:S(2)}, u32[]{:S(2)}) %collective-permute-start.19) | collective-permute-done | bytes 131104 | tf_op jit(solution)/shard_map/ppermute | solution.py:24
  113.3 2.3 %collective-permute-done.11 = bf16[32,2048]{1,0:T(8,128)(2,1)} collective-permute-done((bf16[32,2048]{1,0:T(8,128)(2,1)S(1)}, bf16[32,2048]{1,0:T(8,128)(2,1)}, u32[]{:S(2)}, u32[]{:S(2)}) %collective-permute-start.11) | collective-permute-done | bytes 131104 | tf_op jit(solution)/shard_map/ppermute | solution.py:24
  115.6 1.9 %add_convert_fusion.4 = bf16[32,2048]{1,0:T(8,128)(2,1)} fusion(bf16[32,2048]{1,0:T(8,128)(2,1)} %collective-permute-done.19, bf16[32,2048]{1,0:T(8,128)(2,1)} %collective-permute-done.18, bf16[32,2048]{1,0:T(8,128)(2,1)} %collective-permute-done.11, bf16[32,2048]{1,0:T(8,128)(2,1)} %get-tuple-element.31, bf16[64,2048]{1,0:T(8,128)(2,1)S(1)} %add_convert_fusion.3, ...), kind=kLoop, calls=%fused_computation.28 | loop fusion | flops 917504 | bytes 786944 | tf_op jit(solution)/shard_map/convert_element_type | solution.py:213
  (51 shorter events, 1.0 us)
Async XLA Ops:
  0.0 71.6 %copy-start = (bf16[1,768,2048]{2,1,0:T(8,128)(2,1)S(1)}, bf16[1,768,2048]{2,1,0:T(8,128)(2,1)}, u32[]{:S(2)}) copy-start(bf16[1,768,2048]{2,1,0:T(8,128)(2,1)} %param.27) | copy-start | bytes 9437188
  2.2 15.9 %collective-permute-start = (bf16[144,512]{1,0:T(8,128)(2,1)S(1)}, bf16[144,512]{1,0:T(8,128)(2,1)S(1)}, u32[]{:S(2)}, u32[]{:S(2)}) collective-permute-start(bf16[144,512]{1,0:T(8,128)(2,1)S(1)} %fusion.29), channel_id=1, source_target_pairs={{0,4},{4,8},{8,12},{1,5},{5,9},{9,13},{2,6},{6,10},{10,14},{3,7},{... | collective-permute-start | bytes 442376 | tf_op jit(solution)/shard_map/ppermute | solution.py:24
  7.2 10.9 %collective-permute-start.1 = (bf16[144,512]{1,0:T(8,128)(2,1)S(1)}, bf16[144,512]{1,0:T(8,128)(2,1)}, u32[]{:S(2)}, u32[]{:S(2)}) collective-permute-start(bf16[144,512]{1,0:T(8,128)(2,1)S(1)} %fusion.29), channel_id=1, source_target_pairs={{0,8},{4,12},{1,9},{5,13},{2,10},{6,14},{3,11},{7,15},{16,24},{20,... | collective-permute-start | bytes 442376 | tf_op jit(solution)/shard_map/ppermute | solution.py:24
  12.4 5.7 %collective-permute-start.2 = (bf16[144,512]{1,0:T(8,128)(2,1)S(1)}, bf16[144,512]{1,0:T(8,128)(2,1)}, u32[]{:S(2)}, u32[]{:S(2)}) collective-permute-start(bf16[144,512]{1,0:T(8,128)(2,1)S(1)} %fusion.29), channel_id=1, source_target_pairs={{0,12},{1,13},{2,14},{3,15},{16,28},{17,29},{18,30},{19,31}} | collective-permute-start | bytes 442376 | tf_op jit(solution)/shard_map/ppermute | solution.py:24
  18.1 0.6 copy-start.11
  24.5 5.9 %collective-permute-start.3 = (bf16[32,2048]{1,0:T(8,128)(2,1)}, bf16[32,2048]{1,0:T(8,128)(2,1)S(1)}, u32[]{:S(2)}, u32[]{:S(2)}) collective-permute-start(bf16[32,2048]{1,0:T(8,128)(2,1)} %get-tuple-element.28), channel_id=1, source_target_pairs={{0,3},{1,2},{2,1},{3,0},{4,7},{5,6},{6,5},{7,4},{8,11},{9,10},{10,... | collective-permute-start | bytes 393224 | tf_op jit(solution)/shard_map/ppermute | solution.py:29
  24.9 8.4 %collective-permute-start.4 = (bf16[32,2048]{1,0:T(8,128)(2,1)}, bf16[32,2048]{1,0:T(8,128)(2,1)S(1)}, u32[]{:S(2)}, u32[]{:S(2)}) collective-permute-start(bf16[32,2048]{1,0:T(8,128)(2,1)} %get-tuple-element.29), channel_id=1, source_target_pairs={{0,2},{1,3},{2,0},{3,1},{4,6},{5,7},{6,4},{7,5},{8,10},{9,11},{10,... | collective-permute-start | bytes 393224 | tf_op jit(solution)/shard_map/ppermute | solution.py:29
  26.1 7.3 %collective-permute-start.5 = (bf16[32,2048]{1,0:T(8,128)(2,1)}, bf16[32,2048]{1,0:T(8,128)(2,1)S(1)}, u32[]{:S(2)}, u32[]{:S(2)}) collective-permute-start(bf16[32,2048]{1,0:T(8,128)(2,1)} %get-tuple-element.30), channel_id=1, source_target_pairs={{0,1},{1,0},{2,3},{3,2},{4,5},{5,4},{6,7},{7,6},{8,9},{9,8},{10,11... | collective-permute-start | bytes 393224 | tf_op jit(solution)/shard_map/ppermute | solution.py:29
  30.5 2.9 %copy-start.3 = (bf16[32,2048]{1,0:T(8,128)(2,1)}, bf16[32,2048]{1,0:T(8,128)(2,1)S(1)}, u32[]{:S(2)}) copy-start(bf16[32,2048]{1,0:T(8,128)(2,1)S(1)} %collective-permute-done.3.refs_1_) | copy-start | bytes 393220
  33.4 0.6 copy-start.4
  33.4 0.7 copy-start.5
  36.1 30.8 %copy-start.1 = (bf16[32,2048]{1,0:T(8,128)(2,1)S(1)}, bf16[32,2048]{1,0:T(8,128)(2,1)}, u32[]{:S(2)}) copy-start(bf16[32,2048]{1,0:T(8,128)(2,1)} %get-tuple-element.32) | copy-start | bytes 393220
  36.1 33.7 %copy-start.10 = (bf16[1,2048,768]{2,1,0:T(8,128)(2,1)S(1)}, bf16[1,2048,768]{2,1,0:T(8,128)(2,1)}, u32[]{:S(2)}) copy-start(bf16[1,2048,768]{2,1,0:T(8,128)(2,1)} %param.26) | copy-start | bytes 9437188
  36.1 9.8 %collective-permute-start.12 = (bf16[32,2048]{1,0:T(8,128)(2,1)}, bf16[32,2048]{1,0:T(8,128)(2,1)S(1)}, u32[]{:S(2)}, u32[]{:S(2)}) collective-permute-start(bf16[32,2048]{1,0:T(8,128)(2,1)} %get-tuple-element.32), channel_id=1, source_target_pairs={{0,12},{4,0},{8,4},{12,8},{1,13},{5,1},{9,5},{13,9},{2,14},{6,2},{... | collective-permute-start | bytes 393224 | tf_op jit(solution)/shard_map/ppermute | solution.py:24
  41.6 11.9 %collective-permute-start.13 = (bf16[32,2048]{1,0:T(8,128)(2,1)}, bf16[32,2048]{1,0:T(8,128)(2,1)S(1)}, u32[]{:S(2)}, u32[]{:S(2)}) collective-permute-start(bf16[32,2048]{1,0:T(8,128)(2,1)} %get-tuple-element.32), channel_id=1, source_target_pairs={{0,8},{4,12},{8,0},{12,4},{1,9},{5,13},{9,1},{13,5},{2,10},{6,14},... | collective-permute-start | bytes 393224 | tf_op jit(solution)/shard_map/ppermute | solution.py:24
  41.6 12.7 %collective-permute-start.6 = (bf16[32,2048]{1,0:T(8,128)(2,1)}, bf16[32,2048]{1,0:T(8,128)(2,1)S(1)}, u32[]{:S(2)}, u32[]{:S(2)}) collective-permute-start(bf16[32,2048]{1,0:T(8,128)(2,1)} %get-tuple-element.32), channel_id=1, source_target_pairs={{0,4},{4,8},{8,12},{12,0},{1,5},{5,9},{9,13},{13,1},{2,6},{6,10},{... | collective-permute-start | bytes 393224 | tf_op jit(solution)/shard_map/ppermute | solution.py:24
  53.5 9.2 %collective-permute-start.14 = (bf16[64,2048]{1,0:T(8,128)(2,1)S(1)}, bf16[64,2048]{1,0:T(8,128)(2,1)S(1)}, u32[]{:S(2)}, u32[]{:S(2)}) collective-permute-start(bf16[64,2048]{1,0:T(8,128)(2,1)S(1)} %pad_maximum_fusion.3), channel_id=1, source_target_pairs={{0,2},{1,3},{2,0},{3,1},{4,6},{5,7},{6,4},{7,5},{8,10},{9,11},{10,... | collective-permute-start | bytes 786440 | tf_op jit(solution)/shard_map/ppermute | solution.py:29
  55.3 11.6 %collective-permute-start.7 = (bf16[64,2048]{1,0:T(8,128)(2,1)S(1)}, bf16[64,2048]{1,0:T(8,128)(2,1)S(1)}, u32[]{:S(2)}, u32[]{:S(2)}) collective-permute-start(bf16[64,2048]{1,0:T(8,128)(2,1)S(1)} %pad_maximum_fusion.2), channel_id=1, source_target_pairs={{0,2},{1,3},{2,0},{3,1},{4,6},{5,7},{6,4},{7,5},{8,10},{9,11},{10,... | collective-permute-start | bytes 786440 | tf_op jit(solution)/shard_map/ppermute | solution.py:29
  62.8 5.0 %collective-permute-start.15 = (bf16[128,2048]{1,0:T(8,128)(2,1)S(1)}, bf16[128,2048]{1,0:T(8,128)(2,1)S(1)}, u32[]{:S(2)}, u32[]{:S(2)}) collective-permute-start(bf16[128,2048]{1,0:T(8,128)(2,1)S(1)} %pad_maximum_fusion.1), channel_id=1, source_target_pairs={{0,1},{1,0},{2,3},{3,2},{4,5},{5,4},{6,7},{7,6},{8,9},{9,8},{10,11... | collective-permute-start | bytes 1572872 | tf_op jit(solution)/shard_map/ppermute | solution.py:29
  67.8 11.9 %collective-permute-start.8 = (bf16[128,2048]{1,0:T(8,128)(2,1)}, bf16[128,2048]{1,0:T(8,128)(2,1)}, u32[]{:S(2)}, u32[]{:S(2)}) collective-permute-start(bf16[128,2048]{1,0:T(8,128)(2,1)} %pad_maximum_fusion), channel_id=1, source_target_pairs={{0,1},{1,0},{2,3},{3,2},{4,5},{5,4},{6,7},{7,6},{8,9},{9,8},{10,11... | collective-permute-start | bytes 1572872 | tf_op jit(solution)/shard_map/ppermute | solution.py:29
  67.8 1.0 copy-start.6
  68.8 1.0 copy-start.7
  79.1 13.3 %collective-permute-start.16 = (bf16[128,2048]{1,0:T(8,128)(2,1)}, bf16[128,2048]{1,0:T(8,128)(2,1)}, u32[]{:S(2)}, u32[]{:S(2)}) collective-permute-start(bf16[128,2048]{1,0:T(8,128)(2,1)} %slice.71), channel_id=1, source_target_pairs={{0,1},{1,0},{2,3},{3,2},{4,5},{5,4},{6,7},{7,6},{8,9},{9,8},{10,11... | collective-permute-start | bytes 1572872 | tf_op jit(solution)/shard_map/ppermute | solution.py:29
  91.1 3.5 %copy-start.2 = (bf16[256,2048]{1,0:T(8,128)(2,1)S(1)}, bf16[256,2048]{1,0:T(8,128)(2,1)}, u32[]{:S(2)}) copy-start(bf16[256,2048]{1,0:T(8,128)(2,1)} %fusion.12) | copy-start | bytes 3145732
  92.3 16.1 %copy-start.8 = (f32[32,2]{0,1:T(2,128)S(1)}, f32[32,2]{0,1:T(2,128)}, u32[]{:S(2)}) copy-start(f32[32,2]{0,1:T(2,128)} %param.24) | copy-start | bytes 772
  92.3 16.1 %copy-start.9 = (s32[32,2]{0,1:T(2,128)S(1)}, s32[32,2]{0,1:T(2,128)}, u32[]{:S(2)}) copy-start(s32[32,2]{0,1:T(2,128)} %param.23) | copy-start | bytes 772
  92.3 2.3 %collective-permute-start.9 = (bf16[128,2048]{1,0:T(8,128)(2,1)S(1)}, bf16[128,2048]{1,0:T(8,128)(2,1)S(1)}, u32[]{:S(2)}, u32[]{:S(2)}) collective-permute-start(bf16[128,2048]{1,0:T(8,128)(2,1)S(1)} %slice.65), channel_id=1, source_target_pairs={{0,1},{1,0},{2,3},{3,2},{4,5},{5,4},{6,7},{7,6},{8,9},{9,8},{10,11... | collective-permute-start | bytes 1572872 | tf_op jit(solution)/shard_map/ppermute | solution.py:29
  93.8 9.2 %collective-permute-start.17 = (bf16[64,2048]{1,0:T(8,128)(2,1)S(1)}, bf16[64,2048]{1,0:T(8,128)(2,1)S(1)}, u32[]{:S(2)}, u32[]{:S(2)}) collective-permute-start(bf16[64,2048]{1,0:T(8,128)(2,1)S(1)} %slice.73), channel_id=1, source_target_pairs={{0,2},{1,3},{2,0},{3,1},{4,6},{5,7},{6,4},{7,5},{8,10},{9,11},{10,... | collective-permute-start | bytes 786440 | tf_op jit(solution)/shard_map/ppermute | solution.py:29
  94.8 13.3 %collective-permute-start.10 = (bf16[64,2048]{1,0:T(8,128)(2,1)S(1)}, bf16[64,2048]{1,0:T(8,128)(2,1)S(1)}, u32[]{:S(2)}, u32[]{:S(2)}) collective-permute-start(bf16[64,2048]{1,0:T(8,128)(2,1)S(1)} %slice.67), channel_id=1, source_target_pairs={{0,2},{1,3},{2,0},{3,1},{4,6},{5,7},{6,4},{7,5},{8,10},{9,11},{10,... | collective-permute-start | bytes 786440 | tf_op jit(solution)/shard_map/ppermute | solution.py:29
  103.8 9.5 %collective-permute-start.19 = (bf16[32,2048]{1,0:T(8,128)(2,1)}, bf16[32,2048]{1,0:T(8,128)(2,1)}, u32[]{:S(2)}, u32[]{:S(2)}) collective-permute-start(bf16[32,2048]{1,0:T(8,128)(2,1)} %get-tuple-element.38), channel_id=1, source_target_pairs={{0,8},{4,12},{8,0},{12,4},{1,9},{5,13},{9,1},{13,5},{2,10},{6,14},... | collective-permute-start | bytes 393224 | tf_op jit(solution)/shard_map/ppermute | solution.py:24
  103.8 9.5 %collective-permute-start.18 = (bf16[32,2048]{1,0:T(8,128)(2,1)}, bf16[32,2048]{1,0:T(8,128)(2,1)}, u32[]{:S(2)}, u32[]{:S(2)}) collective-permute-start(bf16[32,2048]{1,0:T(8,128)(2,1)} %get-tuple-element.37), channel_id=1, source_target_pairs={{0,4},{4,8},{8,12},{12,0},{1,5},{5,9},{9,13},{13,1},{2,6},{6,10},{... | collective-permute-start | bytes 393224 | tf_op jit(solution)/shard_map/ppermute | solution.py:24
  108.2 7.4 %collective-permute-start.11 = (bf16[32,2048]{1,0:T(8,128)(2,1)S(1)}, bf16[32,2048]{1,0:T(8,128)(2,1)}, u32[]{:S(2)}, u32[]{:S(2)}) collective-permute-start(bf16[32,2048]{1,0:T(8,128)(2,1)S(1)} %slice.69), channel_id=1, source_target_pairs={{0,12},{4,0},{8,4},{12,8},{1,13},{5,1},{9,5},{13,9},{2,14},{6,2},{... | collective-permute-start | bytes 393224 | tf_op jit(solution)/shard_map/ppermute | solution.py:24

commit v2 on v1

--- a/solution.py
+++ b/solution.py
@@ -6,6 +6,7 @@
 from jax.experimental import pallas as pl
 from jax.experimental.pallas import tpu as pltpu
 from jax.sharding import PartitionSpec as P
+
 
 D = 2048
 HEADS = 16
@@ -14,6 +15,7 @@
 TOPK = 2
 DOC_ROWS = 16
 DIRECT_KEYS = 1024
+SMALL = 20 * 2**20
 VMEM = pl.BlockSpec(memory_space=pltpu.VMEM)
 SMEM = pl.BlockSpec(memory_space=pltpu.SMEM)
 
@@ -124,6 +126,28 @@
     value = middle.astype(jnp.float32)
     scale = lax.rsqrt(jnp.mean(value * value, axis=1, keepdims=True) + 1e-06)
     normed_ref[...] = (value * scale * gain_ref[...]).astype(jnp.bfloat16)
+
+
+def expert_kernel(near_ref, far_ref, gate_ref, up_ref, down_ref, kept_ref, sent_ref, held_ref, hidden_ref):
+    half = near_ref.shape[0]
+    held_ref[:half, :] = near_ref[...]
+    held_ref[half:, :] = far_ref[...]
+    tile = 256
+    for at in range(0, gate_ref.shape[2], tile):
+        gate_value = jnp.dot(
+            held_ref[...], gate_ref[0, :, at : at + tile], preferred_element_type=jnp.float32
+        )
+        up_value = jnp.dot(
+            held_ref[...], up_ref[0, :, at : at + tile], preferred_element_type=jnp.float32
+        )
+        hidden = gate_value / (1.0 + jnp.exp(-gate_value)) * up_value
+        hidden_ref[:, at : at + tile] = hidden.astype(jnp.bfloat16)
+    for at in range(0, down_ref.shape[2], tile):
+        result = jnp.dot(
+            hidden_ref[...], down_ref[0, :, at : at + tile], preferred_element_type=jnp.float32
+        ).astype(jnp.bfloat16)
+        kept_ref[:, at : at + tile] = result[:half]
+        sent_ref[:, at : at + tile] = result[half:]
 
 
 def cost(flops, nbytes):
@@ -152,6 +176,7 @@
         in_specs=[VMEM, VMEM, VMEM, SMEM, VMEM, VMEM],
         out_specs=(VMEM, VMEM),
         cost_estimate=cost(6 * 10**9, 10**6),
+        compiler_params=pltpu.CompilerParams(vmem_limit_bytes=SMALL),
         name="attend_here",
     )(queries, keys, values, head_bias, col, row)
     place = jnp.stack([lax.axis_index("sp"), lax.axis_index("tp")]).astype(jnp.int32)
@@ -164,6 +189,7 @@
         out_specs=[VMEM] * tp_count,
         scratch_shapes=[pltpu.VMEM((rows, width), jnp.float32)],
         cost_estimate=cost(10 * 10**9, 4 * 10**6),
+        compiler_params=pltpu.CompilerParams(vmem_limit_bytes=SMALL),
         name="attend_away",
     )(place, queries, head_bias, col, mix, carry, w_out, *sent)
     arrived = [pieces[0]] + [swapped(pieces[mask], mask) for mask in order[:0:-1]]
@@ -173,6 +199,7 @@
         in_specs=[VMEM] * (2 + tp_count),
         out_specs=[VMEM] * 2,
         cost_estimate=cost(10**8, 10**6),
+        compiler_params=pltpu.CompilerParams(vmem_limit_bytes=SMALL),
         name="middle_norm",
     )(resid, norm_gain.reshape(1, D), *arrived)
 
@@ -185,21 +212,35 @@
     steps = [0] + [s for pair in zip(range(1, sp_count), range(sp_count - 1, 0, -1)) for s in pair]
     steps = list(dict.fromkeys(steps))
     half = (len(steps) + 1) // 2
-    moved = {s: normed if s == 0 else shifted(normed, s, True) for s in steps}
+    moved = {0: normed}
+    for s in steps[1:]:
+        moved[s] = shifted(normed, s, True)
     pieces = {}
     for chunk in (steps[:half], steps[half:]):
         held = jnp.concatenate([moved[s] for s in chunk], axis=0)
-        for mask in masks[::-1]:
-            held = jnp.concatenate([held, swapped(held, mask)], axis=0)
-        gate_value = jnp.dot(held, w_gate[0], preferred_element_type=jnp.float32)
-        up_value = jnp.dot(held, w_up[0], preferred_element_type=jnp.float32)
-        hidden = (jax.nn.silu(gate_value) * up_value).astype(jnp.bfloat16)
-        result = jnp.dot(hidden, w_down[0], preferred_element_type=jnp.float32).astype(jnp.bfloat16)
+        for mask in masks[:0:-1]:
+            other = swapped(held, mask)
+            held = jnp.concatenate([held, other], axis=0)
+        far = swapped(held, 1)
+        count = held.shape[0]
+        result, leaving = pl.pallas_call(
+            expert_kernel,
+            out_shape=[jax.ShapeDtypeStruct((count, D), jnp.bfloat16)] * 2,
+            in_specs=[VMEM] * 5,
+            out_specs=[VMEM] * 2,
+            scratch_shapes=[
+                pltpu.VMEM((2 * count, D), jnp.bfloat16),
+                pltpu.VMEM((2 * count, w_gate.shape[2]), jnp.bfloat16),
+            ],
+            compiler_params=pltpu.CompilerParams(vmem_limit_bytes=32 * 2**20),
+            cost_estimate=cost(12 * count * D * w_gate.shape[2], 12 * 10**6),
+        )(held, far, w_gate, w_up, w_down)
         for mask in masks:
-            kept = result.shape[0] // 2
-            result = (
-                result[:kept].astype(jnp.float32) + swapped(result[kept:], mask).astype(jnp.float32)
-            ).astype(jnp.bfloat16)
+            if mask > 1:
+                kept = result.shape[0] // 2
+                result, leaving = result[:kept], result[kept:]
+            other = swapped(leaving, mask)
+            result = (result.astype(jnp.float32) + other.astype(jnp.float32)).astype(jnp.bfloat16)
         for at, s in enumerate(chunk):
             pieces[s] = result[at * rows : (at + 1) * rows]
     own = lax.axis_index("sp")
@@ -272,7 +313,7 @@
         )
         return (mix_sum + partial_mix, carry_sum + block_keep, key_block, value_block, doc_block)
 
-    mix_total, carried, key_last, value_last, doc_last = lax.fori_loop(
+    mix_total, carried, _, _, _ = lax.fori_loop(
         1, sp_count, visit, (mix_total, carried, keys, values, doc_column)
     )
     mixed = mix_total.reshape(tok_count, kv_local * group_size * DH).astype(jnp.bfloat16)

time: 118 us -> 89.8 us (0.76)
  matrix products: 17 us -> 0 us
  local copies, waits for them, and re-layouts: 10.7 us -> 3.78 us
  other arithmetic: 8.24 us -> 2.97 us
  waiting for transfers between devices: 45.1 us -> 46.4 us
    dot_general x4 -> x0, matrix products: 17 us -> none  [the longest x2 11.1 us: experts_dense(): jnp.dot(hidden, w_down[0], preferred_element_type=jnp.float32)]
    pallas_call x0 -> x2, Pallas kernels: none -> 5.23 us  [experts_dense(): pl.pallas_call(expert_kernel, out_shape=[jax.ShapeDtypeStruct((count, D),...]
    slice x4 -> x2, local copies, waits for them, and re-layouts: 3.13 us -> 0.04 us  [experts_dense(): result, leaving = (result[:kept], result[kept:])]
    pallas_call x1, Pallas kernels: 5.83 us -> 3.79 us  [middle_direct(): pl.pallas_call(functools.partial(away_kernel, sp_count - 1, order), out_s...]
    concatenate x2, local copies, waits for them, and re-layouts: 1.92 us -> 0.04 us  [experts_dense(): held = jnp.concatenate([held, other], axis=0)]
    pallas_call x1, Pallas kernels: 2.03 us -> 0.21 us  [middle_direct(): pl.pallas_call(norm_kernel, out_shape=[jax.ShapeDtypeStruct((share, D), j...]
    ppermute x11, waiting for transfers between devices: 27.7 us -> 29.2 us  [swapped(): return lax.ppermute(value, 'tp', [(i, i ^ mask) for i in range(count)])]
    convert_element_type x4, other arithmetic: 1.58 us -> 0.38 us  [experts_dense(): (result.astype(jnp.float32) + other.astype(jnp.float32)).astype(jnp.bfloa...]
  transfers between devices with their start and end apart: 20 -> 20, of which waited for: 10 -> 11; matrix products, arithmetic and copies ran while one was open for 24% -> 1% of each run, Pallas kernels for 2% -> 7%
where the time goes in v2:
time: 89.8 us; the launch traced here: 89.4 us
  waiting for transfers between devices  46.4 us (52%)
  starting transfers between devices  25.5 us (28%)
  Pallas kernels  10.4 us (12%)
  local copies, waits for them, and re-layouts  3.78 us (4%)
  other arithmetic  2.97 us (3%)
    ppermute x11, waiting for transfers between devices, swapped(): return lax.ppermute(value, 'tp', [(i, i ^ mask) for i in range(count)])  29.2 us
    ppermute x9, starting transfers between devices, shifted(): return lax.ppermute(value, 'sp', pairs)  18.8 us
    ppermute x9, waiting for transfers between devices, shifted(): return lax.ppermute(value, 'sp', pairs)  17.3 us
    ppermute x11, starting transfers between devices, swapped(): return lax.ppermute(value, 'tp', [(i, i ^ mask) for i in range(count)])  6.74 us
    pallas_call x2, Pallas kernels, experts_dense(): pl.pallas_call(expert_kernel, out_shape=[jax.ShapeDtypeStruct((count, D),...  5.23 us
    pallas_call x1, Pallas kernels, middle_direct(): pl.pallas_call(functools.partial(away_kernel, sp_count - 1, order), out_s...  3.79 us
    unnamed x32, local copies, waits for them, and re-layouts  3.56 us
  transfers between devices with their start and end apart: 20, of which 11 were waited for; matrix products, arithmetic and copies ran while one was open for 1% of the time, Pallas kernels for 7%

profile of v2, /device:TPU:0, one launch (start us, length us, event | category | flops | bytes accessed | tf_op | source)
XLA Modules:
  0.0 89.4 jit_solution(9687035046909811656)
XLA Ops:
  0.0 0.7 convert_bitcast_fusion
  0.7 0.9 fusion.1
  1.6 5.0 %collective-permute-start = (bf16[144,512]{1,0:T(8,128)(2,1)S(1)}, bf16[144,512]{1,0:T(8,128)(2,1)S(1)}, u32[]{:S(2)}, u32[]{:S(2)}) collective-permute-start(bf16[144,512]{1,0:T(8,128)(2,1)S(1)} %fusion.1), channel_id=1, source_target_pairs={{0,4},{4,8},{8,12},{1,5},{5,9},{9,13},{2,6},{6,10},{10,14},{3,7},{... | collective-permute-start | bytes 442376 | tf_op jit(solution)/shard_map/ppermute | solution.py:26
  6.6 4.5 %collective-permute-start.1 = (bf16[144,512]{1,0:T(8,128)(2,1)S(1)}, bf16[144,512]{1,0:T(8,128)(2,1)S(1)}, u32[]{:S(2)}, u32[]{:S(2)}) collective-permute-start(bf16[144,512]{1,0:T(8,128)(2,1)S(1)} %fusion.1), channel_id=1, source_target_pairs={{0,8},{4,12},{1,9},{5,13},{2,10},{6,14},{3,11},{7,15},{16,24},{20,... | collective-permute-start | bytes 442376 | tf_op jit(solution)/shard_map/ppermute | solution.py:26
  11.1 1.3 %collective-permute-start.2 = (bf16[144,512]{1,0:T(8,128)(2,1)S(1)}, bf16[144,512]{1,0:T(8,128)(2,1)S(1)}, u32[]{:S(2)}, u32[]{:S(2)}) collective-permute-start(bf16[144,512]{1,0:T(8,128)(2,1)S(1)} %fusion.1), channel_id=1, source_target_pairs={{0,12},{1,13},{2,14},{3,15},{16,28},{17,29},{18,30},{19,31}} | collective-permute-start | bytes 442376 | tf_op jit(solution)/shard_map/ppermute | solution.py:26
  12.4 0.1 copy.15.col_ref
  12.5 0.8 copy-done.4
  13.4 0.8 copy-done.5
  14.2 0.9 %copy-done.8 = bf16[128,512]{1,0:T(8,128)(2,1)S(1)} copy-done((bf16[128,512]{1,0:T(8,128)(2,1)S(1)}, bf16[128,512]{1,0:T(8,128)(2,1)}, u32[]{:S(2)}) %copy-start.8) | copy-done | bytes 131096
  15.1 0.7 copy-done.10
  15.8 1.2 %attend_here.1 = (f32[128,512]{1,0:T(8,128)S(1)}, f32[512,128]{1,0:T(8,128)S(1)}) custom-call(bf16[128,512]{1,0:T(8,128)(2,1)S(1)} %copy-done.8, bf16[128,256]{1,0:T(8,128)(2,1)S(1)} %copy-done.4, bf16[128,256]{1,0:T(8,128)(2,1)S(1)} %copy-done.5, f32[4]{0:T(128)S(1)} %copy-done.10, f32[128,1]{1,0:T(8,128)S(1)} %copy.15.col_ref, ...), custom_call_target="tpu_custom_call" | custom-call | flops 6000000000 | bytes 1000000 | tf_op jit(solution)/shard_map/attend_here/pallas_call | solution.py:170
  17.0 0.1 pad_add_fusion.place_ref
  17.1 0.2 copy-done.7
  17.4 3.8 %attend_away.1 = (bf16[32,2048]{1,0:T(8,128)(2,1)S(1)}, bf16[32,2048]{1,0:T(8,128)(2,1)S(1)}, bf16[32,2048]{1,0:T(8,128)(2,1)S(1)}, bf16[32,2048]{1,0:T(8,128)(2,1)S(1)}) custom-call(s32[2]{0:T(128)S(1)} %pad_add_fusion.place_ref, bf16[128,512]{1,0:T(8,128)(2,1)S(1)} %copy-done.9, f32[4]{0:T(128)S(1)} %copy-done.11, f32[128,1]{1,0:T(8,128)S(1)} %copy.15.col_ref, ...), custom_call_target="tpu_custom_call" | custom-call | flops 10000000000 | bytes 4000000 | tf_op jit(solution)/shard_map/attend_away/pallas_call | solution.py:185
  21.2 0.5 collective-permute-start.3
  21.6 1.2 %collective-permute-start.4 = (bf16[32,2048]{1,0:T(8,128)(2,1)S(1)}, bf16[32,2048]{1,0:T(8,128)(2,1)S(1)}, u32[]{:S(2)}, u32[]{:S(2)}) collective-permute-start(bf16[32,2048]{1,0:T(8,128)(2,1)S(1)} %get-tuple-element.33), channel_id=1, source_target_pairs={{0,2},{1,3},{2,0},{3,1},{4,6},{5,7},{6,4},{7,5},{8,10},{9,11},{10,... | collective-permute-start | bytes 393224 | tf_op jit(solution)/shard_map/ppermute | solution.py:31
  22.8 0.3 collective-permute-start.5
  23.1 3.9 %collective-permute-done.3.refs_1_ = bf16[32,2048]{1,0:T(8,128)(2,1)S(1)} collective-permute-done((bf16[32,2048]{1,0:T(8,128)(2,1)S(1)}, bf16[32,2048]{1,0:T(8,128)(2,1)S(1)}, u32[]{:S(2)}, u32[]{:S(2)}) %collective-permute-start.3) | collective-permute-done | bytes 131104 | tf_op jit(solution)/shard_map/ppermute | solution.py:31
  27.0 2.9 %collective-permute-done.4.refs_2_ = bf16[32,2048]{1,0:T(8,128)(2,1)S(1)} collective-permute-done((bf16[32,2048]{1,0:T(8,128)(2,1)S(1)}, bf16[32,2048]{1,0:T(8,128)(2,1)S(1)}, u32[]{:S(2)}, u32[]{:S(2)}) %collective-permute-start.4) | collective-permute-done | bytes 131104 | tf_op jit(solution)/shard_map/ppermute | solution.py:31
  29.9 0.2 middle_norm.1
  30.1 6.3 %collective-permute-start.12 = (bf16[32,2048]{1,0:T(8,128)(2,1)S(1)}, bf16[32,2048]{1,0:T(8,128)(2,1)S(1)}, u32[]{:S(2)}, u32[]{:S(2)}) collective-permute-start(bf16[32,2048]{1,0:T(8,128)(2,1)S(1)} %get-tuple-element.36), channel_id=1, source_target_pairs={{0,12},{4,0},{8,4},{12,8},{1,13},{5,1},{9,5},{13,9},{2,14},{6,2},{... | collective-permute-start | bytes 393224 | tf_op jit(solution)/shard_map/ppermute | solution.py:26
  36.4 0.6 collective-permute-start.6
  37.0 3.3 %collective-permute-done.12 = bf16[32,2048]{1,0:T(8,128)(2,1)S(1)} collective-permute-done((bf16[32,2048]{1,0:T(8,128)(2,1)S(1)}, bf16[32,2048]{1,0:T(8,128)(2,1)S(1)}, u32[]{:S(2)}, u32[]{:S(2)}) %collective-permute-start.12) | collective-permute-done | bytes 131104 | tf_op jit(solution)/shard_map/ppermute | solution.py:26
  40.3 7.7 %collective-permute-done.13 = bf16[32,2048]{1,0:T(8,128)(2,1)S(1)} collective-permute-done((bf16[32,2048]{1,0:T(8,128)(2,1)S(1)}, bf16[32,2048]{1,0:T(8,128)(2,1)S(1)}, u32[]{:S(2)}, u32[]{:S(2)}) %collective-permute-start.13) | collective-permute-done | bytes 131104 | tf_op jit(solution)/shard_map/ppermute | solution.py:26
  48.0 0.8 collective-permute-start.14
  48.9 1.3 %collective-permute-start.7 = (bf16[64,2048]{1,0:T(8,128)(2,1)S(1)}, bf16[64,2048]{1,0:T(8,128)(2,1)S(1)}, u32[]{:S(2)}, u32[]{:S(2)}) collective-permute-start(bf16[64,2048]{1,0:T(8,128)(2,1)S(1)} %pad_maximum_fusion), channel_id=1, source_target_pairs={{0,2},{1,3},{2,0},{3,1},{4,6},{5,7},{6,4},{7,5},{8,10},{9,11},{10,... | collective-permute-start | bytes 786440 | tf_op jit(solution)/shard_map/ppermute | solution.py:31
  50.2 7.0 %collective-permute-done.14 = bf16[64,2048]{1,0:T(8,128)(2,1)S(1)} collective-permute-done((bf16[64,2048]{1,0:T(8,128)(2,1)S(1)}, bf16[64,2048]{1,0:T(8,128)(2,1)S(1)}, u32[]{:S(2)}, u32[]{:S(2)}) %collective-permute-start.14) | collective-permute-done | bytes 262176 | tf_op jit(solution)/shard_map/ppermute | solution.py:31
  57.3 0.1 collective-permute-start.15
  57.4 4.0 %collective-permute-done.7 = bf16[64,2048]{1,0:T(8,128)(2,1)S(1)} collective-permute-done((bf16[64,2048]{1,0:T(8,128)(2,1)S(1)}, bf16[64,2048]{1,0:T(8,128)(2,1)S(1)}, u32[]{:S(2)}, u32[]{:S(2)}) %collective-permute-start.7) | collective-permute-done | bytes 262176 | tf_op jit(solution)/shard_map/ppermute | solution.py:31
  61.4 0.1 collective-permute-start.8
  61.5 2.6 %shard_map.128 = (bf16[128,2048]{1,0:T(8,128)(2,1)S(1)}, bf16[128,2048]{1,0:T(8,128)(2,1)S(1)}) custom-call(bf16[128,2048]{1,0:T(8,128)(2,1)S(1)} %constant_dynamic-update-slice_fusion.3.near_ref, bf16[128,2048]{1,0:T(8,128)(2,1)S(1)} %collective-permute-done.15.far_ref, bf16[1,2048,768]{2,1,0:T(8,128)(2,1)S(1)} %copy-done, ...), custom_call_target="tpu_custom_call" | custom-call | flops 2415919104 | bytes 12000000 | tf_op jit(solution)/shard_map/pallas_call | solution.py:226
  64.2 0.5 collective-permute-start.16
  64.7 2.6 %shard_map.127 = (bf16[128,2048]{1,0:T(8,128)(2,1)S(1)}, bf16[128,2048]{1,0:T(8,128)(2,1)S(1)}) custom-call(bf16[128,2048]{1,0:T(8,128)(2,1)S(1)} %constant_dynamic-update-slice_fusion.near_ref, bf16[128,2048]{1,0:T(8,128)(2,1)S(1)} %collective-permute-done.8.far_ref, bf16[1,2048,768]{2,1,0:T(8,128)(2,1)S(1)} %copy-done, ...), custom_call_target="tpu_custom_call" | custom-call | flops 2415919104 | bytes 12000000 | tf_op jit(solution)/shard_map/pallas_call | solution.py:226
  67.3 0.1 collective-permute-start.9
  67.4 0.1 add_convert_fusion
  67.6 0.9 %collective-permute-start.17 = (bf16[64,2048]{1,0:T(8,128)(2,1)S(1)}, bf16[64,2048]{1,0:T(8,128)(2,1)S(1)}, u32[]{:S(2)}, u32[]{:S(2)}) collective-permute-start(bf16[64,2048]{1,0:T(8,128)(2,1)S(1)} %slice.53), channel_id=1, source_target_pairs={{0,2},{1,3},{2,0},{3,1},{4,6},{5,7},{6,4},{7,5},{8,10},{9,11},{10,... | collective-permute-start | bytes 786440 | tf_op jit(solution)/shard_map/ppermute | solution.py:31
  68.5 0.8 collective-permute-done.9
  69.3 0.1 add_convert_fusion.1
  69.5 0.9 %collective-permute-start.10 = (bf16[64,2048]{1,0:T(8,128)(2,1)S(1)}, bf16[64,2048]{1,0:T(8,128)(2,1)S(1)}, u32[]{:S(2)}, u32[]{:S(2)}) collective-permute-start(bf16[64,2048]{1,0:T(8,128)(2,1)S(1)} %slice.49), channel_id=1, source_target_pairs={{0,2},{1,3},{2,0},{3,1},{4,6},{5,7},{6,4},{7,5},{8,10},{9,11},{10,... | collective-permute-start | bytes 786440 | tf_op jit(solution)/shard_map/ppermute | solution.py:31
  70.4 6.4 %collective-permute-done.17 = bf16[64,2048]{1,0:T(8,128)(2,1)S(1)} collective-permute-done((bf16[64,2048]{1,0:T(8,128)(2,1)S(1)}, bf16[64,2048]{1,0:T(8,128)(2,1)S(1)}, u32[]{:S(2)}, u32[]{:S(2)}) %collective-permute-start.17) | collective-permute-done | bytes 262176 | tf_op jit(solution)/shard_map/ppermute | solution.py:31
  76.9 0.1 collective-permute-start.19
  77.0 0.8 collective-permute-start.18
  77.8 4.2 %collective-permute-done.10 = bf16[64,2048]{1,0:T(8,128)(2,1)S(1)} collective-permute-done((bf16[64,2048]{1,0:T(8,128)(2,1)S(1)}, bf16[64,2048]{1,0:T(8,128)(2,1)S(1)}, u32[]{:S(2)}, u32[]{:S(2)}) %collective-permute-start.10) | collective-permute-done | bytes 262176 | tf_op jit(solution)/shard_map/ppermute | solution.py:31
  82.0 0.1 add_convert_fusion.3
  82.0 0.3 collective-permute-start.11
  82.3 3.8 %collective-permute-done.19 = bf16[32,2048]{1,0:T(8,128)(2,1)S(1)} collective-permute-done((bf16[32,2048]{1,0:T(8,128)(2,1)S(1)}, bf16[32,2048]{1,0:T(8,128)(2,1)S(1)}, u32[]{:S(2)}, u32[]{:S(2)}) %collective-permute-start.19) | collective-permute-done | bytes 131104 | tf_op jit(solution)/shard_map/ppermute | solution.py:26
  86.2 2.4 %collective-permute-done.11 = bf16[32,2048]{1,0:T(8,128)(2,1)S(1)} collective-permute-done((bf16[32,2048]{1,0:T(8,128)(2,1)S(1)}, bf16[32,2048]{1,0:T(8,128)(2,1)S(1)}, u32[]{:S(2)}, u32[]{:S(2)}) %collective-permute-start.11) | collective-permute-done | bytes 131104 | tf_op jit(solution)/shard_map/ppermute | solution.py:26
  88.6 0.8 add_convert_fusion.4
  (47 shorter events, 0.4 us)
Async XLA Ops:
  1.6 15.4 %collective-permute-start = (bf16[144,512]{1,0:T(8,128)(2,1)S(1)}, bf16[144,512]{1,0:T(8,128)(2,1)S(1)}, u32[]{:S(2)}, u32[]{:S(2)}) collective-permute-start(bf16[144,512]{1,0:T(8,128)(2,1)S(1)} %fusion.1), channel_id=1, source_target_pairs={{0,4},{4,8},{8,12},{1,5},{5,9},{9,13},{2,6},{6,10},{10,14},{3,7},{... | collective-permute-start | bytes 442376 | tf_op jit(solution)/shard_map/ppermute | solution.py:26
  6.6 10.5 %collective-permute-start.1 = (bf16[144,512]{1,0:T(8,128)(2,1)S(1)}, bf16[144,512]{1,0:T(8,128)(2,1)S(1)}, u32[]{:S(2)}, u32[]{:S(2)}) collective-permute-start(bf16[144,512]{1,0:T(8,128)(2,1)S(1)} %fusion.1), channel_id=1, source_target_pairs={{0,8},{4,12},{1,9},{5,13},{2,10},{6,14},{3,11},{7,15},{16,24},{20,... | collective-permute-start | bytes 442376 | tf_op jit(solution)/shard_map/ppermute | solution.py:26
  11.1 6.0 %collective-permute-start.2 = (bf16[144,512]{1,0:T(8,128)(2,1)S(1)}, bf16[144,512]{1,0:T(8,128)(2,1)S(1)}, u32[]{:S(2)}, u32[]{:S(2)}) collective-permute-start(bf16[144,512]{1,0:T(8,128)(2,1)S(1)} %fusion.1), channel_id=1, source_target_pairs={{0,12},{1,13},{2,14},{3,15},{16,28},{17,29},{18,30},{19,31}} | collective-permute-start | bytes 442376 | tf_op jit(solution)/shard_map/ppermute | solution.py:26
  12.5 0.8 copy-start.4
  13.4 0.8 copy-start.5
  14.2 0.9 %copy-start.8 = (bf16[128,512]{1,0:T(8,128)(2,1)S(1)}, bf16[128,512]{1,0:T(8,128)(2,1)}, u32[]{:S(2)}) copy-start(bf16[128,512]{1,0:T(8,128)(2,1)} %q_ref.3) | copy-start | bytes 393220
  15.1 0.7 copy-start.10
  15.8 1.6 %copy-start.7 = (bf16[512,2048]{1,0:T(8,128)(2,1)S(1)}, bf16[512,2048]{1,0:T(8,128)(2,1)}, u32[]{:S(2)}) copy-start(bf16[512,2048]{1,0:T(8,128)(2,1)} %w_ref.1) | copy-start | bytes 6291460
  15.8 1.6 %copy-start.9 = (bf16[128,512]{1,0:T(8,128)(2,1)S(1)}, bf16[128,512]{1,0:T(8,128)(2,1)}, u32[]{:S(2)}) copy-start(bf16[128,512]{1,0:T(8,128)(2,1)} %q_ref.3) | copy-start | bytes 393220
  15.8 1.6 %copy-start.11 = (f32[4]{0:T(128)S(1)}, f32[4]{0:T(128)}, u32[]{:S(2)}) copy-start(f32[4]{0:T(128)} %bias_ref.3) | copy-start | bytes 52
  17.4 12.5 %copy-start.3 = (bf16[32,2048]{1,0:T(8,128)(2,1)S(1)}, bf16[32,2048]{1,0:T(8,128)(2,1)}, u32[]{:S(2)}) copy-start(bf16[32,2048]{1,0:T(8,128)(2,1)} %resid_ref.1) | copy-start | bytes 393220
  17.4 12.5 %copy-start.6 = (f32[2048]{0:T(1024)S(1)}, f32[2048]{0:T(1024)}, u32[]{:S(2)}) copy-start(f32[2048]{0:T(1024)} %param.22) | copy-start | bytes 24580
  17.4 44.1 %copy-start.1 = (bf16[1,2048,768]{2,1,0:T(8,128)(2,1)S(1)}, bf16[1,2048,768]{2,1,0:T(8,128)(2,1)}, u32[]{:S(2)}) copy-start(bf16[1,2048,768]{2,1,0:T(8,128)(2,1)} %up_ref.3) | copy-start | bytes 9437188
  17.4 44.1 %copy-start.2 = (bf16[1,768,2048]{2,1,0:T(8,128)(2,1)S(1)}, bf16[1,768,2048]{2,1,0:T(8,128)(2,1)}, u32[]{:S(2)}) copy-start(bf16[1,768,2048]{2,1,0:T(8,128)(2,1)} %down_ref.3) | copy-start | bytes 9437188
  21.2 40.3 %copy-start = (bf16[1,2048,768]{2,1,0:T(8,128)(2,1)S(1)}, bf16[1,2048,768]{2,1,0:T(8,128)(2,1)}, u32[]{:S(2)}) copy-start(bf16[1,2048,768]{2,1,0:T(8,128)(2,1)} %gate_ref.3) | copy-start | bytes 9437188
  21.2 5.8 %collective-permute-start.3 = (bf16[32,2048]{1,0:T(8,128)(2,1)S(1)}, bf16[32,2048]{1,0:T(8,128)(2,1)S(1)}, u32[]{:S(2)}, u32[]{:S(2)}) collective-permute-start(bf16[32,2048]{1,0:T(8,128)(2,1)S(1)} %get-tuple-element.32), channel_id=1, source_target_pairs={{0,3},{1,2},{2,1},{3,0},{4,7},{5,6},{6,5},{7,4},{8,11},{9,10},{10,... | collective-permute-start | bytes 393224 | tf_op jit(solution)/shard_map/ppermute | solution.py:31
  21.6 8.2 %collective-permute-start.4 = (bf16[32,2048]{1,0:T(8,128)(2,1)S(1)}, bf16[32,2048]{1,0:T(8,128)(2,1)S(1)}, u32[]{:S(2)}, u32[]{:S(2)}) collective-permute-start(bf16[32,2048]{1,0:T(8,128)(2,1)S(1)} %get-tuple-element.33), channel_id=1, source_target_pairs={{0,2},{1,3},{2,0},{3,1},{4,6},{5,7},{6,4},{7,5},{8,10},{9,11},{10,... | collective-permute-start | bytes 393224 | tf_op jit(solution)/shard_map/ppermute | solution.py:31
  22.8 7.0 %collective-permute-start.5 = (bf16[32,2048]{1,0:T(8,128)(2,1)S(1)}, bf16[32,2048]{1,0:T(8,128)(2,1)S(1)}, u32[]{:S(2)}, u32[]{:S(2)}) collective-permute-start(bf16[32,2048]{1,0:T(8,128)(2,1)S(1)} %get-tuple-element.34), channel_id=1, source_target_pairs={{0,1},{1,0},{2,3},{3,2},{4,5},{5,4},{6,7},{7,6},{8,9},{9,8},{10,11... | collective-permute-start | bytes 393224 | tf_op jit(solution)/shard_map/ppermute | solution.py:31
  30.1 10.3 %collective-permute-start.12 = (bf16[32,2048]{1,0:T(8,128)(2,1)S(1)}, bf16[32,2048]{1,0:T(8,128)(2,1)S(1)}, u32[]{:S(2)}, u32[]{:S(2)}) collective-permute-start(bf16[32,2048]{1,0:T(8,128)(2,1)S(1)} %get-tuple-element.36), channel_id=1, source_target_pairs={{0,12},{4,0},{8,4},{12,8},{1,13},{5,1},{9,5},{13,9},{2,14},{6,2},{... | collective-permute-start | bytes 393224 | tf_op jit(solution)/shard_map/ppermute | solution.py:26
  36.4 11.6 %collective-permute-start.13 = (bf16[32,2048]{1,0:T(8,128)(2,1)S(1)}, bf16[32,2048]{1,0:T(8,128)(2,1)S(1)}, u32[]{:S(2)}, u32[]{:S(2)}) collective-permute-start(bf16[32,2048]{1,0:T(8,128)(2,1)S(1)} %get-tuple-element.36), channel_id=1, source_target_pairs={{0,8},{4,12},{8,0},{12,4},{1,9},{5,13},{9,1},{13,5},{2,10},{6,14},... | collective-permute-start | bytes 393224 | tf_op jit(solution)/shard_map/ppermute | solution.py:26
  36.4 12.5 %collective-permute-start.6 = (bf16[32,2048]{1,0:T(8,128)(2,1)S(1)}, bf16[32,2048]{1,0:T(8,128)(2,1)S(1)}, u32[]{:S(2)}, u32[]{:S(2)}) collective-permute-start(bf16[32,2048]{1,0:T(8,128)(2,1)S(1)} %get-tuple-element.36), channel_id=1, source_target_pairs={{0,4},{4,8},{8,12},{12,0},{1,5},{5,9},{9,13},{13,1},{2,6},{6,10},{... | collective-permute-start | bytes 393224 | tf_op jit(solution)/shard_map/ppermute | solution.py:26
  48.0 9.2 %collective-permute-start.14 = (bf16[64,2048]{1,0:T(8,128)(2,1)S(1)}, bf16[64,2048]{1,0:T(8,128)(2,1)S(1)}, u32[]{:S(2)}, u32[]{:S(2)}) collective-permute-start(bf16[64,2048]{1,0:T(8,128)(2,1)S(1)} %pad_maximum_fusion.1), channel_id=1, source_target_pairs={{0,2},{1,3},{2,0},{3,1},{4,6},{5,7},{6,4},{7,5},{8,10},{9,11},{10,... | collective-permute-start | bytes 786440 | tf_op jit(solution)/shard_map/ppermute | solution.py:31
  48.9 12.5 %collective-permute-start.7 = (bf16[64,2048]{1,0:T(8,128)(2,1)S(1)}, bf16[64,2048]{1,0:T(8,128)(2,1)S(1)}, u32[]{:S(2)}, u32[]{:S(2)}) collective-permute-start(bf16[64,2048]{1,0:T(8,128)(2,1)S(1)} %pad_maximum_fusion), channel_id=1, source_target_pairs={{0,2},{1,3},{2,0},{3,1},{4,6},{5,7},{6,4},{7,5},{8,10},{9,11},{10,... | collective-permute-start | bytes 786440 | tf_op jit(solution)/shard_map/ppermute | solution.py:31
  57.3 4.2 %collective-permute-start.15 = (bf16[128,2048]{1,0:T(8,128)(2,1)S(1)}, bf16[128,2048]{1,0:T(8,128)(2,1)S(1)}, u32[]{:S(2)}, u32[]{:S(2)}) collective-permute-start(bf16[128,2048]{1,0:T(8,128)(2,1)S(1)} %constant_dynamic-update-slice_fusion.3.near_ref), channel_id=1, source_target_pairs={{0,1},{1,0},{2,3},{3,2},{4,5},{5,4},{6,7},{7,6},{8,9},{9,8},{10,11... | collective-permute-start | bytes 1572872 | tf_op jit(solution)/shard_map/ppermute | solution.py:31
  61.4 3.3 %collective-permute-start.8 = (bf16[128,2048]{1,0:T(8,128)(2,1)S(1)}, bf16[128,2048]{1,0:T(8,128)(2,1)S(1)}, u32[]{:S(2)}, u32[]{:S(2)}) collective-permute-start(bf16[128,2048]{1,0:T(8,128)(2,1)S(1)} %constant_dynamic-update-slice_fusion.near_ref), channel_id=1, source_target_pairs={{0,1},{1,0},{2,3},{3,2},{4,5},{5,4},{6,7},{7,6},{8,9},{9,8},{10,11... | collective-permute-start | bytes 1572872 | tf_op jit(solution)/shard_map/ppermute | solution.py:31
  64.2 3.3 %collective-permute-start.16 = (bf16[128,2048]{1,0:T(8,128)(2,1)S(1)}, bf16[128,2048]{1,0:T(8,128)(2,1)S(1)}, u32[]{:S(2)}, u32[]{:S(2)}) collective-permute-start(bf16[128,2048]{1,0:T(8,128)(2,1)S(1)} %get-tuple-element.40), channel_id=1, source_target_pairs={{0,1},{1,0},{2,3},{3,2},{4,5},{5,4},{6,7},{7,6},{8,9},{9,8},{10,11... | collective-permute-start | bytes 1572872 | tf_op jit(solution)/shard_map/ppermute | solution.py:31
  67.3 2.0 %collective-permute-start.9 = (bf16[128,2048]{1,0:T(8,128)(2,1)S(1)}, bf16[128,2048]{1,0:T(8,128)(2,1)S(1)}, u32[]{:S(2)}, u32[]{:S(2)}) collective-permute-start(bf16[128,2048]{1,0:T(8,128)(2,1)S(1)} %get-tuple-element.38), channel_id=1, source_target_pairs={{0,1},{1,0},{2,3},{3,2},{4,5},{5,4},{6,7},{7,6},{8,9},{9,8},{10,11... | collective-permute-start | bytes 1572872 | tf_op jit(solution)/shard_map/ppermute | solution.py:31
  67.4 14.9 %copy-start.12 = (f32[32,2]{0,1:T(2,128)S(1)}, f32[32,2]{0,1:T(2,128)}, u32[]{:S(2)}) copy-start(f32[32,2]{0,1:T(2,128)} %param.24) | copy-start | bytes 772
  67.4 14.9 %copy-start.13 = (s32[32,2]{0,1:T(2,128)S(1)}, s32[32,2]{0,1:T(2,128)}, u32[]{:S(2)}) copy-start(s32[32,2]{0,1:T(2,128)} %param.23) | copy-start | bytes 772
  67.6 9.2 %collective-permute-start.17 = (bf16[64,2048]{1,0:T(8,128)(2,1)S(1)}, bf16[64,2048]{1,0:T(8,128)(2,1)S(1)}, u32[]{:S(2)}, u32[]{:S(2)}) collective-permute-start(bf16[64,2048]{1,0:T(8,128)(2,1)S(1)} %slice.53), channel_id=1, source_target_pairs={{0,2},{1,3},{2,0},{3,1},{4,6},{5,7},{6,4},{7,5},{8,10},{9,11},{10,... | collective-permute-start | bytes 786440 | tf_op jit(solution)/shard_map/ppermute | solution.py:31
  69.5 12.5 %collective-permute-start.10 = (bf16[64,2048]{1,0:T(8,128)(2,1)S(1)}, bf16[64,2048]{1,0:T(8,128)(2,1)S(1)}, u32[]{:S(2)}, u32[]{:S(2)}) collective-permute-start(bf16[64,2048]{1,0:T(8,128)(2,1)S(1)} %slice.49), channel_id=1, source_target_pairs={{0,2},{1,3},{2,0},{3,1},{4,6},{5,7},{6,4},{7,5},{8,10},{9,11},{10,... | collective-permute-start | bytes 786440 | tf_op jit(solution)/shard_map/ppermute | solution.py:31
  76.9 9.2 %collective-permute-start.19 = (bf16[32,2048]{1,0:T(8,128)(2,1)S(1)}, bf16[32,2048]{1,0:T(8,128)(2,1)S(1)}, u32[]{:S(2)}, u32[]{:S(2)}) collective-permute-start(bf16[32,2048]{1,0:T(8,128)(2,1)S(1)} %get-tuple-element.46), channel_id=1, source_target_pairs={{0,8},{4,12},{8,0},{12,4},{1,9},{5,13},{9,1},{13,5},{2,10},{6,14},... | collective-permute-start | bytes 393224 | tf_op jit(solution)/shard_map/ppermute | solution.py:26
  77.0 9.2 %collective-permute-start.18 = (bf16[32,2048]{1,0:T(8,128)(2,1)S(1)}, bf16[32,2048]{1,0:T(8,128)(2,1)S(1)}, u32[]{:S(2)}, u32[]{:S(2)}) collective-permute-start(bf16[32,2048]{1,0:T(8,128)(2,1)S(1)} %get-tuple-element.45), channel_id=1, source_target_pairs={{0,4},{4,8},{8,12},{12,0},{1,5},{5,9},{9,13},{13,1},{2,6},{6,10},{... | collective-permute-start | bytes 393224 | tf_op jit(solution)/shard_map/ppermute | solution.py:26
  82.0 6.5 %collective-permute-start.11 = (bf16[32,2048]{1,0:T(8,128)(2,1)S(1)}, bf16[32,2048]{1,0:T(8,128)(2,1)S(1)}, u32[]{:S(2)}, u32[]{:S(2)}) collective-permute-start(bf16[32,2048]{1,0:T(8,128)(2,1)S(1)} %slice.51), channel_id=1, source_target_pairs={{0,12},{4,0},{8,4},{12,8},{1,13},{5,1},{9,5},{13,9},{2,14},{6,2},{... | collective-permute-start | bytes 393224 | tf_op jit(solution)/shard_map/ppermute | solution.py:26

commit v3 on v2

--- a/solution.py
+++ b/solution.py
@@ -13,7 +13,7 @@
 KV_HEADS = 8
 DH = 128
 TOPK = 2
-DOC_ROWS = 16
+DOC_ROWS = 8
 DIRECT_KEYS = 1024
 SMALL = 20 * 2**20
 VMEM = pl.BlockSpec(memory_space=pltpu.VMEM)
@@ -176,7 +176,6 @@
         in_specs=[VMEM, VMEM, VMEM, SMEM, VMEM, VMEM],
         out_specs=(VMEM, VMEM),
         cost_estimate=cost(6 * 10**9, 10**6),
-        compiler_params=pltpu.CompilerParams(vmem_limit_bytes=SMALL),
         name="attend_here",
     )(queries, keys, values, head_bias, col, row)
     place = jnp.stack([lax.axis_index("sp"), lax.axis_index("tp")]).astype(jnp.int32)
@@ -211,12 +210,13 @@
     masks = [1 << bit for bit in range(tp_count.bit_length() - 1)]
     steps = [0] + [s for pair in zip(range(1, sp_count), range(sp_count - 1, 0, -1)) for s in pair]
     steps = list(dict.fromkeys(steps))
-    half = (len(steps) + 1) // 2
+    chunks = [steps[:1]] + [steps[at : at + 2] for at in range(1, len(steps), 2)]
     moved = {0: normed}
-    for s in steps[1:]:
-        moved[s] = shifted(normed, s, True)
+    for chunk in chunks[1:]:
+        for s in chunk:
+            moved[s] = shifted(normed, s, True)
     pieces = {}
-    for chunk in (steps[:half], steps[half:]):
+    for at, chunk in enumerate(chunks):
         held = jnp.concatenate([moved[s] for s in chunk], axis=0)
         for mask in masks[:0:-1]:
             other = swapped(held, mask)

time: 89.8 us -> 88 us (0.980)
  waiting for transfers between devices: 46.4 us -> 35.4 us
  starting transfers between devices: 25.5 us -> 33.7 us
  Pallas kernels: 10.4 us -> 12 us
  local copies, waits for them, and re-layouts: 3.78 us -> 2.82 us
    ppermute x11 -> x15, waiting for transfers between devices: 29.2 us -> 22.1 us  [swapped(): return lax.ppermute(value, 'tp', [(i, i ^ mask) for i in range(count)])]
    ppermute x9, starting transfers between devices: 18.8 us -> 24.4 us  [shifted(): return lax.ppermute(value, 'sp', pairs)]
    ppermute x9, waiting for transfers between devices: 17.3 us -> 13.3 us  [shifted(): return lax.ppermute(value, 'sp', pairs)]
    ppermute x11 -> x15, starting transfers between devices: 6.74 us -> 9.3 us  [swapped(): return lax.ppermute(value, 'tp', [(i, i ^ mask) for i in range(count)])]
    unnamed x32 -> x30, local copies, waits for them, and re-layouts: 3.56 us -> 1.98 us
    pallas_call x1, Pallas kernels: 1.21 us -> 2.5 us  [middle_direct(): pl.pallas_call(here_kernel, out_shape=(jax.ShapeDtypeStruct((rows, width)...]
    pallas_call x2 -> x3, Pallas kernels: 5.23 us -> 5.54 us  [experts_dense(): pl.pallas_call(expert_kernel, out_shape=[jax.ShapeDtypeStruct((count, D),...]
  transfers between devices with their start and end apart: 20 -> 24, of which waited for: 11 -> 11; matrix products, arithmetic and copies ran while one was open for 1% -> 2% of each run, Pallas kernels for 7% -> 9%
where the time goes in v3:
time: 88 us; the launch traced here: 87.7 us
  waiting for transfers between devices  35.4 us (40%)
  starting transfers between devices  33.7 us (38%)
  Pallas kernels  12 us (14%)
  other arithmetic  3.49 us (4%)
  local copies, waits for them, and re-layouts  2.82 us (3%)
    ppermute x9, starting transfers between devices, shifted(): return lax.ppermute(value, 'sp', pairs)  24.4 us
    ppermute x15, waiting for transfers between devices, swapped(): return lax.ppermute(value, 'tp', [(i, i ^ mask) for i in range(count)])  22.1 us
    ppermute x9, waiting for transfers between devices, shifted(): return lax.ppermute(value, 'sp', pairs)  13.3 us
    ppermute x15, starting transfers between devices, swapped(): return lax.ppermute(value, 'tp', [(i, i ^ mask) for i in range(count)])  9.3 us
    pallas_call x3, Pallas kernels, experts_dense(): pl.pallas_call(expert_kernel, out_shape=[jax.ShapeDtypeStruct((count, D),...  5.54 us
    pallas_call x1, Pallas kernels, middle_direct(): pl.pallas_call(functools.partial(away_kernel, sp_count - 1, order), out_s...  3.77 us
    pallas_call x1, Pallas kernels, middle_direct(): pl.pallas_call(here_kernel, out_shape=(jax.ShapeDtypeStruct((rows, width)...  2.5 us
    unnamed x30, local copies, waits for them, and re-layouts  1.98 us
  transfers between devices with their start and end apart: 24, of which 11 were waited for; matrix products, arithmetic and copies ran while one was open for 2% of the time, Pallas kernels for 9%

profile of v3, /device:TPU:0, one launch (start us, length us, event | category | flops | bytes accessed | tf_op | source)
XLA Modules:
  0.0 87.7 jit_solution(9933120297473766283)
XLA Ops:
  0.0 1.3 %convert_bitcast_fusion = (bf16[1,128]{1,0:T(2,128)(2,1)S(1)}, f32[1,128]{1,0:T(1,128)}, f32[128,1]{0,1:T(1,128)S(1)}) fusion(s32[128]{0:T(128)} %param.19), kind=kLoop, calls=%fused_computation.27 | loop fusion | flops 256 | bytes 1792 | tf_op jit(solution)/shard_map/reshape.30
  1.3 0.9 %fusion.1 = bf16[136,512]{1,0:T(8,128)(2,1)S(1)} fusion(bf16[1,128]{1,0:T(2,128)(2,1)S(1)} %get-tuple-element.51, bf16[128,256]{1,0:T(8,128)(2,1)} %v_ref.1, bf16[128,256]{1,0:T(8,128)(2,1)} %k_ref.1), kind=kLoop, calls=%fused_computation.10 | loop fusion | flops 557056 | bytes 270592 | tf_op jit(solution)/shard_map/concatenate | solution.py:165
  2.2 5.0 %collective-permute-start = (bf16[136,512]{1,0:T(8,128)(2,1)S(1)}, bf16[136,512]{1,0:T(8,128)(2,1)S(1)}, u32[]{:S(2)}, u32[]{:S(2)}) collective-permute-start(bf16[136,512]{1,0:T(8,128)(2,1)S(1)} %fusion.1), channel_id=1, source_target_pairs={{0,4},{4,8},{8,12},{1,5},{5,9},{9,13},{2,6},{6,10},{10,14},{3,7},{... | collective-permute-start | bytes 417800 | tf_op jit(solution)/shard_map/ppermute | solution.py:26
  7.2 4.5 %collective-permute-start.1 = (bf16[136,512]{1,0:T(8,128)(2,1)S(1)}, bf16[136,512]{1,0:T(8,128)(2,1)S(1)}, u32[]{:S(2)}, u32[]{:S(2)}) collective-permute-start(bf16[136,512]{1,0:T(8,128)(2,1)S(1)} %fusion.1), channel_id=1, source_target_pairs={{0,8},{4,12},{1,9},{5,13},{2,10},{6,14},{3,11},{7,15},{16,24},{20,... | collective-permute-start | bytes 417800 | tf_op jit(solution)/shard_map/ppermute | solution.py:26
  11.7 1.3 %collective-permute-start.2 = (bf16[136,512]{1,0:T(8,128)(2,1)S(1)}, bf16[136,512]{1,0:T(8,128)(2,1)S(1)}, u32[]{:S(2)}, u32[]{:S(2)}) collective-permute-start(bf16[136,512]{1,0:T(8,128)(2,1)S(1)} %fusion.1), channel_id=1, source_target_pairs={{0,12},{1,13},{2,14},{3,15},{16,28},{17,29},{18,30},{19,31}} | collective-permute-start | bytes 417800 | tf_op jit(solution)/shard_map/ppermute | solution.py:26
  13.0 0.7 copy.15.col_ref
  13.7 2.5 %attend_here.1 = (f32[128,512]{1,0:T(8,128)}, f32[512,128]{1,0:T(8,128)}) custom-call(bf16[128,512]{1,0:T(8,128)(2,1)} %q_ref.3, bf16[128,256]{1,0:T(8,128)(2,1)} %k_ref.1, bf16[128,256]{1,0:T(8,128)(2,1)} %v_ref.1, f32[4]{0:T(128)} %bias_ref.3, f32[128,1]{1,0:T(8,128)} %copy.15.col_ref, f32[1,128]{1,0:T(1,128)} %get-tuple-element.52.row_ref), custom_call_target="tpu_custom_call" | custom-call | flops 6000000000 | bytes 1000000 | tf_op jit(solution)/shard_map/attend_here/pallas_call | solution.py:170
  16.2 0.1 pad_add_fusion.place_ref
  16.3 1.0 %collective-permute-done.2.refs_2_ = bf16[136,512]{1,0:T(8,128)(2,1)S(1)} collective-permute-done((bf16[136,512]{1,0:T(8,128)(2,1)S(1)}, bf16[136,512]{1,0:T(8,128)(2,1)S(1)}, u32[]{:S(2)}, u32[]{:S(2)}) %collective-permute-start.2) | collective-permute-done | bytes 139296 | tf_op jit(solution)/shard_map/ppermute | solution.py:26
  17.3 0.9 %copy-done.9 = f32[128,512]{1,0:T(8,128)S(1)} copy-done((f32[128,512]{1,0:T(8,128)S(1)}, f32[128,512]{1,0:T(8,128)}, u32[]{:S(2)}) %copy-start.9) | copy-done | bytes 262168
  18.3 0.9 %copy-done.10 = f32[512,128]{1,0:T(8,128)S(1)} copy-done((f32[512,128]{1,0:T(8,128)S(1)}, f32[512,128]{1,0:T(8,128)}, u32[]{:S(2)}) %copy-start.10) | copy-done | bytes 262168
  19.3 3.8 %attend_away.1 = (bf16[32,2048]{1,0:T(8,128)(2,1)S(1)}, bf16[32,2048]{1,0:T(8,128)(2,1)S(1)}, bf16[32,2048]{1,0:T(8,128)(2,1)S(1)}, bf16[32,2048]{1,0:T(8,128)(2,1)S(1)}) custom-call(s32[2]{0:T(128)S(1)} %pad_add_fusion.place_ref, bf16[128,512]{1,0:T(8,128)(2,1)S(1)} %copy-done.7, f32[4]{0:T(128)S(1)} %copy-done.8, f32[128,1]{1,0:T(8,128)S(1)} %copy-done.4, ...), custom_call_target="tpu_custom_call" | custom-call | flops 10000000000 | bytes 4000000 | tf_op jit(solution)/shard_map/attend_away/pallas_call | solution.py:184
  23.0 0.1 collective-permute-start.3
  23.1 1.6 %collective-permute-start.4 = (bf16[32,2048]{1,0:T(8,128)(2,1)S(1)}, bf16[32,2048]{1,0:T(8,128)(2,1)S(1)}, u32[]{:S(2)}, u32[]{:S(2)}) collective-permute-start(bf16[32,2048]{1,0:T(8,128)(2,1)S(1)} %get-tuple-element.35), channel_id=1, source_target_pairs={{0,2},{1,3},{2,0},{3,1},{4,6},{5,7},{6,4},{7,5},{8,10},{9,11},{10,... | collective-permute-start | bytes 393224 | tf_op jit(solution)/shard_map/ppermute | solution.py:31
  24.7 0.3 collective-permute-start.5
  25.0 3.9 %collective-permute-done.3.refs_1_ = bf16[32,2048]{1,0:T(8,128)(2,1)S(1)} collective-permute-done((bf16[32,2048]{1,0:T(8,128)(2,1)S(1)}, bf16[32,2048]{1,0:T(8,128)(2,1)S(1)}, u32[]{:S(2)}, u32[]{:S(2)}) %collective-permute-start.3) | collective-permute-done | bytes 131104 | tf_op jit(solution)/shard_map/ppermute | solution.py:31
  28.8 2.9 %collective-permute-done.4.refs_2_ = bf16[32,2048]{1,0:T(8,128)(2,1)S(1)} collective-permute-done((bf16[32,2048]{1,0:T(8,128)(2,1)S(1)}, bf16[32,2048]{1,0:T(8,128)(2,1)S(1)}, u32[]{:S(2)}, u32[]{:S(2)}) %collective-permute-start.4) | collective-permute-done | bytes 131104 | tf_op jit(solution)/shard_map/ppermute | solution.py:31
  31.7 0.2 middle_norm.1
  31.9 1.9 %collective-permute-start.18 = (bf16[32,2048]{1,0:T(8,128)(2,1)S(1)}, bf16[32,2048]{1,0:T(8,128)(2,1)S(1)}, u32[]{:S(2)}, u32[]{:S(2)}) collective-permute-start(bf16[32,2048]{1,0:T(8,128)(2,1)S(1)} %get-tuple-element.38), channel_id=1, source_target_pairs={{0,8},{4,12},{8,0},{12,4},{1,9},{5,13},{9,1},{13,5},{2,10},{6,14},... | collective-permute-start | bytes 393224 | tf_op jit(solution)/shard_map/ppermute | solution.py:26
  33.8 4.8 %collective-permute-start.10 = (bf16[32,2048]{1,0:T(8,128)(2,1)S(1)}, bf16[32,2048]{1,0:T(8,128)(2,1)S(1)}, u32[]{:S(2)}, u32[]{:S(2)}) collective-permute-start(bf16[32,2048]{1,0:T(8,128)(2,1)S(1)} %get-tuple-element.38), channel_id=1, source_target_pairs={{0,4},{4,8},{8,12},{12,0},{1,5},{5,9},{9,13},{13,1},{2,6},{6,10},{... | collective-permute-start | bytes 393224 | tf_op jit(solution)/shard_map/ppermute | solution.py:26
  38.7 0.7 collective-permute-start.6
  39.4 5.9 %collective-permute-done.10 = bf16[32,2048]{1,0:T(8,128)(2,1)S(1)} collective-permute-done((bf16[32,2048]{1,0:T(8,128)(2,1)S(1)}, bf16[32,2048]{1,0:T(8,128)(2,1)S(1)}, u32[]{:S(2)}, u32[]{:S(2)}) %collective-permute-start.10) | collective-permute-done | bytes 131104 | tf_op jit(solution)/shard_map/ppermute | solution.py:26
  45.3 1.1 %collective-permute-done.11 = bf16[32,2048]{1,0:T(8,128)(2,1)S(1)} collective-permute-done((bf16[32,2048]{1,0:T(8,128)(2,1)S(1)}, bf16[32,2048]{1,0:T(8,128)(2,1)S(1)}, u32[]{:S(2)}, u32[]{:S(2)}) %collective-permute-start.11) | collective-permute-done | bytes 131104 | tf_op jit(solution)/shard_map/ppermute | solution.py:26
  46.4 0.9 %collective-permute-start.12 = (bf16[64,2048]{1,0:T(8,128)(2,1)S(1)}, bf16[64,2048]{1,0:T(8,128)(2,1)S(1)}, u32[]{:S(2)}, u32[]{:S(2)}) collective-permute-start(bf16[64,2048]{1,0:T(8,128)(2,1)S(1)} %pad_maximum_fusion), channel_id=1, source_target_pairs={{0,2},{1,3},{2,0},{3,1},{4,6},{5,7},{6,4},{7,5},{8,10},{9,11},{10,... | collective-permute-start | bytes 786440 | tf_op jit(solution)/shard_map/ppermute | solution.py:31
  47.4 0.1 collective-permute-start.7
  47.5 1.2 %collective-permute-start.19 = (bf16[32,2048]{1,0:T(8,128)(2,1)S(1)}, bf16[32,2048]{1,0:T(8,128)(2,1)S(1)}, u32[]{:S(2)}, u32[]{:S(2)}) collective-permute-start(bf16[32,2048]{1,0:T(8,128)(2,1)S(1)} %collective-permute-done.18), channel_id=1, source_target_pairs={{0,2},{1,3},{2,0},{3,1},{4,6},{5,7},{6,4},{7,5},{8,10},{9,11},{10,... | collective-permute-start | bytes 393224 | tf_op jit(solution)/shard_map/ppermute | solution.py:31
  48.7 6.5 %collective-permute-done.12 = bf16[64,2048]{1,0:T(8,128)(2,1)S(1)} collective-permute-done((bf16[64,2048]{1,0:T(8,128)(2,1)S(1)}, bf16[64,2048]{1,0:T(8,128)(2,1)S(1)}, u32[]{:S(2)}, u32[]{:S(2)}) %collective-permute-start.12) | collective-permute-done | bytes 262176 | tf_op jit(solution)/shard_map/ppermute | solution.py:31
  55.2 0.1 collective-permute-start.13
  55.3 1.3 %collective-permute-done.19 = bf16[32,2048]{1,0:T(8,128)(2,1)S(1)} collective-permute-done((bf16[32,2048]{1,0:T(8,128)(2,1)S(1)}, bf16[32,2048]{1,0:T(8,128)(2,1)S(1)}, u32[]{:S(2)}, u32[]{:S(2)}) %collective-permute-start.19) | collective-permute-done | bytes 131104 | tf_op jit(solution)/shard_map/ppermute | solution.py:31
  56.6 0.1 collective-permute-start.20
  56.8 1.5 %shard_map.127 = (bf16[64,2048]{1,0:T(8,128)(2,1)S(1)}, bf16[64,2048]{1,0:T(8,128)(2,1)S(1)}) custom-call(bf16[64,2048]{1,0:T(8,128)(2,1)S(1)} %constant_dynamic-update-slice_fusion.near_ref, bf16[64,2048]{1,0:T(8,128)(2,1)S(1)} %collective-permute-done.7.far_ref, bf16[1,2048,768]{2,1,0:T(8,128)(2,1)S(1)} %copy-done, bf16[1,2048,768]{2,1,0:T(8,128)(2,1)S(1)} %copy-done.1, ...), custom_call_target="tpu_custom_call" | custom-call | flops 1207959552 | bytes 12000000 | tf_op jit(solution)/shard_map/pallas_call | solution.py:226
  58.2 0.5 collective-permute-start.8
  58.8 1.5 %shard_map.129 = (bf16[64,2048]{1,0:T(8,128)(2,1)S(1)}, bf16[64,2048]{1,0:T(8,128)(2,1)S(1)}) custom-call(bf16[64,2048]{1,0:T(8,128)(2,1)S(1)} %constant_dynamic-update-slice_fusion.5.near_ref, bf16[64,2048]{1,0:T(8,128)(2,1)S(1)} %collective-permute-done.20.far_ref, bf16[1,2048,768]{2,1,0:T(8,128)(2,1)S(1)} %copy-done, bf16[1,2048,768]{2,1,0:T(8,128)(2,1)S(1)} %copy-done.1, ...), custom_call_target="tpu_custom_call" | custom-call | flops 1207959552 | bytes 12000000 | tf_op jit(solution)/shard_map/pallas_call | solution.py:226
  60.2 0.1 collective-permute-start.21
  60.3 2.6 %shard_map.128 = (bf16[128,2048]{1,0:T(8,128)(2,1)S(1)}, bf16[128,2048]{1,0:T(8,128)(2,1)S(1)}) custom-call(bf16[128,2048]{1,0:T(8,128)(2,1)S(1)} %constant_dynamic-update-slice_fusion.2.near_ref, bf16[128,2048]{1,0:T(8,128)(2,1)S(1)} %collective-permute-done.13.far_ref, bf16[1,2048,768]{2,1,0:T(8,128)(2,1)S(1)} %copy-done, ...), custom_call_target="tpu_custom_call" | custom-call | flops 2415919104 | bytes 12000000 | tf_op jit(solution)/shard_map/pallas_call | solution.py:226
  63.0 0.5 collective-permute-start.14
  63.6 0.9 %collective-permute-start.9 = (bf16[32,2048]{1,0:T(8,128)(2,1)S(1)}, bf16[32,2048]{1,0:T(8,128)(2,1)S(1)}, u32[]{:S(2)}, u32[]{:S(2)}) collective-permute-start(bf16[32,2048]{1,0:T(8,128)(2,1)S(1)} %slice.49), channel_id=1, source_target_pairs={{0,2},{1,3},{2,0},{3,1},{4,6},{5,7},{6,4},{7,5},{8,10},{9,11},{10,... | collective-permute-start | bytes 393224 | tf_op jit(solution)/shard_map/ppermute | solution.py:31
  64.6 1.2 %collective-permute-start.22 = (bf16[32,2048]{1,0:T(8,128)(2,1)S(1)}, bf16[32,2048]{1,0:T(8,128)(2,1)S(1)}, u32[]{:S(2)}, u32[]{:S(2)}) collective-permute-start(bf16[32,2048]{1,0:T(8,128)(2,1)S(1)} %slice.55), channel_id=1, source_target_pairs={{0,2},{1,3},{2,0},{3,1},{4,6},{5,7},{6,4},{7,5},{8,10},{9,11},{10,... | collective-permute-start | bytes 393224 | tf_op jit(solution)/shard_map/ppermute | solution.py:31
  65.9 0.1 add_convert_fusion
  66.0 0.9 %collective-permute-start.15 = (bf16[64,2048]{1,0:T(8,128)(2,1)S(1)}, bf16[64,2048]{1,0:T(8,128)(2,1)S(1)}, u32[]{:S(2)}, u32[]{:S(2)}) collective-permute-start(bf16[64,2048]{1,0:T(8,128)(2,1)S(1)} %slice.51), channel_id=1, source_target_pairs={{0,2},{1,3},{2,0},{3,1},{4,6},{5,7},{6,4},{7,5},{8,10},{9,11},{10,... | collective-permute-start | bytes 786440 | tf_op jit(solution)/shard_map/ppermute | solution.py:31
  67.0 5.9 %collective-permute-done.22 = bf16[32,2048]{1,0:T(8,128)(2,1)S(1)} collective-permute-done((bf16[32,2048]{1,0:T(8,128)(2,1)S(1)}, bf16[32,2048]{1,0:T(8,128)(2,1)S(1)}, u32[]{:S(2)}, u32[]{:S(2)}) %collective-permute-start.22) | collective-permute-done | bytes 131104 | tf_op jit(solution)/shard_map/ppermute | solution.py:31
  72.9 3.0 %collective-permute-start.23 = (bf16[32,2048]{1,0:T(8,128)(2,1)S(1)}, bf16[32,2048]{1,0:T(8,128)(2,1)S(1)}, u32[]{:S(2)}, u32[]{:S(2)}) collective-permute-start(bf16[32,2048]{1,0:T(8,128)(2,1)S(1)} %add_convert_fusion.5), channel_id=1, source_target_pairs={{0,8},{4,12},{8,0},{12,4},{1,9},{5,13},{9,1},{13,5},{2,10},{6,14},... | collective-permute-start | bytes 393224 | tf_op jit(solution)/shard_map/ppermute | solution.py:26
  75.9 1.6 %collective-permute-done.15 = bf16[64,2048]{1,0:T(8,128)(2,1)S(1)} collective-permute-done((bf16[64,2048]{1,0:T(8,128)(2,1)S(1)}, bf16[64,2048]{1,0:T(8,128)(2,1)S(1)}, u32[]{:S(2)}, u32[]{:S(2)}) %collective-permute-start.15) | collective-permute-done | bytes 262176 | tf_op jit(solution)/shard_map/ppermute | solution.py:31
  77.6 2.6 %collective-permute-start.17 = (bf16[32,2048]{1,0:T(8,128)(2,1)S(1)}, bf16[32,2048]{1,0:T(8,128)(2,1)S(1)}, u32[]{:S(2)}, u32[]{:S(2)}) collective-permute-start(bf16[32,2048]{1,0:T(8,128)(2,1)S(1)} %get-tuple-element.50), channel_id=1, source_target_pairs={{0,4},{4,8},{8,12},{12,0},{1,5},{5,9},{9,13},{13,1},{2,6},{6,10},{... | collective-permute-start | bytes 393224 | tf_op jit(solution)/shard_map/ppermute | solution.py:26
  80.2 1.3 %collective-permute-start.16 = (bf16[32,2048]{1,0:T(8,128)(2,1)S(1)}, bf16[32,2048]{1,0:T(8,128)(2,1)S(1)}, u32[]{:S(2)}, u32[]{:S(2)}) collective-permute-start(bf16[32,2048]{1,0:T(8,128)(2,1)S(1)} %get-tuple-element.49), channel_id=1, source_target_pairs={{0,12},{4,0},{8,4},{12,8},{1,13},{5,1},{9,5},{13,9},{2,14},{6,2},{... | collective-permute-start | bytes 393224 | tf_op jit(solution)/shard_map/ppermute | solution.py:26
  81.6 3.9 %collective-permute-done.17 = bf16[32,2048]{1,0:T(8,128)(2,1)S(1)} collective-permute-done((bf16[32,2048]{1,0:T(8,128)(2,1)S(1)}, bf16[32,2048]{1,0:T(8,128)(2,1)S(1)}, u32[]{:S(2)}, u32[]{:S(2)}) %collective-permute-start.17) | collective-permute-done | bytes 131104 | tf_op jit(solution)/shard_map/ppermute | solution.py:26
  85.5 1.4 %collective-permute-done.16 = bf16[32,2048]{1,0:T(8,128)(2,1)S(1)} collective-permute-done((bf16[32,2048]{1,0:T(8,128)(2,1)S(1)}, bf16[32,2048]{1,0:T(8,128)(2,1)S(1)}, u32[]{:S(2)}, u32[]{:S(2)}) %collective-permute-start.16) | collective-permute-done | bytes 131104 | tf_op jit(solution)/shard_map/ppermute | solution.py:26
  86.9 0.8 add_convert_fusion.4
  (55 shorter events, 0.5 us)
Async XLA Ops:
  2.2 14.1 %collective-permute-start = (bf16[136,512]{1,0:T(8,128)(2,1)S(1)}, bf16[136,512]{1,0:T(8,128)(2,1)S(1)}, u32[]{:S(2)}, u32[]{:S(2)}) collective-permute-start(bf16[136,512]{1,0:T(8,128)(2,1)S(1)} %fusion.1), channel_id=1, source_target_pairs={{0,4},{4,8},{8,12},{1,5},{5,9},{9,13},{2,6},{6,10},{10,14},{3,7},{... | collective-permute-start | bytes 417800 | tf_op jit(solution)/shard_map/ppermute | solution.py:26
  7.2 9.1 %collective-permute-start.1 = (bf16[136,512]{1,0:T(8,128)(2,1)S(1)}, bf16[136,512]{1,0:T(8,128)(2,1)S(1)}, u32[]{:S(2)}, u32[]{:S(2)}) collective-permute-start(bf16[136,512]{1,0:T(8,128)(2,1)S(1)} %fusion.1), channel_id=1, source_target_pairs={{0,8},{4,12},{1,9},{5,13},{2,10},{6,14},{3,11},{7,15},{16,24},{20,... | collective-permute-start | bytes 417800 | tf_op jit(solution)/shard_map/ppermute | solution.py:26
  11.7 5.7 %collective-permute-start.2 = (bf16[136,512]{1,0:T(8,128)(2,1)S(1)}, bf16[136,512]{1,0:T(8,128)(2,1)S(1)}, u32[]{:S(2)}, u32[]{:S(2)}) collective-permute-start(bf16[136,512]{1,0:T(8,128)(2,1)S(1)} %fusion.1), channel_id=1, source_target_pairs={{0,12},{1,13},{2,14},{3,15},{16,28},{17,29},{18,30},{19,31}} | collective-permute-start | bytes 417800 | tf_op jit(solution)/shard_map/ppermute | solution.py:26
  13.7 3.6 %copy-start.4 = (f32[128,1]{1,0:T(8,128)S(1)}, f32[128,1]{1,0:T(8,128)}, u32[]{:S(2)}) copy-start(f32[128,1]{1,0:T(8,128)} %copy.15.col_ref) | copy-start | bytes 1540
  13.7 3.6 %copy-start.6 = (bf16[512,2048]{1,0:T(8,128)(2,1)S(1)}, bf16[512,2048]{1,0:T(8,128)(2,1)}, u32[]{:S(2)}) copy-start(bf16[512,2048]{1,0:T(8,128)(2,1)} %w_ref.1) | copy-start | bytes 6291460
  13.7 3.6 %copy-start.7 = (bf16[128,512]{1,0:T(8,128)(2,1)S(1)}, bf16[128,512]{1,0:T(8,128)(2,1)}, u32[]{:S(2)}) copy-start(bf16[128,512]{1,0:T(8,128)(2,1)} %q_ref.3) | copy-start | bytes 393220
  13.7 3.6 %copy-start.8 = (f32[4]{0:T(128)S(1)}, f32[4]{0:T(128)}, u32[]{:S(2)}) copy-start(f32[4]{0:T(128)} %bias_ref.3) | copy-start | bytes 52
  17.3 1.0 %copy-start.9 = (f32[128,512]{1,0:T(8,128)S(1)}, f32[128,512]{1,0:T(8,128)}, u32[]{:S(2)}) copy-start(f32[128,512]{1,0:T(8,128)} %get-tuple-element.31.mix_ref) | copy-start | bytes 786436
  18.3 0.9 %copy-start.10 = (f32[512,128]{1,0:T(8,128)S(1)}, f32[512,128]{1,0:T(8,128)}, u32[]{:S(2)}) copy-start(f32[512,128]{1,0:T(8,128)} %get-tuple-element.32.carry_ref) | copy-start | bytes 786436
  19.2 12.5 %copy-start.3 = (bf16[32,2048]{1,0:T(8,128)(2,1)S(1)}, bf16[32,2048]{1,0:T(8,128)(2,1)}, u32[]{:S(2)}) copy-start(bf16[32,2048]{1,0:T(8,128)(2,1)} %resid_ref.1) | copy-start | bytes 393220
  19.2 12.5 %copy-start.5 = (f32[2048]{0:T(1024)S(1)}, f32[2048]{0:T(1024)}, u32[]{:S(2)}) copy-start(f32[2048]{0:T(1024)} %param.22) | copy-start | bytes 24580
  19.2 37.5 %copy-start.1 = (bf16[1,2048,768]{2,1,0:T(8,128)(2,1)S(1)}, bf16[1,2048,768]{2,1,0:T(8,128)(2,1)}, u32[]{:S(2)}) copy-start(bf16[1,2048,768]{2,1,0:T(8,128)(2,1)} %up_ref.5) | copy-start | bytes 9437188
  19.2 37.5 %copy-start.2 = (bf16[1,768,2048]{2,1,0:T(8,128)(2,1)S(1)}, bf16[1,768,2048]{2,1,0:T(8,128)(2,1)}, u32[]{:S(2)}) copy-start(bf16[1,768,2048]{2,1,0:T(8,128)(2,1)} %down_ref.5) | copy-start | bytes 9437188
  23.0 33.7 %copy-start = (bf16[1,2048,768]{2,1,0:T(8,128)(2,1)S(1)}, bf16[1,2048,768]{2,1,0:T(8,128)(2,1)}, u32[]{:S(2)}) copy-start(bf16[1,2048,768]{2,1,0:T(8,128)(2,1)} %gate_ref.5) | copy-start | bytes 9437188
  23.0 5.8 %collective-permute-start.3 = (bf16[32,2048]{1,0:T(8,128)(2,1)S(1)}, bf16[32,2048]{1,0:T(8,128)(2,1)S(1)}, u32[]{:S(2)}, u32[]{:S(2)}) collective-permute-start(bf16[32,2048]{1,0:T(8,128)(2,1)S(1)} %get-tuple-element.34), channel_id=1, source_target_pairs={{0,3},{1,2},{2,1},{3,0},{4,7},{5,6},{6,5},{7,4},{8,11},{9,10},{10,... | collective-permute-start | bytes 393224 | tf_op jit(solution)/shard_map/ppermute | solution.py:31
  23.1 8.6 %collective-permute-start.4 = (bf16[32,2048]{1,0:T(8,128)(2,1)S(1)}, bf16[32,2048]{1,0:T(8,128)(2,1)S(1)}, u32[]{:S(2)}, u32[]{:S(2)}) collective-permute-start(bf16[32,2048]{1,0:T(8,128)(2,1)S(1)} %get-tuple-element.35), channel_id=1, source_target_pairs={{0,2},{1,3},{2,0},{3,1},{4,6},{5,7},{6,4},{7,5},{8,10},{9,11},{10,... | collective-permute-start | bytes 393224 | tf_op jit(solution)/shard_map/ppermute | solution.py:31
  24.7 7.0 %collective-permute-start.5 = (bf16[32,2048]{1,0:T(8,128)(2,1)S(1)}, bf16[32,2048]{1,0:T(8,128)(2,1)S(1)}, u32[]{:S(2)}, u32[]{:S(2)}) collective-permute-start(bf16[32,2048]{1,0:T(8,128)(2,1)S(1)} %get-tuple-element.36), channel_id=1, source_target_pairs={{0,1},{1,0},{2,3},{3,2},{4,5},{5,4},{6,7},{7,6},{8,9},{9,8},{10,11... | collective-permute-start | bytes 393224 | tf_op jit(solution)/shard_map/ppermute | solution.py:31
  31.9 15.5 %collective-permute-start.18 = (bf16[32,2048]{1,0:T(8,128)(2,1)S(1)}, bf16[32,2048]{1,0:T(8,128)(2,1)S(1)}, u32[]{:S(2)}, u32[]{:S(2)}) collective-permute-start(bf16[32,2048]{1,0:T(8,128)(2,1)S(1)} %get-tuple-element.38), channel_id=1, source_target_pairs={{0,8},{4,12},{8,0},{12,4},{1,9},{5,13},{9,1},{13,5},{2,10},{6,14},... | collective-permute-start | bytes 393224 | tf_op jit(solution)/shard_map/ppermute | solution.py:26
  33.8 11.5 %collective-permute-start.10 = (bf16[32,2048]{1,0:T(8,128)(2,1)S(1)}, bf16[32,2048]{1,0:T(8,128)(2,1)S(1)}, u32[]{:S(2)}, u32[]{:S(2)}) collective-permute-start(bf16[32,2048]{1,0:T(8,128)(2,1)S(1)} %get-tuple-element.38), channel_id=1, source_target_pairs={{0,4},{4,8},{8,12},{12,0},{1,5},{5,9},{9,13},{13,1},{2,6},{6,10},{... | collective-permute-start | bytes 393224 | tf_op jit(solution)/shard_map/ppermute | solution.py:26
  38.7 7.7 %collective-permute-start.11 = (bf16[32,2048]{1,0:T(8,128)(2,1)S(1)}, bf16[32,2048]{1,0:T(8,128)(2,1)S(1)}, u32[]{:S(2)}, u32[]{:S(2)}) collective-permute-start(bf16[32,2048]{1,0:T(8,128)(2,1)S(1)} %get-tuple-element.38), channel_id=1, source_target_pairs={{0,12},{4,0},{8,4},{12,8},{1,13},{5,1},{9,5},{13,9},{2,14},{6,2},{... | collective-permute-start | bytes 393224 | tf_op jit(solution)/shard_map/ppermute | solution.py:26
  38.7 8.7 %collective-permute-start.6 = (bf16[32,2048]{1,0:T(8,128)(2,1)S(1)}, bf16[32,2048]{1,0:T(8,128)(2,1)S(1)}, u32[]{:S(2)}, u32[]{:S(2)}) collective-permute-start(bf16[32,2048]{1,0:T(8,128)(2,1)S(1)} %get-tuple-element.38), channel_id=1, source_target_pairs={{0,2},{1,3},{2,0},{3,1},{4,6},{5,7},{6,4},{7,5},{8,10},{9,11},{10,... | collective-permute-start | bytes 393224 | tf_op jit(solution)/shard_map/ppermute | solution.py:31
  46.4 8.8 %collective-permute-start.12 = (bf16[64,2048]{1,0:T(8,128)(2,1)S(1)}, bf16[64,2048]{1,0:T(8,128)(2,1)S(1)}, u32[]{:S(2)}, u32[]{:S(2)}) collective-permute-start(bf16[64,2048]{1,0:T(8,128)(2,1)S(1)} %pad_maximum_fusion), channel_id=1, source_target_pairs={{0,2},{1,3},{2,0},{3,1},{4,6},{5,7},{6,4},{7,5},{8,10},{9,11},{10,... | collective-permute-start | bytes 786440 | tf_op jit(solution)/shard_map/ppermute | solution.py:31
  47.4 9.3 %collective-permute-start.7 = (bf16[64,2048]{1,0:T(8,128)(2,1)S(1)}, bf16[64,2048]{1,0:T(8,128)(2,1)S(1)}, u32[]{:S(2)}, u32[]{:S(2)}) collective-permute-start(bf16[64,2048]{1,0:T(8,128)(2,1)S(1)} %constant_dynamic-update-slice_fusion.near_ref), channel_id=1, source_target_pairs={{0,1},{1,0},{2,3},{3,2},{4,5},{5,4},{6,7},{7,6},{8,9},{9,8},{10,11... | collective-permute-start | bytes 786440 | tf_op jit(solution)/shard_map/ppermute | solution.py:31
  47.5 9.1 %collective-permute-start.19 = (bf16[32,2048]{1,0:T(8,128)(2,1)S(1)}, bf16[32,2048]{1,0:T(8,128)(2,1)S(1)}, u32[]{:S(2)}, u32[]{:S(2)}) collective-permute-start(bf16[32,2048]{1,0:T(8,128)(2,1)S(1)} %collective-permute-done.18), channel_id=1, source_target_pairs={{0,2},{1,3},{2,0},{3,1},{4,6},{5,7},{6,4},{7,5},{8,10},{9,11},{10,... | collective-permute-start | bytes 393224 | tf_op jit(solution)/shard_map/ppermute | solution.py:31
  55.2 5.1 %collective-permute-start.13 = (bf16[128,2048]{1,0:T(8,128)(2,1)S(1)}, bf16[128,2048]{1,0:T(8,128)(2,1)S(1)}, u32[]{:S(2)}, u32[]{:S(2)}) collective-permute-start(bf16[128,2048]{1,0:T(8,128)(2,1)S(1)} %constant_dynamic-update-slice_fusion.2.near_ref), channel_id=1, source_target_pairs={{0,1},{1,0},{2,3},{3,2},{4,5},{5,4},{6,7},{7,6},{8,9},{9,8},{10,11... | collective-permute-start | bytes 1572872 | tf_op jit(solution)/shard_map/ppermute | solution.py:31
  56.6 2.1 %collective-permute-start.20 = (bf16[64,2048]{1,0:T(8,128)(2,1)S(1)}, bf16[64,2048]{1,0:T(8,128)(2,1)S(1)}, u32[]{:S(2)}, u32[]{:S(2)}) collective-permute-start(bf16[64,2048]{1,0:T(8,128)(2,1)S(1)} %constant_dynamic-update-slice_fusion.5.near_ref), channel_id=1, source_target_pairs={{0,1},{1,0},{2,3},{3,2},{4,5},{5,4},{6,7},{7,6},{8,9},{9,8},{10,11... | collective-permute-start | bytes 786440 | tf_op jit(solution)/shard_map/ppermute | solution.py:31
  58.2 5.3 %collective-permute-start.8 = (bf16[64,2048]{1,0:T(8,128)(2,1)S(1)}, bf16[64,2048]{1,0:T(8,128)(2,1)S(1)}, u32[]{:S(2)}, u32[]{:S(2)}) collective-permute-start(bf16[64,2048]{1,0:T(8,128)(2,1)S(1)} %get-tuple-element.40), channel_id=1, source_target_pairs={{0,1},{1,0},{2,3},{3,2},{4,5},{5,4},{6,7},{7,6},{8,9},{9,8},{10,11... | collective-permute-start | bytes 786440 | tf_op jit(solution)/shard_map/ppermute | solution.py:31
  60.2 4.3 %collective-permute-start.21 = (bf16[64,2048]{1,0:T(8,128)(2,1)S(1)}, bf16[64,2048]{1,0:T(8,128)(2,1)S(1)}, u32[]{:S(2)}, u32[]{:S(2)}) collective-permute-start(bf16[64,2048]{1,0:T(8,128)(2,1)S(1)} %get-tuple-element.44), channel_id=1, source_target_pairs={{0,1},{1,0},{2,3},{3,2},{4,5},{5,4},{6,7},{7,6},{8,9},{9,8},{10,11... | collective-permute-start | bytes 786440 | tf_op jit(solution)/shard_map/ppermute | solution.py:31
  63.0 18.6 %copy-start.11 = (f32[32,2]{0,1:T(2,128)S(1)}, f32[32,2]{0,1:T(2,128)}, u32[]{:S(2)}) copy-start(f32[32,2]{0,1:T(2,128)} %param.24) | copy-start | bytes 772
  63.0 18.6 %copy-start.12 = (s32[32,2]{0,1:T(2,128)S(1)}, s32[32,2]{0,1:T(2,128)}, u32[]{:S(2)}) copy-start(s32[32,2]{0,1:T(2,128)} %param.23) | copy-start | bytes 772
  63.0 2.9 %collective-permute-start.14 = (bf16[128,2048]{1,0:T(8,128)(2,1)S(1)}, bf16[128,2048]{1,0:T(8,128)(2,1)S(1)}, u32[]{:S(2)}, u32[]{:S(2)}) collective-permute-start(bf16[128,2048]{1,0:T(8,128)(2,1)S(1)} %get-tuple-element.42), channel_id=1, source_target_pairs={{0,1},{1,0},{2,3},{3,2},{4,5},{5,4},{6,7},{7,6},{8,9},{9,8},{10,11... | collective-permute-start | bytes 1572872 | tf_op jit(solution)/shard_map/ppermute | solution.py:31
  63.6 17.9 %collective-permute-start.9 = (bf16[32,2048]{1,0:T(8,128)(2,1)S(1)}, bf16[32,2048]{1,0:T(8,128)(2,1)S(1)}, u32[]{:S(2)}, u32[]{:S(2)}) collective-permute-start(bf16[32,2048]{1,0:T(8,128)(2,1)S(1)} %slice.49), channel_id=1, source_target_pairs={{0,2},{1,3},{2,0},{3,1},{4,6},{5,7},{6,4},{7,5},{8,10},{9,11},{10,... | collective-permute-start | bytes 393224 | tf_op jit(solution)/shard_map/ppermute | solution.py:31
  64.6 8.2 %collective-permute-start.22 = (bf16[32,2048]{1,0:T(8,128)(2,1)S(1)}, bf16[32,2048]{1,0:T(8,128)(2,1)S(1)}, u32[]{:S(2)}, u32[]{:S(2)}) collective-permute-start(bf16[32,2048]{1,0:T(8,128)(2,1)S(1)} %slice.55), channel_id=1, source_target_pairs={{0,2},{1,3},{2,0},{3,1},{4,6},{5,7},{6,4},{7,5},{8,10},{9,11},{10,... | collective-permute-start | bytes 393224 | tf_op jit(solution)/shard_map/ppermute | solution.py:31
  66.0 11.5 %collective-permute-start.15 = (bf16[64,2048]{1,0:T(8,128)(2,1)S(1)}, bf16[64,2048]{1,0:T(8,128)(2,1)S(1)}, u32[]{:S(2)}, u32[]{:S(2)}) collective-permute-start(bf16[64,2048]{1,0:T(8,128)(2,1)S(1)} %slice.51), channel_id=1, source_target_pairs={{0,2},{1,3},{2,0},{3,1},{4,6},{5,7},{6,4},{7,5},{8,10},{9,11},{10,... | collective-permute-start | bytes 786440 | tf_op jit(solution)/shard_map/ppermute | solution.py:31
  72.9 8.7 %collective-permute-start.23 = (bf16[32,2048]{1,0:T(8,128)(2,1)S(1)}, bf16[32,2048]{1,0:T(8,128)(2,1)S(1)}, u32[]{:S(2)}, u32[]{:S(2)}) collective-permute-start(bf16[32,2048]{1,0:T(8,128)(2,1)S(1)} %add_convert_fusion.5), channel_id=1, source_target_pairs={{0,8},{4,12},{8,0},{12,4},{1,9},{5,13},{9,1},{13,5},{2,10},{6,14},... | collective-permute-start | bytes 393224 | tf_op jit(solution)/shard_map/ppermute | solution.py:26
  77.6 7.8 %collective-permute-start.17 = (bf16[32,2048]{1,0:T(8,128)(2,1)S(1)}, bf16[32,2048]{1,0:T(8,128)(2,1)S(1)}, u32[]{:S(2)}, u32[]{:S(2)}) collective-permute-start(bf16[32,2048]{1,0:T(8,128)(2,1)S(1)} %get-tuple-element.50), channel_id=1, source_target_pairs={{0,4},{4,8},{8,12},{12,0},{1,5},{5,9},{9,13},{13,1},{2,6},{6,10},{... | collective-permute-start | bytes 393224 | tf_op jit(solution)/shard_map/ppermute | solution.py:26
  80.2 6.6 %collective-permute-start.16 = (bf16[32,2048]{1,0:T(8,128)(2,1)S(1)}, bf16[32,2048]{1,0:T(8,128)(2,1)S(1)}, u32[]{:S(2)}, u32[]{:S(2)}) collective-permute-start(bf16[32,2048]{1,0:T(8,128)(2,1)S(1)} %get-tuple-element.49), channel_id=1, source_target_pairs={{0,12},{4,0},{8,4},{12,8},{1,13},{5,1},{9,5},{13,9},{2,14},{6,2},{... | collective-permute-start | bytes 393224 | tf_op jit(solution)/shard_map/ppermute | solution.py:26

commit v4 on v3

--- a/solution.py
+++ b/solution.py
@@ -86,7 +86,9 @@
         carry,
     )
     mix_ref[...] = mix
-    carry_ref[...] = jnp.broadcast_to(carry, carry_ref.shape)
+    lanes = [carry[at : at + rows] for at in range(0, carry.shape[0], rows)]
+    lanes.append(jnp.zeros((rows, DH - len(lanes)), jnp.float32))
+    carry_ref[...] = jnp.concatenate(lanes, axis=1)
 
 
 def away_kernel(count, order, place_ref, q_ref, bias_ref, col_ref, mix_ref, carry_ref, w_ref, *refs):
@@ -94,7 +96,8 @@
     rows = q_ref.shape[0]
     width = q_ref.shape[1] // (HEADS // KV_HEADS)
     mix = mix_ref[...]
-    carry = carry_ref[:, 0:1]
+    heads = q_ref.shape[1] // DH
+    carry = jnp.concatenate([carry_ref[:, h : h + 1] for h in range(heads)], axis=0)
     for step, block in enumerate(sent, 1):
         doc_row = block[rows : rows + 1, 0:rows].astype(jnp.float32)
         doc_row = jnp.where(place_ref[0] >= step, doc_row, -1.0)
@@ -166,12 +169,11 @@
     sent = [shifted(packed, steps, False) for steps in range(1, sp_count)]
     col = documents.astype(jnp.float32).reshape(rows, 1)
     row = documents.astype(jnp.float32).reshape(1, rows)
-    heads = width // DH
     mix, carry = pl.pallas_call(
         here_kernel,
         out_shape=(
             jax.ShapeDtypeStruct((rows, width), jnp.float32),
-            jax.ShapeDtypeStruct((rows * heads, DH), jnp.float32),
+            jax.ShapeDtypeStruct((rows, DH), jnp.float32),
         ),
         in_specs=[VMEM, VMEM, VMEM, SMEM, VMEM, VMEM],
         out_specs=(VMEM, VMEM),

time: 88 us -> 87.9 us (level)
  no operation moved by 1% of the time
where the time goes in v4:
time: 87.9 us; the launch traced here: 87.6 us
  waiting for transfers between devices  35.4 us (40%)
  starting transfers between devices  33.7 us (38%)
  Pallas kernels  12 us (14%)
  other arithmetic  3.49 us (4%)
  local copies, waits for them, and re-layouts  2.71 us (3%)
    ppermute x9, starting transfers between devices, shifted(): return lax.ppermute(value, 'sp', pairs)  24.4 us
    ppermute x15, waiting for transfers between devices, swapped(): return lax.ppermute(value, 'tp', [(i, i ^ mask) for i in range(count)])  22.1 us
    ppermute x9, waiting for transfers between devices, shifted(): return lax.ppermute(value, 'sp', pairs)  13.3 us
    ppermute x15, starting transfers between devices, swapped(): return lax.ppermute(value, 'tp', [(i, i ^ mask) for i in range(count)])  9.29 us
    pallas_call x3, Pallas kernels, experts_dense(): pl.pallas_call(expert_kernel, out_shape=[jax.ShapeDtypeStruct((count, D),...  5.54 us
    pallas_call x1, Pallas kernels, middle_direct(): pl.pallas_call(functools.partial(away_kernel, sp_count - 1, order), out_s...  3.76 us
    pallas_call x1, Pallas kernels, middle_direct(): pl.pallas_call(here_kernel, out_shape=(jax.ShapeDtypeStruct((rows, width)...  2.51 us
    unnamed x30, local copies, waits for them, and re-layouts  1.87 us
  transfers between devices with their start and end apart: 24, of which 11 were waited for; matrix products, arithmetic and copies ran while one was open for 2% of the time, Pallas kernels for 9%

profile of v4, /device:TPU:0, one launch (start us, length us, event | category | flops | bytes accessed | tf_op | source)
XLA Modules:
  0.0 87.6 jit_solution(10192088282087542890)
XLA Ops:
  0.0 1.3 %convert_bitcast_fusion = (bf16[1,128]{1,0:T(2,128)(2,1)S(1)}, f32[1,128]{1,0:T(1,128)}, f32[128,1]{0,1:T(1,128)S(1)}) fusion(s32[128]{0:T(128)} %param.19), kind=kLoop, calls=%fused_computation.27 | loop fusion | flops 256 | bytes 1792 | tf_op jit(solution)/shard_map/reshape.30
  1.3 0.9 %fusion.1 = bf16[136,512]{1,0:T(8,128)(2,1)S(1)} fusion(bf16[1,128]{1,0:T(2,128)(2,1)S(1)} %get-tuple-element.51, bf16[128,256]{1,0:T(8,128)(2,1)} %v_ref.1, bf16[128,256]{1,0:T(8,128)(2,1)} %k_ref.1), kind=kLoop, calls=%fused_computation.10 | loop fusion | flops 557056 | bytes 270592 | tf_op jit(solution)/shard_map/concatenate | solution.py:168
  2.2 5.0 %collective-permute-start = (bf16[136,512]{1,0:T(8,128)(2,1)S(1)}, bf16[136,512]{1,0:T(8,128)(2,1)S(1)}, u32[]{:S(2)}, u32[]{:S(2)}) collective-permute-start(bf16[136,512]{1,0:T(8,128)(2,1)S(1)} %fusion.1), channel_id=1, source_target_pairs={{0,4},{4,8},{8,12},{1,5},{5,9},{9,13},{2,6},{6,10},{10,14},{3,7},{... | collective-permute-start | bytes 417800 | tf_op jit(solution)/shard_map/ppermute | solution.py:26
  7.2 4.5 %collective-permute-start.1 = (bf16[136,512]{1,0:T(8,128)(2,1)S(1)}, bf16[136,512]{1,0:T(8,128)(2,1)S(1)}, u32[]{:S(2)}, u32[]{:S(2)}) collective-permute-start(bf16[136,512]{1,0:T(8,128)(2,1)S(1)} %fusion.1), channel_id=1, source_target_pairs={{0,8},{4,12},{1,9},{5,13},{2,10},{6,14},{3,11},{7,15},{16,24},{20,... | collective-permute-start | bytes 417800 | tf_op jit(solution)/shard_map/ppermute | solution.py:26
  11.7 1.3 %collective-permute-start.2 = (bf16[136,512]{1,0:T(8,128)(2,1)S(1)}, bf16[136,512]{1,0:T(8,128)(2,1)S(1)}, u32[]{:S(2)}, u32[]{:S(2)}) collective-permute-start(bf16[136,512]{1,0:T(8,128)(2,1)S(1)} %fusion.1), channel_id=1, source_target_pairs={{0,12},{1,13},{2,14},{3,15},{16,28},{17,29},{18,30},{19,31}} | collective-permute-start | bytes 417800 | tf_op jit(solution)/shard_map/ppermute | solution.py:26
  13.0 0.7 copy.15.col_ref
  13.7 2.5 %attend_here.1 = (f32[128,512]{1,0:T(8,128)}, f32[128,128]{1,0:T(8,128)}) custom-call(bf16[128,512]{1,0:T(8,128)(2,1)} %q_ref.3, bf16[128,256]{1,0:T(8,128)(2,1)} %k_ref.1, bf16[128,256]{1,0:T(8,128)(2,1)} %v_ref.1, f32[4]{0:T(128)} %bias_ref.3, f32[128,1]{1,0:T(8,128)} %copy.15.col_ref, f32[1,128]{1,0:T(1,128)} %get-tuple-element.52.row_ref), custom_call_target="tpu_custom_call" | custom-call | flops 6000000000 | bytes 1000000 | tf_op jit(solution)/shard_map/attend_here/pallas_call | solution.py:172
  16.2 0.1 pad_add_fusion.place_ref
  16.3 1.0 %collective-permute-done.2.refs_2_ = bf16[136,512]{1,0:T(8,128)(2,1)S(1)} collective-permute-done((bf16[136,512]{1,0:T(8,128)(2,1)S(1)}, bf16[136,512]{1,0:T(8,128)(2,1)S(1)}, u32[]{:S(2)}, u32[]{:S(2)}) %collective-permute-start.2) | collective-permute-done | bytes 139296 | tf_op jit(solution)/shard_map/ppermute | solution.py:26
  17.3 0.9 %copy-done.9 = f32[128,512]{1,0:T(8,128)S(1)} copy-done((f32[128,512]{1,0:T(8,128)S(1)}, f32[128,512]{1,0:T(8,128)}, u32[]{:S(2)}) %copy-start.9) | copy-done | bytes 262168
  18.3 0.8 copy-done.10
  19.1 3.8 %attend_away.1 = (bf16[32,2048]{1,0:T(8,128)(2,1)S(1)}, bf16[32,2048]{1,0:T(8,128)(2,1)S(1)}, bf16[32,2048]{1,0:T(8,128)(2,1)S(1)}, bf16[32,2048]{1,0:T(8,128)(2,1)S(1)}) custom-call(s32[2]{0:T(128)S(1)} %pad_add_fusion.place_ref, bf16[128,512]{1,0:T(8,128)(2,1)S(1)} %copy-done.7, f32[4]{0:T(128)S(1)} %copy-done.8, f32[128,1]{1,0:T(8,128)S(1)} %copy-done.4, ...), custom_call_target="tpu_custom_call" | custom-call | flops 10000000000 | bytes 4000000 | tf_op jit(solution)/shard_map/attend_away/pallas_call | solution.py:186
  22.9 0.1 collective-permute-start.3
  23.0 1.6 %collective-permute-start.4 = (bf16[32,2048]{1,0:T(8,128)(2,1)S(1)}, bf16[32,2048]{1,0:T(8,128)(2,1)S(1)}, u32[]{:S(2)}, u32[]{:S(2)}) collective-permute-start(bf16[32,2048]{1,0:T(8,128)(2,1)S(1)} %get-tuple-element.35), channel_id=1, source_target_pairs={{0,2},{1,3},{2,0},{3,1},{4,6},{5,7},{6,4},{7,5},{8,10},{9,11},{10,... | collective-permute-start | bytes 393224 | tf_op jit(solution)/shard_map/ppermute | solution.py:31
  24.6 0.3 collective-permute-start.5
  24.8 3.9 %collective-permute-done.3.refs_1_ = bf16[32,2048]{1,0:T(8,128)(2,1)S(1)} collective-permute-done((bf16[32,2048]{1,0:T(8,128)(2,1)S(1)}, bf16[32,2048]{1,0:T(8,128)(2,1)S(1)}, u32[]{:S(2)}, u32[]{:S(2)}) %collective-permute-start.3) | collective-permute-done | bytes 131104 | tf_op jit(solution)/shard_map/ppermute | solution.py:31
  28.7 2.9 %collective-permute-done.4.refs_2_ = bf16[32,2048]{1,0:T(8,128)(2,1)S(1)} collective-permute-done((bf16[32,2048]{1,0:T(8,128)(2,1)S(1)}, bf16[32,2048]{1,0:T(8,128)(2,1)S(1)}, u32[]{:S(2)}, u32[]{:S(2)}) %collective-permute-start.4) | collective-permute-done | bytes 131104 | tf_op jit(solution)/shard_map/ppermute | solution.py:31
  31.6 0.2 middle_norm.1
  31.8 1.9 %collective-permute-start.18 = (bf16[32,2048]{1,0:T(8,128)(2,1)S(1)}, bf16[32,2048]{1,0:T(8,128)(2,1)S(1)}, u32[]{:S(2)}, u32[]{:S(2)}) collective-permute-start(bf16[32,2048]{1,0:T(8,128)(2,1)S(1)} %get-tuple-element.38), channel_id=1, source_target_pairs={{0,8},{4,12},{8,0},{12,4},{1,9},{5,13},{9,1},{13,5},{2,10},{6,14},... | collective-permute-start | bytes 393224 | tf_op jit(solution)/shard_map/ppermute | solution.py:26
  33.7 4.8 %collective-permute-start.10 = (bf16[32,2048]{1,0:T(8,128)(2,1)S(1)}, bf16[32,2048]{1,0:T(8,128)(2,1)S(1)}, u32[]{:S(2)}, u32[]{:S(2)}) collective-permute-start(bf16[32,2048]{1,0:T(8,128)(2,1)S(1)} %get-tuple-element.38), channel_id=1, source_target_pairs={{0,4},{4,8},{8,12},{12,0},{1,5},{5,9},{9,13},{13,1},{2,6},{6,10},{... | collective-permute-start | bytes 393224 | tf_op jit(solution)/shard_map/ppermute | solution.py:26
  38.6 0.7 collective-permute-start.6
  39.3 5.9 %collective-permute-done.10 = bf16[32,2048]{1,0:T(8,128)(2,1)S(1)} collective-permute-done((bf16[32,2048]{1,0:T(8,128)(2,1)S(1)}, bf16[32,2048]{1,0:T(8,128)(2,1)S(1)}, u32[]{:S(2)}, u32[]{:S(2)}) %collective-permute-start.10) | collective-permute-done | bytes 131104 | tf_op jit(solution)/shard_map/ppermute | solution.py:26
  45.2 1.1 %collective-permute-done.11 = bf16[32,2048]{1,0:T(8,128)(2,1)S(1)} collective-permute-done((bf16[32,2048]{1,0:T(8,128)(2,1)S(1)}, bf16[32,2048]{1,0:T(8,128)(2,1)S(1)}, u32[]{:S(2)}, u32[]{:S(2)}) %collective-permute-start.11) | collective-permute-done | bytes 131104 | tf_op jit(solution)/shard_map/ppermute | solution.py:26
  46.3 0.9 %collective-permute-start.12 = (bf16[64,2048]{1,0:T(8,128)(2,1)S(1)}, bf16[64,2048]{1,0:T(8,128)(2,1)S(1)}, u32[]{:S(2)}, u32[]{:S(2)}) collective-permute-start(bf16[64,2048]{1,0:T(8,128)(2,1)S(1)} %pad_maximum_fusion), channel_id=1, source_target_pairs={{0,2},{1,3},{2,0},{3,1},{4,6},{5,7},{6,4},{7,5},{8,10},{9,11},{10,... | collective-permute-start | bytes 786440 | tf_op jit(solution)/shard_map/ppermute | solution.py:31
  47.2 0.1 collective-permute-start.7
  47.3 1.2 %collective-permute-start.19 = (bf16[32,2048]{1,0:T(8,128)(2,1)S(1)}, bf16[32,2048]{1,0:T(8,128)(2,1)S(1)}, u32[]{:S(2)}, u32[]{:S(2)}) collective-permute-start(bf16[32,2048]{1,0:T(8,128)(2,1)S(1)} %collective-permute-done.18), channel_id=1, source_target_pairs={{0,2},{1,3},{2,0},{3,1},{4,6},{5,7},{6,4},{7,5},{8,10},{9,11},{10,... | collective-permute-start | bytes 393224 | tf_op jit(solution)/shard_map/ppermute | solution.py:31
  48.6 6.5 %collective-permute-done.12 = bf16[64,2048]{1,0:T(8,128)(2,1)S(1)} collective-permute-done((bf16[64,2048]{1,0:T(8,128)(2,1)S(1)}, bf16[64,2048]{1,0:T(8,128)(2,1)S(1)}, u32[]{:S(2)}, u32[]{:S(2)}) %collective-permute-start.12) | collective-permute-done | bytes 262176 | tf_op jit(solution)/shard_map/ppermute | solution.py:31
  55.1 0.1 collective-permute-start.13
  55.2 1.3 %collective-permute-done.19 = bf16[32,2048]{1,0:T(8,128)(2,1)S(1)} collective-permute-done((bf16[32,2048]{1,0:T(8,128)(2,1)S(1)}, bf16[32,2048]{1,0:T(8,128)(2,1)S(1)}, u32[]{:S(2)}, u32[]{:S(2)}) %collective-permute-start.19) | collective-permute-done | bytes 131104 | tf_op jit(solution)/shard_map/ppermute | solution.py:31
  56.5 0.1 collective-permute-start.20
  56.6 1.5 %shard_map.127 = (bf16[64,2048]{1,0:T(8,128)(2,1)S(1)}, bf16[64,2048]{1,0:T(8,128)(2,1)S(1)}) custom-call(bf16[64,2048]{1,0:T(8,128)(2,1)S(1)} %constant_dynamic-update-slice_fusion.near_ref, bf16[64,2048]{1,0:T(8,128)(2,1)S(1)} %collective-permute-done.7.far_ref, bf16[1,2048,768]{2,1,0:T(8,128)(2,1)S(1)} %copy-done, bf16[1,2048,768]{2,1,0:T(8,128)(2,1)S(1)} %copy-done.1, ...), custom_call_target="tpu_custom_call" | custom-call | flops 1207959552 | bytes 12000000 | tf_op jit(solution)/shard_map/pallas_call | solution.py:228
  58.1 0.5 collective-permute-start.8
  58.6 1.5 %shard_map.129 = (bf16[64,2048]{1,0:T(8,128)(2,1)S(1)}, bf16[64,2048]{1,0:T(8,128)(2,1)S(1)}) custom-call(bf16[64,2048]{1,0:T(8,128)(2,1)S(1)} %constant_dynamic-update-slice_fusion.5.near_ref, bf16[64,2048]{1,0:T(8,128)(2,1)S(1)} %collective-permute-done.20.far_ref, bf16[1,2048,768]{2,1,0:T(8,128)(2,1)S(1)} %copy-done, bf16[1,2048,768]{2,1,0:T(8,128)(2,1)S(1)} %copy-done.1, ...), custom_call_target="tpu_custom_call" | custom-call | flops 1207959552 | bytes 12000000 | tf_op jit(solution)/shard_map/pallas_call | solution.py:228
  60.1 0.1 collective-permute-start.21
  60.2 2.6 %shard_map.128 = (bf16[128,2048]{1,0:T(8,128)(2,1)S(1)}, bf16[128,2048]{1,0:T(8,128)(2,1)S(1)}) custom-call(bf16[128,2048]{1,0:T(8,128)(2,1)S(1)} %constant_dynamic-update-slice_fusion.2.near_ref, bf16[128,2048]{1,0:T(8,128)(2,1)S(1)} %collective-permute-done.13.far_ref, bf16[1,2048,768]{2,1,0:T(8,128)(2,1)S(1)} %copy-done, ...), custom_call_target="tpu_custom_call" | custom-call | flops 2415919104 | bytes 12000000 | tf_op jit(solution)/shard_map/pallas_call | solution.py:228
  62.8 0.5 collective-permute-start.14
  63.5 0.9 %collective-permute-start.9 = (bf16[32,2048]{1,0:T(8,128)(2,1)S(1)}, bf16[32,2048]{1,0:T(8,128)(2,1)S(1)}, u32[]{:S(2)}, u32[]{:S(2)}) collective-permute-start(bf16[32,2048]{1,0:T(8,128)(2,1)S(1)} %slice.49), channel_id=1, source_target_pairs={{0,2},{1,3},{2,0},{3,1},{4,6},{5,7},{6,4},{7,5},{8,10},{9,11},{10,... | collective-permute-start | bytes 393224 | tf_op jit(solution)/shard_map/ppermute | solution.py:31
  64.5 1.2 %collective-permute-start.22 = (bf16[32,2048]{1,0:T(8,128)(2,1)S(1)}, bf16[32,2048]{1,0:T(8,128)(2,1)S(1)}, u32[]{:S(2)}, u32[]{:S(2)}) collective-permute-start(bf16[32,2048]{1,0:T(8,128)(2,1)S(1)} %slice.55), channel_id=1, source_target_pairs={{0,2},{1,3},{2,0},{3,1},{4,6},{5,7},{6,4},{7,5},{8,10},{9,11},{10,... | collective-permute-start | bytes 393224 | tf_op jit(solution)/shard_map/ppermute | solution.py:31
  65.7 0.1 add_convert_fusion
  65.9 0.9 %collective-permute-start.15 = (bf16[64,2048]{1,0:T(8,128)(2,1)S(1)}, bf16[64,2048]{1,0:T(8,128)(2,1)S(1)}, u32[]{:S(2)}, u32[]{:S(2)}) collective-permute-start(bf16[64,2048]{1,0:T(8,128)(2,1)S(1)} %slice.51), channel_id=1, source_target_pairs={{0,2},{1,3},{2,0},{3,1},{4,6},{5,7},{6,4},{7,5},{8,10},{9,11},{10,... | collective-permute-start | bytes 786440 | tf_op jit(solution)/shard_map/ppermute | solution.py:31
  66.8 5.9 %collective-permute-done.22 = bf16[32,2048]{1,0:T(8,128)(2,1)S(1)} collective-permute-done((bf16[32,2048]{1,0:T(8,128)(2,1)S(1)}, bf16[32,2048]{1,0:T(8,128)(2,1)S(1)}, u32[]{:S(2)}, u32[]{:S(2)}) %collective-permute-start.22) | collective-permute-done | bytes 131104 | tf_op jit(solution)/shard_map/ppermute | solution.py:31
  72.8 3.0 %collective-permute-start.23 = (bf16[32,2048]{1,0:T(8,128)(2,1)S(1)}, bf16[32,2048]{1,0:T(8,128)(2,1)S(1)}, u32[]{:S(2)}, u32[]{:S(2)}) collective-permute-start(bf16[32,2048]{1,0:T(8,128)(2,1)S(1)} %add_convert_fusion.5), channel_id=1, source_target_pairs={{0,8},{4,12},{8,0},{12,4},{1,9},{5,13},{9,1},{13,5},{2,10},{6,14},... | collective-permute-start | bytes 393224 | tf_op jit(solution)/shard_map/ppermute | solution.py:26
  75.8 1.6 %collective-permute-done.15 = bf16[64,2048]{1,0:T(8,128)(2,1)S(1)} collective-permute-done((bf16[64,2048]{1,0:T(8,128)(2,1)S(1)}, bf16[64,2048]{1,0:T(8,128)(2,1)S(1)}, u32[]{:S(2)}, u32[]{:S(2)}) %collective-permute-start.15) | collective-permute-done | bytes 262176 | tf_op jit(solution)/shard_map/ppermute | solution.py:31
  77.5 2.6 %collective-permute-start.17 = (bf16[32,2048]{1,0:T(8,128)(2,1)S(1)}, bf16[32,2048]{1,0:T(8,128)(2,1)S(1)}, u32[]{:S(2)}, u32[]{:S(2)}) collective-permute-start(bf16[32,2048]{1,0:T(8,128)(2,1)S(1)} %get-tuple-element.50), channel_id=1, source_target_pairs={{0,4},{4,8},{8,12},{12,0},{1,5},{5,9},{9,13},{13,1},{2,6},{6,10},{... | collective-permute-start | bytes 393224 | tf_op jit(solution)/shard_map/ppermute | solution.py:26
  80.1 1.3 %collective-permute-start.16 = (bf16[32,2048]{1,0:T(8,128)(2,1)S(1)}, bf16[32,2048]{1,0:T(8,128)(2,1)S(1)}, u32[]{:S(2)}, u32[]{:S(2)}) collective-permute-start(bf16[32,2048]{1,0:T(8,128)(2,1)S(1)} %get-tuple-element.49), channel_id=1, source_target_pairs={{0,12},{4,0},{8,4},{12,8},{1,13},{5,1},{9,5},{13,9},{2,14},{6,2},{... | collective-permute-start | bytes 393224 | tf_op jit(solution)/shard_map/ppermute | solution.py:26
  81.4 3.9 %collective-permute-done.17 = bf16[32,2048]{1,0:T(8,128)(2,1)S(1)} collective-permute-done((bf16[32,2048]{1,0:T(8,128)(2,1)S(1)}, bf16[32,2048]{1,0:T(8,128)(2,1)S(1)}, u32[]{:S(2)}, u32[]{:S(2)}) %collective-permute-start.17) | collective-permute-done | bytes 131104 | tf_op jit(solution)/shard_map/ppermute | solution.py:26
  85.3 1.4 %collective-permute-done.16 = bf16[32,2048]{1,0:T(8,128)(2,1)S(1)} collective-permute-done((bf16[32,2048]{1,0:T(8,128)(2,1)S(1)}, bf16[32,2048]{1,0:T(8,128)(2,1)S(1)}, u32[]{:S(2)}, u32[]{:S(2)}) %collective-permute-start.16) | collective-permute-done | bytes 131104 | tf_op jit(solution)/shard_map/ppermute | solution.py:26
  86.7 0.8 add_convert_fusion.4
  (55 shorter events, 0.5 us)
Async XLA Ops:
  2.2 14.1 %collective-permute-start = (bf16[136,512]{1,0:T(8,128)(2,1)S(1)}, bf16[136,512]{1,0:T(8,128)(2,1)S(1)}, u32[]{:S(2)}, u32[]{:S(2)}) collective-permute-start(bf16[136,512]{1,0:T(8,128)(2,1)S(1)} %fusion.1), channel_id=1, source_target_pairs={{0,4},{4,8},{8,12},{1,5},{5,9},{9,13},{2,6},{6,10},{10,14},{3,7},{... | collective-permute-start | bytes 417800 | tf_op jit(solution)/shard_map/ppermute | solution.py:26
  7.2 9.2 %collective-permute-start.1 = (bf16[136,512]{1,0:T(8,128)(2,1)S(1)}, bf16[136,512]{1,0:T(8,128)(2,1)S(1)}, u32[]{:S(2)}, u32[]{:S(2)}) collective-permute-start(bf16[136,512]{1,0:T(8,128)(2,1)S(1)} %fusion.1), channel_id=1, source_target_pairs={{0,8},{4,12},{1,9},{5,13},{2,10},{6,14},{3,11},{7,15},{16,24},{20,... | collective-permute-start | bytes 417800 | tf_op jit(solution)/shard_map/ppermute | solution.py:26
  11.7 5.7 %collective-permute-start.2 = (bf16[136,512]{1,0:T(8,128)(2,1)S(1)}, bf16[136,512]{1,0:T(8,128)(2,1)S(1)}, u32[]{:S(2)}, u32[]{:S(2)}) collective-permute-start(bf16[136,512]{1,0:T(8,128)(2,1)S(1)} %fusion.1), channel_id=1, source_target_pairs={{0,12},{1,13},{2,14},{3,15},{16,28},{17,29},{18,30},{19,31}} | collective-permute-start | bytes 417800 | tf_op jit(solution)/shard_map/ppermute | solution.py:26
  13.7 3.6 %copy-start.4 = (f32[128,1]{1,0:T(8,128)S(1)}, f32[128,1]{1,0:T(8,128)}, u32[]{:S(2)}) copy-start(f32[128,1]{1,0:T(8,128)} %copy.15.col_ref) | copy-start | bytes 1540
  13.7 3.6 %copy-start.6 = (bf16[512,2048]{1,0:T(8,128)(2,1)S(1)}, bf16[512,2048]{1,0:T(8,128)(2,1)}, u32[]{:S(2)}) copy-start(bf16[512,2048]{1,0:T(8,128)(2,1)} %w_ref.1) | copy-start | bytes 6291460
  13.7 3.6 %copy-start.7 = (bf16[128,512]{1,0:T(8,128)(2,1)S(1)}, bf16[128,512]{1,0:T(8,128)(2,1)}, u32[]{:S(2)}) copy-start(bf16[128,512]{1,0:T(8,128)(2,1)} %q_ref.3) | copy-start | bytes 393220
  13.7 3.6 %copy-start.8 = (f32[4]{0:T(128)S(1)}, f32[4]{0:T(128)}, u32[]{:S(2)}) copy-start(f32[4]{0:T(128)} %bias_ref.3) | copy-start | bytes 52
  17.3 1.0 %copy-start.9 = (f32[128,512]{1,0:T(8,128)S(1)}, f32[128,512]{1,0:T(8,128)}, u32[]{:S(2)}) copy-start(f32[128,512]{1,0:T(8,128)} %get-tuple-element.31.mix_ref) | copy-start | bytes 786436
  18.3 0.8 copy-start.10
  19.1 12.5 %copy-start.3 = (bf16[32,2048]{1,0:T(8,128)(2,1)S(1)}, bf16[32,2048]{1,0:T(8,128)(2,1)}, u32[]{:S(2)}) copy-start(bf16[32,2048]{1,0:T(8,128)(2,1)} %resid_ref.1) | copy-start | bytes 393220
  19.1 12.5 %copy-start.5 = (f32[2048]{0:T(1024)S(1)}, f32[2048]{0:T(1024)}, u32[]{:S(2)}) copy-start(f32[2048]{0:T(1024)} %param.22) | copy-start | bytes 24580
  19.1 37.5 %copy-start.1 = (bf16[1,2048,768]{2,1,0:T(8,128)(2,1)S(1)}, bf16[1,2048,768]{2,1,0:T(8,128)(2,1)}, u32[]{:S(2)}) copy-start(bf16[1,2048,768]{2,1,0:T(8,128)(2,1)} %up_ref.5) | copy-start | bytes 9437188
  19.1 37.5 %copy-start.2 = (bf16[1,768,2048]{2,1,0:T(8,128)(2,1)S(1)}, bf16[1,768,2048]{2,1,0:T(8,128)(2,1)}, u32[]{:S(2)}) copy-start(bf16[1,768,2048]{2,1,0:T(8,128)(2,1)} %down_ref.5) | copy-start | bytes 9437188
  22.9 33.7 %copy-start = (bf16[1,2048,768]{2,1,0:T(8,128)(2,1)S(1)}, bf16[1,2048,768]{2,1,0:T(8,128)(2,1)}, u32[]{:S(2)}) copy-start(bf16[1,2048,768]{2,1,0:T(8,128)(2,1)} %gate_ref.5) | copy-start | bytes 9437188
  22.9 5.8 %collective-permute-start.3 = (bf16[32,2048]{1,0:T(8,128)(2,1)S(1)}, bf16[32,2048]{1,0:T(8,128)(2,1)S(1)}, u32[]{:S(2)}, u32[]{:S(2)}) collective-permute-start(bf16[32,2048]{1,0:T(8,128)(2,1)S(1)} %get-tuple-element.34), channel_id=1, source_target_pairs={{0,3},{1,2},{2,1},{3,0},{4,7},{5,6},{6,5},{7,4},{8,11},{9,10},{10,... | collective-permute-start | bytes 393224 | tf_op jit(solution)/shard_map/ppermute | solution.py:31
  23.0 8.6 %collective-permute-start.4 = (bf16[32,2048]{1,0:T(8,128)(2,1)S(1)}, bf16[32,2048]{1,0:T(8,128)(2,1)S(1)}, u32[]{:S(2)}, u32[]{:S(2)}) collective-permute-start(bf16[32,2048]{1,0:T(8,128)(2,1)S(1)} %get-tuple-element.35), channel_id=1, source_target_pairs={{0,2},{1,3},{2,0},{3,1},{4,6},{5,7},{6,4},{7,5},{8,10},{9,11},{10,... | collective-permute-start | bytes 393224 | tf_op jit(solution)/shard_map/ppermute | solution.py:31
  24.6 7.0 %collective-permute-start.5 = (bf16[32,2048]{1,0:T(8,128)(2,1)S(1)}, bf16[32,2048]{1,0:T(8,128)(2,1)S(1)}, u32[]{:S(2)}, u32[]{:S(2)}) collective-permute-start(bf16[32,2048]{1,0:T(8,128)(2,1)S(1)} %get-tuple-element.36), channel_id=1, source_target_pairs={{0,1},{1,0},{2,3},{3,2},{4,5},{5,4},{6,7},{7,6},{8,9},{9,8},{10,11... | collective-permute-start | bytes 393224 | tf_op jit(solution)/shard_map/ppermute | solution.py:31
  31.8 15.5 %collective-permute-start.18 = (bf16[32,2048]{1,0:T(8,128)(2,1)S(1)}, bf16[32,2048]{1,0:T(8,128)(2,1)S(1)}, u32[]{:S(2)}, u32[]{:S(2)}) collective-permute-start(bf16[32,2048]{1,0:T(8,128)(2,1)S(1)} %get-tuple-element.38), channel_id=1, source_target_pairs={{0,8},{4,12},{8,0},{12,4},{1,9},{5,13},{9,1},{13,5},{2,10},{6,14},... | collective-permute-start | bytes 393224 | tf_op jit(solution)/shard_map/ppermute | solution.py:26
  33.7 11.5 %collective-permute-start.10 = (bf16[32,2048]{1,0:T(8,128)(2,1)S(1)}, bf16[32,2048]{1,0:T(8,128)(2,1)S(1)}, u32[]{:S(2)}, u32[]{:S(2)}) collective-permute-start(bf16[32,2048]{1,0:T(8,128)(2,1)S(1)} %get-tuple-element.38), channel_id=1, source_target_pairs={{0,4},{4,8},{8,12},{12,0},{1,5},{5,9},{9,13},{13,1},{2,6},{6,10},{... | collective-permute-start | bytes 393224 | tf_op jit(solution)/shard_map/ppermute | solution.py:26
  38.6 7.7 %collective-permute-start.11 = (bf16[32,2048]{1,0:T(8,128)(2,1)S(1)}, bf16[32,2048]{1,0:T(8,128)(2,1)S(1)}, u32[]{:S(2)}, u32[]{:S(2)}) collective-permute-start(bf16[32,2048]{1,0:T(8,128)(2,1)S(1)} %get-tuple-element.38), channel_id=1, source_target_pairs={{0,12},{4,0},{8,4},{12,8},{1,13},{5,1},{9,5},{13,9},{2,14},{6,2},{... | collective-permute-start | bytes 393224 | tf_op jit(solution)/shard_map/ppermute | solution.py:26
  38.6 8.7 %collective-permute-start.6 = (bf16[32,2048]{1,0:T(8,128)(2,1)S(1)}, bf16[32,2048]{1,0:T(8,128)(2,1)S(1)}, u32[]{:S(2)}, u32[]{:S(2)}) collective-permute-start(bf16[32,2048]{1,0:T(8,128)(2,1)S(1)} %get-tuple-element.38), channel_id=1, source_target_pairs={{0,2},{1,3},{2,0},{3,1},{4,6},{5,7},{6,4},{7,5},{8,10},{9,11},{10,... | collective-permute-start | bytes 393224 | tf_op jit(solution)/shard_map/ppermute | solution.py:31
  46.3 8.8 %collective-permute-start.12 = (bf16[64,2048]{1,0:T(8,128)(2,1)S(1)}, bf16[64,2048]{1,0:T(8,128)(2,1)S(1)}, u32[]{:S(2)}, u32[]{:S(2)}) collective-permute-start(bf16[64,2048]{1,0:T(8,128)(2,1)S(1)} %pad_maximum_fusion), channel_id=1, source_target_pairs={{0,2},{1,3},{2,0},{3,1},{4,6},{5,7},{6,4},{7,5},{8,10},{9,11},{10,... | collective-permute-start | bytes 786440 | tf_op jit(solution)/shard_map/ppermute | solution.py:31
  47.2 9.3 %collective-permute-start.7 = (bf16[64,2048]{1,0:T(8,128)(2,1)S(1)}, bf16[64,2048]{1,0:T(8,128)(2,1)S(1)}, u32[]{:S(2)}, u32[]{:S(2)}) collective-permute-start(bf16[64,2048]{1,0:T(8,128)(2,1)S(1)} %constant_dynamic-update-slice_fusion.near_ref), channel_id=1, source_target_pairs={{0,1},{1,0},{2,3},{3,2},{4,5},{5,4},{6,7},{7,6},{8,9},{9,8},{10,11... | collective-permute-start | bytes 786440 | tf_op jit(solution)/shard_map/ppermute | solution.py:31
  47.3 9.1 %collective-permute-start.19 = (bf16[32,2048]{1,0:T(8,128)(2,1)S(1)}, bf16[32,2048]{1,0:T(8,128)(2,1)S(1)}, u32[]{:S(2)}, u32[]{:S(2)}) collective-permute-start(bf16[32,2048]{1,0:T(8,128)(2,1)S(1)} %collective-permute-done.18), channel_id=1, source_target_pairs={{0,2},{1,3},{2,0},{3,1},{4,6},{5,7},{6,4},{7,5},{8,10},{9,11},{10,... | collective-permute-start | bytes 393224 | tf_op jit(solution)/shard_map/ppermute | solution.py:31
  55.1 5.1 %collective-permute-start.13 = (bf16[128,2048]{1,0:T(8,128)(2,1)S(1)}, bf16[128,2048]{1,0:T(8,128)(2,1)S(1)}, u32[]{:S(2)}, u32[]{:S(2)}) collective-permute-start(bf16[128,2048]{1,0:T(8,128)(2,1)S(1)} %constant_dynamic-update-slice_fusion.2.near_ref), channel_id=1, source_target_pairs={{0,1},{1,0},{2,3},{3,2},{4,5},{5,4},{6,7},{7,6},{8,9},{9,8},{10,11... | collective-permute-start | bytes 1572872 | tf_op jit(solution)/shard_map/ppermute | solution.py:31
  56.5 2.1 %collective-permute-start.20 = (bf16[64,2048]{1,0:T(8,128)(2,1)S(1)}, bf16[64,2048]{1,0:T(8,128)(2,1)S(1)}, u32[]{:S(2)}, u32[]{:S(2)}) collective-permute-start(bf16[64,2048]{1,0:T(8,128)(2,1)S(1)} %constant_dynamic-update-slice_fusion.5.near_ref), channel_id=1, source_target_pairs={{0,1},{1,0},{2,3},{3,2},{4,5},{5,4},{6,7},{7,6},{8,9},{9,8},{10,11... | collective-permute-start | bytes 786440 | tf_op jit(solution)/shard_map/ppermute | solution.py:31
  58.1 5.3 %collective-permute-start.8 = (bf16[64,2048]{1,0:T(8,128)(2,1)S(1)}, bf16[64,2048]{1,0:T(8,128)(2,1)S(1)}, u32[]{:S(2)}, u32[]{:S(2)}) collective-permute-start(bf16[64,2048]{1,0:T(8,128)(2,1)S(1)} %get-tuple-element.40), channel_id=1, source_target_pairs={{0,1},{1,0},{2,3},{3,2},{4,5},{5,4},{6,7},{7,6},{8,9},{9,8},{10,11... | collective-permute-start | bytes 786440 | tf_op jit(solution)/shard_map/ppermute | solution.py:31
  60.1 4.3 %collective-permute-start.21 = (bf16[64,2048]{1,0:T(8,128)(2,1)S(1)}, bf16[64,2048]{1,0:T(8,128)(2,1)S(1)}, u32[]{:S(2)}, u32[]{:S(2)}) collective-permute-start(bf16[64,2048]{1,0:T(8,128)(2,1)S(1)} %get-tuple-element.44), channel_id=1, source_target_pairs={{0,1},{1,0},{2,3},{3,2},{4,5},{5,4},{6,7},{7,6},{8,9},{9,8},{10,11... | collective-permute-start | bytes 786440 | tf_op jit(solution)/shard_map/ppermute | solution.py:31
  62.8 18.6 %copy-start.11 = (f32[32,2]{0,1:T(2,128)S(1)}, f32[32,2]{0,1:T(2,128)}, u32[]{:S(2)}) copy-start(f32[32,2]{0,1:T(2,128)} %param.24) | copy-start | bytes 772
  62.8 18.6 %copy-start.12 = (s32[32,2]{0,1:T(2,128)S(1)}, s32[32,2]{0,1:T(2,128)}, u32[]{:S(2)}) copy-start(s32[32,2]{0,1:T(2,128)} %param.23) | copy-start | bytes 772
  62.8 2.9 %collective-permute-start.14 = (bf16[128,2048]{1,0:T(8,128)(2,1)S(1)}, bf16[128,2048]{1,0:T(8,128)(2,1)S(1)}, u32[]{:S(2)}, u32[]{:S(2)}) collective-permute-start(bf16[128,2048]{1,0:T(8,128)(2,1)S(1)} %get-tuple-element.42), channel_id=1, source_target_pairs={{0,1},{1,0},{2,3},{3,2},{4,5},{5,4},{6,7},{7,6},{8,9},{9,8},{10,11... | collective-permute-start | bytes 1572872 | tf_op jit(solution)/shard_map/ppermute | solution.py:31
  63.5 17.9 %collective-permute-start.9 = (bf16[32,2048]{1,0:T(8,128)(2,1)S(1)}, bf16[32,2048]{1,0:T(8,128)(2,1)S(1)}, u32[]{:S(2)}, u32[]{:S(2)}) collective-permute-start(bf16[32,2048]{1,0:T(8,128)(2,1)S(1)} %slice.49), channel_id=1, source_target_pairs={{0,2},{1,3},{2,0},{3,1},{4,6},{5,7},{6,4},{7,5},{8,10},{9,11},{10,... | collective-permute-start | bytes 393224 | tf_op jit(solution)/shard_map/ppermute | solution.py:31
  64.5 8.2 %collective-permute-start.22 = (bf16[32,2048]{1,0:T(8,128)(2,1)S(1)}, bf16[32,2048]{1,0:T(8,128)(2,1)S(1)}, u32[]{:S(2)}, u32[]{:S(2)}) collective-permute-start(bf16[32,2048]{1,0:T(8,128)(2,1)S(1)} %slice.55), channel_id=1, source_target_pairs={{0,2},{1,3},{2,0},{3,1},{4,6},{5,7},{6,4},{7,5},{8,10},{9,11},{10,... | collective-permute-start | bytes 393224 | tf_op jit(solution)/shard_map/ppermute | solution.py:31
  65.9 11.5 %collective-permute-start.15 = (bf16[64,2048]{1,0:T(8,128)(2,1)S(1)}, bf16[64,2048]{1,0:T(8,128)(2,1)S(1)}, u32[]{:S(2)}, u32[]{:S(2)}) collective-permute-start(bf16[64,2048]{1,0:T(8,128)(2,1)S(1)} %slice.51), channel_id=1, source_target_pairs={{0,2},{1,3},{2,0},{3,1},{4,6},{5,7},{6,4},{7,5},{8,10},{9,11},{10,... | collective-permute-start | bytes 786440 | tf_op jit(solution)/shard_map/ppermute | solution.py:31
  72.8 8.7 %collective-permute-start.23 = (bf16[32,2048]{1,0:T(8,128)(2,1)S(1)}, bf16[32,2048]{1,0:T(8,128)(2,1)S(1)}, u32[]{:S(2)}, u32[]{:S(2)}) collective-permute-start(bf16[32,2048]{1,0:T(8,128)(2,1)S(1)} %add_convert_fusion.5), channel_id=1, source_target_pairs={{0,8},{4,12},{8,0},{12,4},{1,9},{5,13},{9,1},{13,5},{2,10},{6,14},... | collective-permute-start | bytes 393224 | tf_op jit(solution)/shard_map/ppermute | solution.py:26
  77.5 7.8 %collective-permute-start.17 = (bf16[32,2048]{1,0:T(8,128)(2,1)S(1)}, bf16[32,2048]{1,0:T(8,128)(2,1)S(1)}, u32[]{:S(2)}, u32[]{:S(2)}) collective-permute-start(bf16[32,2048]{1,0:T(8,128)(2,1)S(1)} %get-tuple-element.50), channel_id=1, source_target_pairs={{0,4},{4,8},{8,12},{12,0},{1,5},{5,9},{9,13},{13,1},{2,6},{6,10},{... | collective-permute-start | bytes 393224 | tf_op jit(solution)/shard_map/ppermute | solution.py:26
  80.1 6.6 %collective-permute-start.16 = (bf16[32,2048]{1,0:T(8,128)(2,1)S(1)}, bf16[32,2048]{1,0:T(8,128)(2,1)S(1)}, u32[]{:S(2)}, u32[]{:S(2)}) collective-permute-start(bf16[32,2048]{1,0:T(8,128)(2,1)S(1)} %get-tuple-element.49), channel_id=1, source_target_pairs={{0,12},{4,0},{8,4},{12,8},{1,13},{5,1},{9,5},{13,9},{2,14},{6,2},{... | collective-permute-start | bytes 393224 | tf_op jit(solution)/shard_map/ppermute | solution.py:26
